TPU v7x, 256 devices: a whole 4x4x8 slice. The times are simulated.
256 devices in a mesh: kv: 32 (over z, x), tp: 8 (over y, core).
Axes of the slice: x: 4, y: 4, z: 8, core: 2. Of those that a mesh axis runs over, the one named last changes fastest.
Arguments:
- tokens: bfloat16 [384, 2048], P(None, 'kv'), may hold values from -40 to 40
- norm_gain: float32 [2048], P('kv'), may hold values from 0.1 to 1.9
- w_query: bfloat16 [2048, 1024], P('kv', 'tp'), may hold values from -0.088388348 to 0.088388348
- w_key: bfloat16 [2048, 1024], P('kv', 'tp'), may hold values from -0.125 to 0.125
- w_value: bfloat16 [2048, 1024], P('kv', 'tp'), may hold values from -0.125 to 0.125
- w_gate: bfloat16 [2048, 16], replicated, may hold values from -0.125 to 0.125
- gate_bias: float32 [16], replicated, may hold values from -1 to 3
- w_out: bfloat16 [1024, 2048], P('tp', 'kv'), may hold values from -0.1875 to 0.1875
- keys_cache: bfloat16 [24, 16384, 1024], P(None, 'kv', 'tp'), may hold values from -512 to 512
- values_cache: bfloat16 [24, 16384, 1024], P(None, 'kv', 'tp'), may hold values from -6 to 6
- cum_gates: float32 [24, 16, 16384], P(None, 'tp', 'kv'), may hold values from -16784 to 0, as said below
- prior_len: int32 [24], replicated, may hold values from 8192 to 16362, as said below
- accepted: int32 [24], replicated, may hold values from 0 to 6
- parents: int32 [24, 16], replicated, may hold values from -1 to 14, as said below
Outputs:
- mixed_rows: bfloat16 [384, 2048], P('tp', 'kv')
- keys_out: bfloat16 [24, 16384, 1024], P(None, 'kv', 'tp')
- values_out: bfloat16 [24, 16384, 1024], P(None, 'kv', 'tp')
Inputs may be any that keep to these rules, and one draw needn't show every extreme that they name: parents[b, 0] = -1 and 0 <= parents[b, j] < j for later j. prior_len is at least half of 16384, and prior_len + accepted + 16 <= 16384. `cum_gates`: non-increasing along positions.
All inputs are finite; a program needn't handle non-finite values.
Results may differ from a plain program's by a relative error of at most 0.04.
Values may be sent and summed in bfloat16 or wider, within the bound.
No kernel may reach another device: no remote copies, remote signals or barrier semaphores. Data moves between devices by JAX's collectives and lax.ppermute only.
A program may use at most 64 MiB of HBM per device.

v0:
```python
import jax
import jax.numpy as jnp
from jax import lax
from jax.sharding import Mesh
from jax.sharding import PartitionSpec as P

D = 2048
HEAD = 64
PROPS = 16
KV = ("kv_0", "kv_1")


masked_score = -1e30
norm_eps = 1e-06


def from_everyone(shard, axis):
    count = lax.axis_size(axis)
    return lax.all_to_all(
        jnp.broadcast_to(shard[None], (count, *shard.shape)), axis, 0, 0, tiled=True
    )


def of_everyone(shard, axis):
    return from_everyone(shard, axis).sum(axis=0)


def in_one(arrays, axis):
    ends = [0]
    for a in arrays:
        ends.append(ends[-1] + a.size)
    running = of_everyone(jnp.concatenate([a.ravel() for a in arrays]), axis)
    return tuple((running[b:e].reshape(a.shape) for a, b, e in zip(arrays, ends, ends[1:])))


def in_blocks(shard, dim, count):
    lengths = shard.shape
    blocks = shard.reshape(*lengths[:dim], count, lengths[dim] // count, *lengths[dim + 1 :])
    return jnp.moveaxis(blocks, dim, 0)


def summed_on_arrival(shard, axis, dim):
    count = lax.axis_size(axis)
    blocks = lax.all_to_all(in_blocks(shard, dim, count), axis, 0, 0, tiled=True)
    return jnp.sum(blocks.astype(jnp.float32), axis=0)


def joined_along(blocks, dim):
    blocks = jnp.moveaxis(blocks, 0, dim)
    lengths = blocks.shape
    return blocks.reshape(*lengths[:dim], lengths[dim] * lengths[dim + 1], *lengths[dim + 2 :])


def collect(shard, axis, dim):
    blocks = from_everyone(shard, axis)
    return joined_along(blocks, dim)


def collected_together(shard, axis):
    leaves = jax.tree.leaves(shard)
    sequence = sorted(range(len(leaves)), key=lambda k: -leaves[k].size)
    width = (1, *leaves[sequence[0]].shape)[-1]
    lines = [
        jnp.pad(leaves[k].reshape(-1), (0, -leaves[k].size % width)).reshape(-1, width)
        for k in sequence
    ]
    both, at, found = (lax.all_gather(jnp.concatenate(lines), axis), 0, {})
    for k, line in zip(sequence, lines):
        section = both[:, at : at + len(line)].reshape(len(both), -1)
        found[k] = section[:, : leaves[k].size].reshape(-1, *leaves[k].shape)
        at += len(line)
    numbers = iter(range(len(leaves)))
    return jax.tree.map(lambda _: found[next(numbers)], shard)


def combined_by_axis(shard, axes, combine):
    for axis in axes:
        pieces = collected_together(shard, axis)
        shard = jax.tree.map(lambda part: part[0], pieces)
        for k in range(1, lax.axis_size(axis)):
            shard = combine(shard, jax.tree.map(lambda part: part[k], pieces))
    return shard


def ancestry(parents):
    columns = jnp.arange(PROPS, dtype=jnp.int32)
    parent_link = (parents[:, :, None] == columns[None, None, :]).astype(jnp.float32)
    reached = jnp.eye(PROPS, dtype=jnp.float32)[None] + parent_link
    for squaring in range(PROPS.bit_length()):
        reached = jnp.minimum(jnp.einsum("bij,bjk->bik", reached, reached), 1.0)
    return reached


def combine(earlier, later):
    max_one, sum_one, val_one = earlier
    max_two, sum_two, val_two = later
    joint = jnp.maximum(max_one, max_two)
    factor_one = jnp.exp(max_one - joint)
    factor_two = jnp.exp(max_two - joint)
    return (
        joint,
        factor_one * sum_one + factor_two * sum_two,
        factor_one[..., None] * val_one + factor_two[..., None] * val_two,
    )


def shards(
    tokens,
    norm_gain,
    w_query,
    w_key,
    w_value,
    w_gate,
    gate_bias,
    w_out,
    keys_cache,
    values_cache,
    cum_gates,
    prior_len,
    accepted,
    parents,
):
    row_count = tokens.shape[0]
    column_count = tokens.shape[1]
    seq_count = keys_cache.shape[0]
    length = keys_cache.shape[1]
    head_width = w_query.shape[1]
    head_count = head_width // HEAD
    kv_index = lax.axis_index(KV)
    tp_index = lax.axis_index("tp")
    floats = tokens.astype(jnp.float32)
    square_part = jnp.sum(floats * floats, axis=1)
    scaled = (floats * norm_gain).astype(jnp.bfloat16)
    gate_rows = lax.dynamic_slice_in_dim(w_gate, kv_index * column_count, column_count, 0)
    gate_cols = lax.dynamic_slice_in_dim(gate_rows, tp_index * head_count, head_count, 1)
    gate_part = jnp.dot(scaled, gate_cols, preferred_element_type=jnp.float32)
    bias_local = lax.dynamic_slice_in_dim(gate_bias, tp_index * head_count, head_count, 0)
    gate_sum, square_sum = in_one((gate_part, square_part), KV)
    inv_rms = lax.rsqrt(square_sum / D + norm_eps)
    row_share = row_count // lax.axis_size(KV)
    summed = summed_on_arrival(
        jnp.concatenate(
            [
                jnp.dot(scaled, w_query, preferred_element_type=jnp.float32),
                jnp.dot(scaled, w_key, preferred_element_type=jnp.float32),
                jnp.dot(scaled, w_value, preferred_element_type=jnp.float32),
            ],
            axis=1,
        ).astype(jnp.bfloat16),
        KV,
        0,
    )
    own_rms = lax.dynamic_slice_in_dim(inv_rms, kv_index * row_share, row_share, 0)
    rounded = (own_rms[:, None] * summed).astype(jnp.bfloat16)
    joined = collect(rounded, KV, 0)
    queries = joined[:, :head_width]
    new_keys = joined[:, head_width : 2 * head_width]
    new_values = joined[:, 2 * head_width :]
    log_gates = jax.nn.log_sigmoid(inv_rms[:, None] * gate_sum + bias_local).reshape(
        seq_count, PROPS, head_count
    )
    reached = ancestry(parents)
    tree_gates = jnp.einsum("bij,bjh->bih", reached, log_gates)
    filled = prior_len + accepted
    offset = kv_index * length
    local_last = filled - 1 - offset
    owner_mask = (local_last >= 0) & (local_last < length)
    index_last = jnp.broadcast_to(
        jnp.clip(local_last, 0, length - 1)[:, None, None], (seq_count, head_count, 1)
    )
    last_gate = jnp.take_along_axis(cum_gates, index_last, axis=2)[:, :, 0]
    prop_cum = last_gate[:, None, :] + tree_gates
    scale = HEAD ** (-0.5)
    query_four = queries.reshape(seq_count, PROPS, head_count, HEAD)
    keys_four = keys_cache.reshape(seq_count, length, head_count, HEAD)
    values_four = values_cache.reshape(seq_count, length, head_count, HEAD)
    newk_four = new_keys.reshape(seq_count, PROPS, head_count, HEAD)
    newv_four = new_values.reshape(seq_count, PROPS, head_count, HEAD)
    positions = offset + jnp.arange(length, dtype=jnp.int32)
    valid_keys = positions[None, :] < filled[:, None]
    scores = (
        jnp.einsum("bihd,bphd->bhip", query_four, keys_four, preferred_element_type=jnp.float32)
        * scale
    )
    scores = jnp.where(
        valid_keys[:, None, None, :], scores - cum_gates[:, :, None, :], masked_score
    )
    tree_scores = (
        jnp.einsum("bihd,bjhd->bhij", query_four, newk_four, preferred_element_type=jnp.float32)
        * scale
    )
    tree_scores = tree_scores - jnp.transpose(prop_cum, (0, 2, 1))[:, :, None, :]
    tree_live = (reached > 0.5)[:, None, :, :] & owner_mask[:, None, None, None]
    tree_scores = jnp.where(tree_live, tree_scores, masked_score)
    local_max = jnp.maximum(jnp.max(scores, axis=3), jnp.max(tree_scores, axis=3))
    weights = jnp.where(valid_keys[:, None, None, :], jnp.exp(scores - local_max[..., None]), 0.0)
    tree_weights = jnp.where(tree_live, jnp.exp(tree_scores - local_max[..., None]), 0.0)
    local_sum = jnp.sum(weights, axis=3) + jnp.sum(tree_weights, axis=3)
    local_values = jnp.einsum(
        "bhip,bphd->bhid",
        weights.astype(jnp.bfloat16),
        values_four,
        preferred_element_type=jnp.float32,
    )
    local_values = local_values + jnp.einsum(
        "bhij,bjhd->bhid",
        tree_weights.astype(jnp.bfloat16),
        newv_four,
        preferred_element_type=jnp.float32,
    )
    local_values = lax.optimization_barrier(local_values.astype(jnp.bfloat16)).astype(jnp.float32)
    top_score, grand_total, weighted = combined_by_axis(
        (local_max, local_sum, local_values), KV, combine
    )
    result = weighted / grand_total[..., None]
    attended = (
        jnp.transpose(result, (0, 2, 1, 3)).reshape(row_count, head_width).astype(jnp.bfloat16)
    )
    partial_value = jnp.dot(attended, w_out, preferred_element_type=jnp.float32)
    mixed_rows = summed_on_arrival(partial_value.astype(jnp.bfloat16), "tp", 0).astype(jnp.bfloat16)
    slot_index = positions[None, :] - filled[:, None]
    inside = (slot_index >= 0) & (slot_index < PROPS)
    selector = (slot_index[:, :, None] == jnp.arange(PROPS, dtype=jnp.int32)[None, None, :]).astype(
        jnp.bfloat16
    )
    placed_keys = jnp.einsum(
        "bpj,bjc->bpc",
        selector,
        new_keys.reshape(seq_count, PROPS, head_width),
        preferred_element_type=jnp.float32,
    ).astype(jnp.bfloat16)
    placed_values = jnp.einsum(
        "bpj,bjc->bpc",
        selector,
        new_values.reshape(seq_count, PROPS, head_width),
        preferred_element_type=jnp.float32,
    ).astype(jnp.bfloat16)
    keys_out = jnp.where(inside[:, :, None], placed_keys, keys_cache)
    values_out = jnp.where(inside[:, :, None], placed_values, values_cache)
    return (mixed_rows, keys_out, values_out)


def solution(mesh):
    torus = Mesh(mesh.devices.reshape(8, 4, mesh.shape["tp"]), ("kv_0", "kv_1", "tp"))
    in_specs = (
        P(None, KV),
        P(KV),
        P(KV, "tp"),
        P(KV, "tp"),
        P(KV, "tp"),
        P(),
        P(),
        P("tp", KV),
        P(None, KV, "tp"),
        P(None, KV, "tp"),
        P(None, "tp", KV),
        P(),
        P(),
        P(),
    )
    out_specs = (P("tp", KV), P(None, KV, "tp"), P(None, KV, "tp"))
    return jax.shard_map(
        shards, mesh=torus, in_specs=in_specs, out_specs=out_specs, check_vma=False
    )
```

profile of v0, /device:TPU:8, one launch (start us, length us, event | category | flops | bytes accessed | tf_op | source)
XLA Modules:
  0.0 172.0 jit_solution(7093638999539466821)
XLA Ops:
  7.2 0.9 fusion.43
  8.1 1.1 fusion.84
  9.2 0.1 reshape.915
  9.4 0.7 broadcast_in_dim.65
  10.1 11.3 %all-to-all-start = ((f32[32,1,1152]{2,1,0:T(1,128)}), f32[32,1,1152]{2,1,0:T(1,128)S(1)}, u32[]{:S(2)}, u32[]{:S(2)}) async-start(f32[32,1,1152]{2,1,0:T(1,128)} %broadcast_in_dim.65), calls=%async_computation | async-start | bytes 294912 | tf_op jit(solution)/shard_map/all_to_all | solution.py:19
  21.4 0.7 compare_and_fusion.2
  22.1 0.8 copy.286
  22.9 0.3 convolution_minimum_fusion.4
  23.2 0.4 convolution_minimum_fusion.2
  23.6 1.1 convolution_convert_fusion.2
  24.8 0.3 convolution_convert_fusion.1
  25.1 0.3 convolution_convert_fusion
  25.5 0.8 pad_maximum_fusion
  26.3 1.0 compare_and_fusion
  27.3 4.9 %all-to-all-done = f32[32,1,1152]{2,1,0:T(1,128)S(1)} async-done(((f32[32,1,1152]{2,1,0:T(1,128)}), f32[32,1,1152]{2,1,0:T(1,128)S(1)}, u32[]{:S(2)}, u32[]{:S(2)}) %all-to-all-start) | async-done | bytes 147488 | tf_op jit(solution)/shard_map/all_to_all | solution.py:19
  32.2 5.0 %all-to-all-start.1 = ((bf16[32,12,384]{2,1,0:T(8,128)(2,1)}), bf16[32,12,384]{2,1,0:T(8,128)(2,1)}, u32[]{:S(2)}, u32[]{:S(2)}) async-start(bf16[32,12,384]{2,1,0:T(8,128)(2,1)} %pad_maximum_fusion), calls=%async_computation.1 | async-start | bytes 786432 | tf_op jit(solution)/shard_map/all_to_all | solution.py:44
  37.4 1.3 gather_fusion
  38.9 0.2 copy.287
  39.1 4.8 %copy.284 = bf16[24,512,128]{1,2,0:T(8,128)(2,1)} copy(bf16[24,512,128]{2,1,0:T(8,128)(2,1)} %param.22) | data formatting | bytes 6291456 | tf_op args[8]
  43.9 2.8 %copy.297 = bf16[24,512,128]{1,2,0:T(8,128)(2,1)} copy(bf16[24,512,128]{2,1,0:T(8,128)(2,1)S(1)} %copy-done.2) | data formatting | bytes 6291456 | tf_op args[9]
  47.0 5.1 %all-to-all-done.1 = bf16[32,12,384]{2,1,0:T(8,128)(2,1)} async-done(((bf16[32,12,384]{2,1,0:T(8,128)(2,1)}), bf16[32,12,384]{2,1,0:T(8,128)(2,1)}, u32[]{:S(2)}, u32[]{:S(2)}) %all-to-all-start.1) | async-done | bytes 294944 | tf_op jit(solution)/shard_map/all_to_all | solution.py:44
  52.1 1.1 convert_reduce_fusion
  53.2 0.8 broadcast_in_dim.66
  54.0 4.6 %all-to-all-start.2 = ((bf16[32,12,384]{2,1,0:T(8,128)(2,1)}), bf16[32,12,384]{2,1,0:T(8,128)(2,1)S(1)}, u32[]{:S(2)}, u32[]{:S(2)}) async-start(bf16[32,12,384]{2,1,0:T(8,128)(2,1)} %broadcast_in_dim.66), calls=%async_computation.2 | async-start | bytes 786432 | tf_op jit(solution)/shard_map/all_to_all | solution.py:19
  58.9 0.2 reshape.920
  59.1 0.2 copy.293
  59.5 0.2 convolution_add_fusion.1
  59.7 13.1 %all-to-all-done.2 = bf16[32,12,384]{2,1,0:T(8,128)(2,1)S(1)} async-done(((bf16[32,12,384]{2,1,0:T(8,128)(2,1)}), bf16[32,12,384]{2,1,0:T(8,128)(2,1)S(1)}, u32[]{:S(2)}, u32[]{:S(2)}) %all-to-all-start.2) | async-done | bytes 294944 | tf_op jit(solution)/shard_map/all_to_all | solution.py:19
  73.2 0.2 fusion.33
  73.4 0.3 copy.290
  73.9 2.6 %fusion.99 = (f32[24,2,16]{2,1,0:T(2,128)S(1)}, f32[24,2,16,512]{3,2,1,0:T(8,128)S(1)}) fusion(f32[24,2,512]{2,1,0:T(2,128)S(1)} %copy-done.1, bf16[24,512,2,64]{1,3,2,0:T(8,128)(2,1)} %bitcast.362, bf16[24,16,2,64]{3,2,1,0:T(2,128)(2,1)S(1)} %reshape.917, pred[24,512]{1,0:T(8,128)(4,1)S(1)} %get-tuple-element.91), kind=kOutput, calls=%fused_computation.196 | convolution fusion | flops 51903744 | bytes 4930560 | tf_op jit(solution)/shard_map/bihd,bphd->bhip/dot_general | solution.py:182
  76.6 0.1 fusion.41
  76.8 0.4 copy.299
  77.3 0.5 fusion
  77.8 0.2 fusion.31
  78.0 2.9 %fusion.2 = bf16[24,2,16,64]{3,2,1,0:T(8,128)(2,1)S(1)} fusion(f32[24,2,16,64]{3,2,1,0:T(8,128)S(1)} %fusion.31, bf16[24,512,2,64]{1,3,2,0:T(8,128)(2,1)} %bitcast.361, f32[24,2,16,512]{3,2,1,0:T(8,128)S(1)} %get-tuple-element.93, f32[24,2,16]{2,1,0:T(2,128)S(1)} %max.309, pred[24,512]{1,0:T(8,128)(4,1)S(1)} %get-tuple-element.91), kind=kOutput, calls=%fused_computation.8 | convolution fusion | flops 51609600 | bytes 5028864 | tf_op jit(solution)/shard_map/bhip,bphd->bhid/dot_general | solution.py:199
  81.0 0.1 copy.302
  81.5 0.8 maximum_bitcast_fusion
  82.4 7.9 %convert_select_fusion = bf16[24,512,128]{2,1,0:T(8,128)(2,1)} fusion(bf16[24,512,128]{2,1,0:T(8,128)(2,1)} %param.23, pred[24,512]{1,0:T(8,128)(4,1)S(1)} %get-tuple-element.90, bf16[24,16,128]{2,1,0:T(8,128)(2,1)S(1)} %bitcast.368, s32[24,512]{1,0:T(8,128)S(1)} %broadcast_subtract_fusion), kind=kOutput, calls=%fused_computation.1 | convolution fusion | flops 53673984 | bytes 6451200 | tf_op jit(solution)/shard_map/bpj,bjc->bpc/dot_general | solution.py:232
  90.3 28.4 %all-gather.6.cloned.1.call-done = f32[8,792,64]{1,2,0:T(8,128)} async-done(((f32[1,792,64]{1,2,0:T(8,128)}), f32[8,792,64]{1,2,0:T(8,128)}) %all-gather.6.cloned.1.call-update) | async-done | bytes 1622032 | tf_op jit(solution)/shard_map/all_gather | solution.py:67
  118.6 1.3 fusion.95
  121.2 0.1 copy.354
  122.1 0.2 fusion.11
  122.4 15.3 %all-gather.3 = f32[4,792,64]{1,2,0:T(8,128)S(1)} all-gather(f32[1,792,64]{1,2,0:T(8,128)S(1)} %maximum_bitcast_fusion.1), channel_id=3, replica_groups=mesh['kv_0'=8,'kv_1'=4,'tp'=8] {'kv_1'}, dimensions={0}, use_global_device_ids=true | all-gather | bytes 1013760 | tf_op jit(solution)/shard_map/all_gather | solution.py:67
  137.8 0.9 copy.361
  138.7 0.9 copy.362
  139.6 0.9 copy.363
  140.5 0.9 copy.364
  141.5 0.7 squeeze.167
  142.3 0.7 squeeze.166
  143.2 0.7 squeeze.164
  144.0 0.7 squeeze.156
  144.8 0.7 squeeze.157
  145.5 0.7 squeeze.158
  146.3 0.7 squeeze.159
  147.0 1.1 multiply_add_fusion
  148.1 2.1 %fusion.37 = bf16[24,16,2,64]{3,1,2,0:T(8,128)(2,1)S(1)} fusion(f32[24,2,16]{2,1,0:T(2,128)S(1)} %bitcast.370, f32[24,2,16,64]{3,2,1,0:T(8,128)} %bitcast.366, f32[24,2,16]{2,1,0:T(2,128)S(1)} %bitcast.376, f32[24,2,16,64]{3,2,1,0:T(8,128)} %bitcast.365, f32[24,2,16]{2,1,0:T(2,128)S(1)} %bitcast.374, f32[24,2,16,64]{3,2,1,0:T(8,128)} %bitcast.364, ...), kind=kLoop, calls=%fused_computation.71 | loop fusion | flops 540672 | bytes 906240 | tf_op jit(solution)/shard_map/convert_element_type | solution.py:217
  150.2 0.2 copy.335
  150.4 0.8 convert_element_type.70
  151.1 1.1 convolution_convert_fusion.3
  152.3 0.7 reshape.948
  153.1 4.8 %all-to-all-start.3 = ((bf16[8,2,1536]{2,1,0:T(2,128)(2,1)}), bf16[8,2,1536]{2,1,0:T(2,128)(2,1)S(1)}, u32[]{:S(2)}, u32[]{:S(2)}) async-start(bf16[8,2,1536]{2,1,0:T(2,128)(2,1)} %reshape.948), calls=%async_computation.3 | async-start | bytes 98304 | tf_op jit(solution)/shard_map/all_to_all | solution.py:44
  157.9 6.5 %convert_select_fusion.1 = bf16[24,512,128]{2,1,0:T(8,128)(2,1)} fusion(bf16[24,512,128]{2,1,0:T(8,128)(2,1)S(1)} %copy-done.3, pred[24,512]{1,0:T(8,128)(4,1)} %copy-done.6, bf16[24,16,128]{2,1,0:T(8,128)(2,1)S(1)} %bitcast.367, s32[24,512]{1,0:T(8,128)S(1)} %broadcast_subtract_fusion), kind=kOutput, calls=%fused_computation.2 | convolution fusion | flops 53673984 | bytes 6451200 | tf_op jit(solution)/shard_map/bpj,bjc->bpc/dot_general | solution.py:226
  164.5 0.6 reduce_sum.62
  (119 shorter events, 5.9 us)
Async XLA Ops:
  7.2 0.9 copy-start
  7.2 17.6 %copy-start.5 = (bf16[384,64]{0,1:T(8,128)(2,1)S(1)}, bf16[384,64]{0,1:T(8,128)(2,1)}, u32[]{:S(2)}) copy-start(bf16[384,64]{0,1:T(8,128)(2,1)} %param.14) | copy-start | bytes 147460
  7.2 17.6 %copy-start.9 = (f32[64]{0:T(128)S(1)}, f32[64]{0:T(128)}, u32[]{:S(2)}) copy-start(f32[64]{0:T(128)} %param.15) | copy-start | bytes 772
  7.2 17.6 %copy-start.7 = (bf16[64,128]{1,0:T(8,128)(2,1)S(1)}, bf16[64,128]{1,0:T(8,128)(2,1)}, u32[]{:S(2)}) copy-start(bf16[64,128]{1,0:T(8,128)(2,1)} %param.17) | copy-start | bytes 49156
  7.2 17.9 %copy-start.8 = (bf16[64,128]{1,0:T(8,128)(2,1)S(1)}, bf16[64,128]{1,0:T(8,128)(2,1)}, u32[]{:S(2)}) copy-start(bf16[64,128]{1,0:T(8,128)(2,1)} %param.18) | copy-start | bytes 49156
  10.1 22.1 %all-to-all-start = ((f32[32,1,1152]{2,1,0:T(1,128)}), f32[32,1,1152]{2,1,0:T(1,128)S(1)}, u32[]{:S(2)}, u32[]{:S(2)}) async-start(f32[32,1,1152]{2,1,0:T(1,128)} %broadcast_in_dim.65), calls=%async_computation | async-start | bytes 294912 | tf_op jit(solution)/shard_map/all_to_all | solution.py:19
  22.1 24.5 %copy-start.10 = (s32[24]{0:T(128)}, s32[24]{0:T(128)S(1)}, u32[]{:S(2)}) copy-start(s32[24]{0:T(128)S(1)} %get-tuple-element.33) | copy-start | bytes 292
  23.6 13.8 %copy-start.1 = (f32[24,2,512]{2,1,0:T(2,128)S(1)}, f32[24,2,512]{2,1,0:T(2,128)}, u32[]{:S(2)}) copy-start(f32[24,2,512]{2,1,0:T(2,128)} %param.24) | copy-start | bytes 294916
  32.2 19.9 %all-to-all-start.1 = ((bf16[32,12,384]{2,1,0:T(8,128)(2,1)}), bf16[32,12,384]{2,1,0:T(8,128)(2,1)}, u32[]{:S(2)}, u32[]{:S(2)}) async-start(bf16[32,12,384]{2,1,0:T(8,128)(2,1)} %pad_maximum_fusion), calls=%async_computation.1 | async-start | bytes 786432 | tf_op jit(solution)/shard_map/all_to_all | solution.py:44
  37.4 1.4 copy-start.12
  39.1 4.8 %copy-start.2 = (bf16[24,512,128]{2,1,0:T(8,128)(2,1)S(1)}, bf16[24,512,128]{2,1,0:T(8,128)(2,1)}, u32[]{:S(2)}) copy-start(bf16[24,512,128]{2,1,0:T(8,128)(2,1)} %param.23) | copy-start | bytes 9437188
  46.7 12.8 %copy-start.13 = (bf16[24,16,16]{2,1,0:T(8,128)(2,1)S(1)}, bf16[24,16,16]{2,1,0:T(8,128)(2,1)}, u32[]{:S(2)}) copy-start(bf16[24,16,16]{2,1,0:T(8,128)(2,1)} %get-tuple-element.95) | copy-start | bytes 36868
  46.8 35.6 %copy-start.6 = (pred[24,512]{1,0:T(8,128)(4,1)}, pred[24,512]{1,0:T(8,128)(4,1)S(1)}, u32[]{:S(2)}) copy-start(pred[24,512]{1,0:T(8,128)(4,1)S(1)} %get-tuple-element.90) | copy-start | bytes 36868
  54.0 18.8 %all-to-all-start.2 = ((bf16[32,12,384]{2,1,0:T(8,128)(2,1)}), bf16[32,12,384]{2,1,0:T(8,128)(2,1)S(1)}, u32[]{:S(2)}, u32[]{:S(2)}) async-start(bf16[32,12,384]{2,1,0:T(8,128)(2,1)} %broadcast_in_dim.66), calls=%async_computation.2 | async-start | bytes 786432 | tf_op jit(solution)/shard_map/all_to_all | solution.py:19
  58.6 60.0 %all-gather.6.cloned.1.call-start = ((), (), s32[]{:S(2)}) async-start(), calls=%async_computation.4 | async-start | bytes 2064384 | tf_op jit(solution)/shard_map/all_gather | solution.py:67
  80.9 1.4 copy-start.11
  118.6 3.5 %copy-start.4 = (f32[8,792,64]{1,2,0:T(8,128)S(1)}, f32[8,792,64]{1,2,0:T(8,128)}, u32[]{:S(2)}) copy-start(f32[8,792,64]{1,2,0:T(8,128)} %all-gather.6.cloned.1.call-done) | copy-start | bytes 4866052
  146.2 11.7 %copy-start.3 = (bf16[24,512,128]{2,1,0:T(8,128)(2,1)S(1)}, bf16[24,512,128]{2,1,0:T(8,128)(2,1)}, u32[]{:S(2)}) copy-start(bf16[24,512,128]{2,1,0:T(8,128)(2,1)} %param.22) | copy-start | bytes 9437188
  153.1 11.3 %all-to-all-start.3 = ((bf16[8,2,1536]{2,1,0:T(2,128)(2,1)}), bf16[8,2,1536]{2,1,0:T(2,128)(2,1)S(1)}, u32[]{:S(2)}, u32[]{:S(2)}) async-start(bf16[8,2,1536]{2,1,0:T(2,128)(2,1)} %reshape.948), calls=%async_computation.3 | async-start | bytes 98304 | tf_op jit(solution)/shard_map/all_to_all | solution.py:44
Sparse Core Ops, SparseCore 0:
  82.4 36.1 all-gather.5
where the time goes:
time: 174 us; the launch traced here: 172 us
  waiting for transfers between devices  51.5 us (30%)
  local copies, waits for them, and re-layouts  29.2 us (17%)
  matrix products  25.9 us (15%)
  starting transfers between devices  25.8 us (15%)
  blocking collectives  15.3 us (9%)
  between operations  14.6 us (8%)
  other arithmetic  9.74 us (6%)
    all_gather x1, waiting for transfers between devices, collected_together(): both, at, found = (lax.all_gather(jnp.concatenate(lines), axis), 0, {})  28.4 us
    all_to_all x2, waiting for transfers between devices, from_everyone(): lax.all_to_all(jnp.broadcast_to(shard[None], (count, *shard.shape)), axis...  18 us
    all_to_all x2, starting transfers between devices, from_everyone(): lax.all_to_all(jnp.broadcast_to(shard[None], (count, *shard.shape)), axis...  15.9 us
    all_gather x1, blocking collectives, collected_together(): both, at, found = (lax.all_gather(jnp.concatenate(lines), axis), 0, {})  15.3 us
    unnamed x55, local copies, waits for them, and re-layouts  14.2 us
    all_to_all x2, starting transfers between devices, summed_on_arrival(): lax.all_to_all(in_blocks(shard, dim, count), axis, 0, 0, tiled=True)  9.81 us
    dot_general x1, matrix products, shards(): jnp.einsum('bpj,bjc->bpc', selector, new_values.reshape(seq_count, PROPS,...  7.86 us
    dot_general x1, matrix products, shards(): jnp.einsum('bpj,bjc->bpc', selector, new_keys.reshape(seq_count, PROPS, h...  6.47 us
  transfers between devices with their start and end apart: 5, of which 4 were waited for; matrix products, arithmetic and copies ran while one was open for 18% of the time, Pallas kernels for 0%

commit v1 on v0

v1 whole, which is shorter than its diff:
```python
import jax
import jax.numpy as jnp
from jax import lax
from jax.experimental import pallas as pl
from jax.experimental.pallas import tpu as pltpu
from jax.sharding import Mesh
from jax.sharding import PartitionSpec as P

D = 2048
HEAD = 64
PROPS = 16
ROWS = 384
SEQS = 24
LEN = 512
WIDTH = 128
N_KV = 32
N_TP = 8
STATS = 24
WINDOW = 32
KV = ("kv_0", "kv_1")

masked_score = -1e30
lowest_max = -1e20
norm_eps = 1e-06

VM = pl.BlockSpec(memory_space=pltpu.VMEM)
SM = pl.BlockSpec(memory_space=pltpu.SMEM)
ANY = pl.BlockSpec(memory_space=pl.ANY)
bf16 = jnp.bfloat16
f32 = jnp.float32


def iota(shape, dim):
    return lax.broadcasted_iota(jnp.int32, shape, dim)


def high_low(x):
    high = x.astype(bf16).astype(f32)
    return high, (x - high).astype(bf16).astype(f32)


def dot_t(a, b):
    return lax.dot_general(a, b, (((1,), (1,)), ((), ())), preferred_element_type=f32)


def project_kernel(
    ids, prior, accepted, tokens, gain, w_q, w_k, w_v, w_gate, cum, out, gate_rows, gates, sem
):
    kv, tp = ids[0], ids[1]
    copy = pltpu.make_async_copy(
        w_gate.at[pl.ds(pl.multiple_of(kv * 64, 64), 64)], gate_rows, sem
    )
    copy.start()
    floats = tokens[...].astype(f32)
    scaled = (floats * gain[...]).astype(bf16)
    for n, w in enumerate((w_q, w_k, w_v)):
        part = jnp.dot(scaled, w[...], preferred_element_type=f32).astype(bf16)
        out[0:SEQS, :, n * WIDTH : (n + 1) * WIDTH] = part.reshape(SEQS, PROPS, WIDTH)
    squares = floats * floats
    sq_high, sq_low = high_low(squares)
    ones = jnp.ones((8, 64), bf16)
    square_sum = dot_t(ones, sq_high.astype(bf16)) + dot_t(ones, sq_low.astype(bf16))
    lane = iota((2, WIDTH), 1)
    position = iota((2, LEN), 1)
    last = jnp.zeros((2, WIDTH), f32)
    for b in range(SEQS):
        at = prior[b] + accepted[b] - 1 - kv * LEN
        found = jnp.sum(jnp.where(position == at, cum[b], 0.0), axis=1, keepdims=True)
        last = jnp.where(lane == b, found, last)
    last_high, last_low = high_low(last)
    rest = last - last_high - last_low
    copy.wait()
    gates[...] = lax.dot_general(
        gate_rows[...], scaled, (((0,), (1,)), ((), ())), preferred_element_type=f32
    )
    row = iota((8, ROWS), 0)
    gate_0 = gates[pl.ds(2 * tp, 1), :]
    gate_1 = gates[pl.ds(2 * tp + 1, 1), :]
    stats = jnp.where(row == 0, gate_0, jnp.where(row == 1, gate_1, 0.0))
    stats = jnp.where(row == 2, square_sum, stats)
    wide = jnp.zeros((2, ROWS - WIDTH), f32)
    last = jnp.concatenate([last, wide], axis=1)
    rest = jnp.concatenate([rest, wide], axis=1)
    stats = jnp.where(row == 3, last[0:1], jnp.where(row == 4, last[1:2], stats))
    stats = jnp.where(row == 5, rest[0:1], jnp.where(row == 6, rest[1:2], stats))
    out[STATS] = jnp.concatenate(high_low(stats), axis=0).astype(bf16)
    out[STATS + 1 :] = jnp.zeros((N_KV - STATS - 1, PROPS, ROWS), bf16)


def share_kernel(ids, bias, parts, out):
    kv, tp = ids[0], ids[1]
    total = jnp.zeros((PROPS, ROWS), f32)
    for k in range(N_KV):
        total = total + parts[k].astype(f32)
    stats = total[0:8] + total[8:16]
    row = iota((8, ROWS), 0)
    inv_rms = lax.rsqrt(stats[2:3] / D + norm_eps)
    logits = inv_rms * stats + jnp.where(row == 0, bias[2 * tp], bias[2 * tp + 1])
    log_gates = jnp.minimum(logits, 0.0) - jnp.log1p(jnp.exp(-jnp.abs(logits)))
    stats = jnp.where(row < 2, log_gates, jnp.where(row == 2, inv_rms, stats))
    stats = jnp.concatenate(high_low(stats), axis=0)
    block = jnp.where(kv == STATS, stats, total).astype(bf16)
    for k in range(N_KV):
        out[k] = block


def attention_kernel(
    ids,
    prior,
    accepted,
    parents,
    joined,
    cum,
    keys,
    values,
    out,
    k_buf,
    v_buf,
    columns,
    k_sem,
    v_sem,
):
    kv = ids[0]
    k_copies = []
    v_copies = []
    for t in range(N_TP):
        three = pl.ds(3 * t, 3)
        k_copies.append(pltpu.make_async_copy(keys.at[three], k_buf.at[three], k_sem.at[t]))
        v_copies.append(pltpu.make_async_copy(values.at[three], v_buf.at[three], v_sem.at[t]))
        k_copies[t].start()
        v_copies[t].start()
    coded = joined[STATS].astype(f32)
    columns[...] = jnp.transpose(coded[0:8] + coded[8:16])
    lane = iota((PROPS, WIDTH), 1)
    first_head = lane < HEAD
    lane_out = iota((2 * PROPS, WIDTH), 1)
    row_out = iota((2 * PROPS, WIDTH), 0)
    own_lanes = (lane_out < HEAD) == (row_out < PROPS)
    stat_lane = jnp.where(row_out < PROPS, lane_out - HEAD, lane_out)
    position = iota((2, LEN), 1)
    scale = HEAD**-0.5

    def both_heads(b_rows, b_block):
        inv = columns[b_rows, 2:3]
        q = (inv * joined[b_block, :, 0:WIDTH].astype(f32)).astype(bf16).astype(f32) * scale
        zero = jnp.zeros_like(q)
        return jnp.concatenate(
            [jnp.where(first_head, q, zero), jnp.where(first_head, zero, q)], axis=0
        ).astype(bf16)

    def packed(v, top, total):
        top_high, top_low = high_low(top)
        sum_high, sum_low = high_low(total)
        stats = jnp.where(
            stat_lane == 0,
            top_high,
            jnp.where(stat_lane == 1, top_low, jnp.where(stat_lane == 2, sum_high, sum_low)),
        )
        return jnp.where(own_lanes, v, stats).astype(bf16)

    def sendable(top):
        high, low = high_low(jnp.maximum(top, lowest_max))
        return high + low

    for t in range(N_TP):
        k_copies[t].wait()
        v_copies[t].wait()
        for s in range(3):
            b = 3 * t + s
            q = both_heads(pl.ds(PROPS * b, PROPS), b)
            filled_here = prior[b] + accepted[b] - kv * LEN
            bias = jnp.where(position < filled_here, -cum[b], masked_score)
            bias = jnp.concatenate(
                [
                    jnp.broadcast_to(bias[0:1], (PROPS, LEN)),
                    jnp.broadcast_to(bias[1:2], (PROPS, LEN)),
                ],
                axis=0,
            )
            scores = dot_t(q, k_buf[b]) + bias
            top = sendable(jnp.max(scores, axis=1, keepdims=True))
            weights = jnp.exp(scores - top)
            total = jnp.sum(weights, axis=1, keepdims=True)
            v = jnp.dot(weights.astype(bf16), v_buf[b], preferred_element_type=f32)
            out[t, 32 * s : 32 * s + 32, :] = packed(v, top, total)
        out[t, 96:128, :] = jnp.zeros((32, WIDTH), bf16)

    @pl.when(kv < SEQS)
    def _():
        square = iota((PROPS, WIDTH), 0)
        link = jnp.where(lane == square, 1.0, 0.0)
        for i in range(PROPS):
            link = jnp.where((square == i) & (lane == parents[kv, i]), 1.0, link)
        reached = link
        pad = jnp.zeros((WIDTH - PROPS, WIDTH), f32)
        for _ in range(PROPS.bit_length()):
            other = jnp.concatenate([reached, pad], axis=0).astype(bf16)
            reached = jnp.minimum(
                jnp.dot(reached.astype(bf16), other, preferred_element_type=f32), 1.0
            )
        mine = pl.ds(pl.multiple_of(PROPS * kv, PROPS), PROPS)
        picks = (iota((ROWS, WIDTH), 0) == iota((ROWS, WIDTH), 1) + PROPS * kv) & (
            iota((ROWS, WIDTH), 1) < PROPS
        )
        own_gates = jnp.dot(
            joined[STATS], jnp.where(picks, 1.0, 0.0).astype(bf16), preferred_element_type=f32
        ).astype(bf16)
        tree = dot_t(own_gates, jnp.concatenate([reached, pad], axis=0).astype(bf16))
        tree = tree[0:8] + tree[8:16]
        whole = (coded[0:8] + coded[8:16])[:, 0:WIDTH]
        last = jnp.sum(
            jnp.where(iota((8, WIDTH), 1) == kv, whole, 0.0), axis=1, keepdims=True
        )
        bias = jnp.concatenate(
            [
                jnp.broadcast_to(-(last[3:4] + last[5:6] + tree[0:1]), (PROPS, WIDTH)),
                jnp.broadcast_to(-(last[4:5] + last[6:7] + tree[1:2]), (PROPS, WIDTH)),
            ],
            axis=0,
        )
        q = both_heads(mine, kv)
        inv = columns[mine, 2:3]
        new_keys = inv * joined[kv, :, WIDTH : 2 * WIDTH].astype(f32)
        new_values = inv * joined[kv, :, 2 * WIDTH : 3 * WIDTH].astype(f32)
        new_keys = jnp.concatenate([new_keys, pad], axis=0).astype(bf16)
        new_values = jnp.concatenate([new_values, pad], axis=0).astype(bf16)
        live = jnp.concatenate([reached, reached], axis=0) > 0.5
        scores = jnp.where(live, dot_t(q, new_keys) + bias, masked_score)
        tree_top = jnp.max(scores, axis=1, keepdims=True)
        at = pl.ds(pl.multiple_of(32 * lax.rem(kv, 3), 32), 32)
        held = out[lax.div(kv, 3), at, :].astype(f32)

        def stat(n):
            pick = (stat_lane == n) & jnp.logical_not(own_lanes)
            return jnp.sum(jnp.where(pick, held, 0.0), axis=1, keepdims=True)

        old_top = stat(0) + stat(1)
        old_sum = stat(2) + stat(3)
        top = sendable(jnp.maximum(old_top, tree_top))
        weights = jnp.exp(scores - top)
        keep = jnp.exp(old_top - top)
        total = keep * old_sum + jnp.sum(weights, axis=1, keepdims=True)
        v = keep * held + jnp.dot(
            weights.astype(bf16), new_values, preferred_element_type=f32
        )
        out[lax.div(kv, 3), at, :] = packed(v, top, total)


def combine_kernel(ids, parts, out):
    kv = ids[0]
    head = lax.rem(lax.div(kv, 4), 2)
    start = HEAD * (1 - head)
    row = iota((WIDTH, 2 * WIDTH), 0) - start
    row = row - jnp.where(iota((WIDTH, 2 * WIDTH), 1) < WIDTH, 0, 2)
    spread = jnp.where((row == 0) | (row == 1), 1.0, 0.0).astype(bf16)
    results = []
    for g in range(N_TP):
        block = parts[128 * g : 128 * g + 128]
        stats = jnp.dot(block, spread, preferred_element_type=f32)
        tops = stats[:, 0:WIDTH].reshape(16, 8, WIDTH)
        sums = stats[:, WIDTH:].reshape(16, 8, WIDTH)
        floats = block.astype(f32).reshape(16, 8, WIDTH)
        top = jnp.max(tops, axis=0)
        top = jnp.maximum(top, pltpu.roll(top, 4, 0))
        factor = jnp.exp(tops - top[None])
        above = jnp.sum(factor * floats, axis=0)
        below = jnp.sum(factor * sums, axis=0)
        above = above + pltpu.roll(above, 4, 0)
        below = below + pltpu.roll(below, 4, 0)
        results.append(above / below)
    lane = iota((8, WIDTH), 1)
    first = iota((8, WIDTH), 0) < 4
    pairs = []
    for p in range(4):
        even, odd = results[2 * p], results[2 * p + 1]
        even = jnp.where(head == 0, even, pltpu.roll(even, HEAD, 1))
        odd = jnp.where(head == 1, odd, pltpu.roll(odd, HEAD, 1))
        pairs.append(jnp.where(lane < HEAD, even, odd))
    block = jnp.concatenate(
        [jnp.where(first, pairs[0], pairs[1]), jnp.where(first, pairs[2], pairs[3])], axis=0
    ).astype(bf16)
    for k in range(N_KV):
        out[k] = block


def output_kernel(shared, w_out, out, rows):
    for s in range(3):
        for h in range(2):
            for i in range(4):
                block = shared[8 * s + 4 * h + i].astype(f32)
                for p in range(4):
                    rows[16 * s + 4 * i : 16 * s + 4 * i + 4, pl.ds((2 * p + h) * WIDTH, WIDTH)] = (
                        block[4 * p : 4 * p + 4]
                    )
    total = jnp.zeros((48, 64), f32)
    for p in range(4):
        for h in range(2):
            weight = jnp.concatenate(
                [
                    w_out[2 * p, HEAD * h : HEAD * h + HEAD, :],
                    w_out[2 * p + 1, HEAD * h : HEAD * h + HEAD, :],
                ],
                axis=0,
            )
            block = rows[:, (2 * p + h) * WIDTH : (2 * p + h + 1) * WIDTH].astype(bf16)
            total = total + jnp.dot(block, weight, preferred_element_type=f32)
    out[...] = total.astype(bf16)


def copy_kernel(after, keys, values, keys_out, values_out, sems):
    copies = []
    for n, (source, target) in enumerate(((keys, keys_out), (values, values_out))):
        for t in range(8):
            three = pl.ds(3 * t, 3)
            copies.append(
                pltpu.make_async_copy(source.at[three], target.at[three], sems.at[8 * n + t])
            )
    for copy in copies:
        copy.start()
    for copy in copies:
        copy.wait()


def write_kernel(
    ids, prior, accepted, joined, after, keys_in, values_in, keys, values, buf, columns, in_sem, out_sem
):
    offset = ids[0] * LEN
    coded = joined[STATS].astype(f32)
    columns[...] = jnp.transpose(coded[0:8] + coded[8:16])

    def place(b):
        start = prior[b] + accepted[b] - offset
        base = jnp.clip(lax.div(jnp.maximum(start, 0), 16) * 16, 0, LEN - WINDOW)
        hit = (start > -PROPS) & (start < LEN)
        return start, pl.multiple_of(base, 16), hit

    def copy_in(n, b, base):
        source = (keys, values)[n].at[b, pl.ds(base, WINDOW), :]
        return pltpu.make_async_copy(source, buf.at[n, b], in_sem.at[n, b])

    def copy_out(n, b, base):
        target = (keys, values)[n].at[b, pl.ds(base, WINDOW), :]
        return pltpu.make_async_copy(buf.at[n, b], target, out_sem.at[n, b])

    @pl.loop(0, SEQS)
    def _(b):
        start, base, hit = place(b)

        @pl.when(hit)
        def _():
            for n in range(2):
                copy_in(n, b, base).start()

    @pl.loop(0, SEQS)
    def _(b):
        start, base, hit = place(b)

        @pl.when(hit)
        def _():
            inv = columns[pl.ds(pl.multiple_of(PROPS * b, PROPS), PROPS), 2:3]
            slot = iota((WINDOW, PROPS), 0) + (base - start)
            selector = jnp.where(slot == iota((WINDOW, PROPS), 1), 1.0, 0.0).astype(bf16)
            slot = iota((WINDOW, WIDTH), 0) + (base - start)
            inside = (slot >= 0) & (slot < PROPS)
            for n in range(2):
                raw = joined[b, :, (n + 1) * WIDTH : (n + 2) * WIDTH].astype(f32)
                rows = jnp.dot(selector, (inv * raw).astype(bf16), preferred_element_type=f32)
                copy_in(n, b, base).wait()
                held = buf[n, b].astype(f32)
                buf[n, b] = jnp.where(inside, rows, held).astype(bf16)
                copy_out(n, b, base).start()

    @pl.loop(0, SEQS)
    def _(b):
        start, base, hit = place(b)

        @pl.when(hit)
        def _():
            for n in range(2):
                copy_out(n, b, base).wait()


def shards(
    tokens,
    norm_gain,
    w_query,
    w_key,
    w_value,
    w_gate,
    gate_bias,
    w_out,
    keys_cache,
    values_cache,
    cum_gates,
    prior_len,
    accepted,
    parents,
):
    ids = jnp.stack([lax.axis_index(KV), lax.axis_index("tp")]).astype(jnp.int32)
    cache = jax.ShapeDtypeStruct(keys_cache.shape, bf16)

    parts = pl.pallas_call(
        project_kernel,
        out_shape=jax.ShapeDtypeStruct((N_KV, PROPS, ROWS), bf16),
        in_specs=[SM, SM, SM, VM, VM, VM, VM, VM, ANY, VM],
        out_specs=VM,
        scratch_shapes=[
            pltpu.VMEM((64, 16), bf16),
            pltpu.VMEM((16, ROWS), f32),
            pltpu.SemaphoreType.DMA,
        ],
        name="project",
    )(
        ids,
        prior_len,
        accepted,
        tokens,
        norm_gain[None],
        w_query,
        w_key,
        w_value,
        w_gate,
        cum_gates,
    )
    arrived = lax.all_to_all(parts, KV, 0, 0, tiled=True)

    keys_copy, values_copy = pl.pallas_call(
        copy_kernel,
        out_shape=(cache, cache),
        in_specs=[ANY, ANY, ANY],
        out_specs=(ANY, ANY),
        scratch_shapes=[pltpu.SemaphoreType.DMA((16,))],
        cost_estimate=pl.CostEstimate(
            flops=8_000_000_000, bytes_accessed=12_600_000, transcendentals=0
        ),
        name="copy",
    )(parts, keys_cache, values_cache)

    block = pl.pallas_call(
        share_kernel,
        out_shape=jax.ShapeDtypeStruct((N_KV, PROPS, ROWS), bf16),
        in_specs=[SM, SM, VM],
        out_specs=VM,
        name="share",
    )(ids, gate_bias, arrived)
    joined = lax.all_to_all(block, KV, 0, 0, tiled=True)

    w_all = lax.all_to_all(
        jnp.broadcast_to(w_out[None], (N_TP, *w_out.shape)), "tp", 0, 0, tiled=True
    )

    sent = pl.pallas_call(
        attention_kernel,
        out_shape=jax.ShapeDtypeStruct((N_TP, 128, WIDTH), bf16),
        in_specs=[SM, SM, SM, SM, VM, VM, ANY, ANY],
        out_specs=VM,
        scratch_shapes=[
            pltpu.VMEM((SEQS, LEN, WIDTH), bf16),
            pltpu.VMEM((SEQS, LEN, WIDTH), bf16),
            pltpu.VMEM((ROWS, 8), f32),
            pltpu.SemaphoreType.DMA((8,)),
            pltpu.SemaphoreType.DMA((8,)),
        ],
        name="attention",
    )(ids, prior_len, accepted, parents, joined, cum_gates, keys_cache, values_cache)
    pieces = lax.all_to_all(sent.reshape(256, 4, WIDTH), ("tp", *KV), 0, 0, tiled=True)

    keys_out, values_out = pl.pallas_call(
        write_kernel,
        out_shape=(cache, cache),
        in_specs=[SM, SM, SM, VM, ANY, ANY, ANY],
        out_specs=(ANY, ANY),
        input_output_aliases={5: 0, 6: 1},
        scratch_shapes=[
            pltpu.VMEM((2, SEQS, WINDOW, WIDTH), bf16),
            pltpu.VMEM((ROWS, 8), f32),
            pltpu.SemaphoreType.DMA((2, SEQS)),
            pltpu.SemaphoreType.DMA((2, SEQS)),
        ],
        cost_estimate=pl.CostEstimate(
            flops=8_000_000_000, bytes_accessed=100_000, transcendentals=0
        ),
        name="write",
    )(ids, prior_len, accepted, joined, sent, keys_copy, values_copy)

    combined = pl.pallas_call(
        combine_kernel,
        out_shape=jax.ShapeDtypeStruct((N_KV, PROPS, WIDTH), bf16),
        in_specs=[SM, VM],
        out_specs=VM,
        name="combine",
    )(ids, pieces.reshape(1024, WIDTH))
    shared = lax.all_to_all(combined, KV, 0, 0, tiled=True)

    mixed_rows = pl.pallas_call(
        output_kernel,
        out_shape=jax.ShapeDtypeStruct((48, 64), bf16),
        in_specs=[VM, VM],
        out_specs=VM,
        scratch_shapes=[pltpu.VMEM((48, 1024), f32)],
        name="output",
    )(shared, w_all)
    return (mixed_rows, keys_out, values_out)


def solution(mesh):
    torus = Mesh(mesh.devices.reshape(8, 4, mesh.shape["tp"]), ("kv_0", "kv_1", "tp"))
    in_specs = (
        P(None, KV),
        P(KV),
        P(KV, "tp"),
        P(KV, "tp"),
        P(KV, "tp"),
        P(),
        P(),
        P("tp", KV),
        P(None, KV, "tp"),
        P(None, KV, "tp"),
        P(None, "tp", KV),
        P(),
        P(),
        P(),
    )
    out_specs = (P("tp", KV), P(None, KV, "tp"), P(None, KV, "tp"))
    return jax.shard_map(
        shards, mesh=torus, in_specs=in_specs, out_specs=out_specs, check_vma=False
    )
```

time: 174 us -> 300 us (1.72)
  Pallas kernels: 0 us -> 215 us
  waiting for transfers between devices: 51.5 us -> 7.73 us
  blocking collectives: 15.3 us -> 45.7 us
  matrix products: 25.9 us -> 0 us
  local copies, waits for them, and re-layouts: 29.2 us -> 6.92 us
  between operations: 14.6 us -> 0.72 us
  other arithmetic: 9.74 us -> 0.65 us
    pallas_call x0 -> x7, Pallas kernels: none -> 215 us  [the longest x1 192 us: shards(): pl.pallas_call(copy_kernel, out_shape=(cache, cache), in_specs=[ANY, ANY,...]
    all_to_all x0 -> x2, blocking collectives: none -> 45.7 us  [the longest x1 26.7 us: shards(): arrived = lax.all_to_all(parts, KV, 0, 0, tiled=True)]
    all_gather x1 -> x0, waiting for transfers between devices: 28.4 us -> none  [collected_together(): both, at, found = (lax.all_gather(jnp.concatenate(lines), axis), 0, {})]
    dot_general x15 -> x0, matrix products: 25.9 us -> none  [the longest x1 7.86 us: shards(): jnp.einsum('bpj,bjc->bpc', selector, new_values.reshape(seq_count, PROPS,...]
    all_to_all x4 -> x3, waiting for transfers between devices: 23.1 us -> 7.73 us  [the longest x1 7.73 us: shards(): shared = lax.all_to_all(combined, KV, 0, 0, tiled=True)]
    all_gather x1 -> x0, blocking collectives: 15.3 us -> none  [collected_together(): both, at, found = (lax.all_gather(jnp.concatenate(lines), axis), 0, {})]
    unnamed x55 -> x11, local copies, waits for them, and re-layouts: 14.2 us -> 5.41 us
    squeeze x16 -> x0, local copies, waits for them, and re-layouts: 5.55 us -> none  [the longest x13 4.08 us: combined_by_axis(): shard = combine(shard, jax.tree.map(lambda part: part[k], pieces))]
  transfers between devices with their start and end apart: 5 -> 3, of which waited for: 4 -> 1; matrix products, arithmetic and copies ran while one was open for 18% -> 1% of each run, Pallas kernels for 0% -> 69%
where the time goes in v1:
time: 300 us; the launch traced here: 299 us
  Pallas kernels  215 us (72%)
  blocking collectives  45.7 us (15%)
  starting transfers between devices  22.9 us (8%)
  waiting for transfers between devices  7.73 us (3%)
  local copies, waits for them, and re-layouts  6.92 us (2%)
    pallas_call x1, Pallas kernels, shards(): pl.pallas_call(copy_kernel, out_shape=(cache, cache), in_specs=[ANY, ANY,...  192 us
    all_to_all x1, blocking collectives, shards(): arrived = lax.all_to_all(parts, KV, 0, 0, tiled=True)  26.7 us
    all_to_all x1, blocking collectives, shards(): joined = lax.all_to_all(block, KV, 0, 0, tiled=True)  18.9 us
    pallas_call x1, Pallas kernels, shards(): pl.pallas_call(attention_kernel, out_shape=jax.ShapeDtypeStruct((N_TP, 12...  11.4 us
    all_to_all x1, starting transfers between devices, shards(): shared = lax.all_to_all(combined, KV, 0, 0, tiled=True)  10.5 us
    all_to_all x1, waiting for transfers between devices, shards(): shared = lax.all_to_all(combined, KV, 0, 0, tiled=True)  7.73 us
    all_to_all x1, starting transfers between devices, shards(): lax.all_to_all(sent.reshape(256, 4, WIDTH), ('tp', *KV), 0, 0, tiled=True)  7.5 us
  transfers between devices with their start and end apart: 3, of which 1 were waited for; matrix products, arithmetic and copies ran while one was open for 1% of the time, Pallas kernels for 69%

profile of v1, /device:TPU:8, one launch (start us, length us, event | category | flops | bytes accessed | tf_op | source)
XLA Modules:
  0.0 299.4 jit_solution(13913377525609755983)
XLA Ops:
  0.6 0.0 copy-start.2
  0.6 0.0 copy-start.3
  0.7 1.8 copy.25.w_gate
  2.5 1.5 copy.24.tokens
  4.0 0.6 pad_add_fusion.ids
  4.7 2.8 project.1.after
  7.5 26.7 %all_to_all.25.parts = bf16[32,16,384]{2,1,0:T(8,128)(2,1)} all-to-all(bf16[32,16,384]{2,1,0:T(8,128)(2,1)} %project.1.after), channel_id=1, replica_groups=mesh['kv_0'=8,'kv_1'=4,'tp'=8] {'kv_0','kv_1'}, dimensions={0} | all-to-all | bytes 786432 | tf_op jit(solution)/shard_map/all_to_all | solution.py:425
  34.3 1.9 share.1
  36.1 18.9 %all_to_all.26.joined = bf16[32,16,384]{2,1,0:T(8,128)(2,1)} all-to-all(bf16[32,16,384]{2,1,0:T(8,128)(2,1)} %share.1), channel_id=1, replica_groups=mesh['kv_0'=8,'kv_1'=4,'tp'=8] {'kv_0','kv_1'}, dimensions={0} | all-to-all | bytes 786432 | tf_op jit(solution)/shard_map/all_to_all | solution.py:446
  55.1 0.0 copy-done.2
  55.1 0.7 broadcast_in_dim.10
  55.7 4.9 %all-to-all-start.4 = ((bf16[8,128,64]{1,2,0:T(8,128)(2,1)}), bf16[8,128,64]{1,2,0:T(8,128)(2,1)S(1)}, u32[]{:S(2)}, u32[]{:S(2)}) async-start(bf16[8,128,64]{1,2,0:T(8,128)(2,1)} %broadcast_in_dim.10), calls=%async_computation.4 | async-start | bytes 262144 | tf_op jit(solution)/shard_map/all_to_all | solution.py:448
  60.7 0.0 copy-done.3
  60.7 0.7 copy.26.parents
  61.3 11.4 %attention.1.after = bf16[8,128,128]{2,1,0:T(8,128)(2,1)} custom-call(s32[2]{0:T(128)} %pad_add_fusion.ids, s32[24]{0:T(128)} %prior.5, s32[24]{0:T(128)} %accepted.5, s32[24,16]{1,0:T(8,128)} %copy.26.parents, bf16[32,16,384]{2,1,0:T(8,128)(2,1)} %all_to_all.26.joined, f32[24,2,512]{2,1,0:T(2,128)} %cum.3, bf16[24,512,128]{2,1,0:T(8,128)(2,1)} %keys.3, ...), custom_call_target="tpu_custom_call" | custom-call | tf_op jit(solution)/shard_map/attention/pallas_call | solution.py:452
  72.7 0.0 all-to-all-done.4
  72.7 7.5 %all-to-all-start.2 = ((bf16[256,4,128]{2,1,0:T(4,128)(2,1)}), bf16[256,4,128]{2,1,0:T(4,128)(2,1)S(1)}, u32[]{:S(2)}, u32[]{:S(2)}) async-start(bf16[256,4,128]{2,1,0:T(4,128)(2,1)} %bitcast.5), calls=%async_computation.2 | async-start | bytes 524288 | tf_op jit(solution)/shard_map/all_to_all | solution.py:466
  80.2 191.8 %copy.30 = (bf16[24,512,128]{2,1,0:T(8,128)(2,1)}, bf16[24,512,128]{2,1,0:T(8,128)(2,1)}) custom-call(bf16[32,16,384]{2,1,0:T(8,128)(2,1)} %project.1.after, bf16[24,512,128]{2,1,0:T(8,128)(2,1)} %keys.3, bf16[24,512,128]{2,1,0:T(8,128)(2,1)} %values.3), custom_call_target="tpu_custom_call" | custom-call | flops 8000000000 | bytes 12600000 | tf_op jit(solution)/shard_map/copy/pallas_call | solution.py:427
  272.1 0.8 copy.27.w_out
  272.9 0.0 all-to-all-done.2
  272.9 0.0 copy-start
  272.9 0.7 copy-done
  273.6 2.1 combine.1
  275.7 10.5 %all-to-all-start.3 = ((bf16[32,16,128]{2,1,0:T(8,128)(2,1)}), bf16[32,16,128]{2,1,0:T(8,128)(2,1)S(1)}, u32[]{:S(2)}, u32[]{:S(2)}) async-start(bf16[32,16,128]{2,1,0:T(8,128)(2,1)} %combine.1), calls=%async_computation.3 | async-start | bytes 262144 | tf_op jit(solution)/shard_map/all_to_all | solution.py:493
  286.2 3.0 %write.1 = (bf16[24,512,128]{2,1,0:T(8,128)(2,1)}, bf16[24,512,128]{2,1,0:T(8,128)(2,1)}) custom-call(s32[2]{0:T(128)} %pad_add_fusion.ids, s32[24]{0:T(128)} %prior.5, s32[24]{0:T(128)} %accepted.5, bf16[32,16,384]{2,1,0:T(8,128)(2,1)} %all_to_all.26.joined, bf16[8,128,128]{2,1,0:T(8,128)(2,1)} %attention.1.after, ...), custom_call_target="tpu_custom_call", output_to_operand_aliasing={{0}: (5, {}), {1}: (6, {})} | custom-call | flops 8000000000 | bytes 100000 | tf_op jit(solution)/shard_map/write/pallas_call | solution.py:468
  289.2 7.7 %all-to-all-done.3.shared = bf16[32,16,128]{2,1,0:T(8,128)(2,1)S(1)} async-done(((bf16[32,16,128]{2,1,0:T(8,128)(2,1)}), bf16[32,16,128]{2,1,0:T(8,128)(2,1)S(1)}, u32[]{:S(2)}, u32[]{:S(2)}) %all-to-all-start.3) | async-done | bytes 131104 | tf_op jit(solution)/shard_map/all_to_all | solution.py:493
  296.9 0.0 copy-start.1
  296.9 0.6 copy-done.1
  297.6 1.8 output.1
Async XLA Ops:
  0.6 54.4 %copy-start.2 = (bf16[128,64]{0,1:T(8,128)(2,1)S(1)}, bf16[128,64]{0,1:T(8,128)(2,1)}, u32[]{:S(2)}) copy-start(bf16[128,64]{0,1:T(8,128)(2,1)} %param.21) | copy-start | bytes 49156
  0.6 60.0 %copy-start.3 = (s32[24,16]{0,1:T(8,128)S(1)}, s32[24,16]{0,1:T(8,128)}, u32[]{:S(2)}) copy-start(s32[24,16]{0,1:T(8,128)} %param.27) | copy-start | bytes 4612
  55.7 17.0 %all-to-all-start.4 = ((bf16[8,128,64]{1,2,0:T(8,128)(2,1)}), bf16[8,128,64]{1,2,0:T(8,128)(2,1)S(1)}, u32[]{:S(2)}, u32[]{:S(2)}) async-start(bf16[8,128,64]{1,2,0:T(8,128)(2,1)} %broadcast_in_dim.10), calls=%async_computation.4 | async-start | bytes 262144 | tf_op jit(solution)/shard_map/all_to_all | solution.py:448
  72.7 200.2 %all-to-all-start.2 = ((bf16[256,4,128]{2,1,0:T(4,128)(2,1)}), bf16[256,4,128]{2,1,0:T(4,128)(2,1)S(1)}, u32[]{:S(2)}, u32[]{:S(2)}) async-start(bf16[256,4,128]{2,1,0:T(4,128)(2,1)} %bitcast.5), calls=%async_computation.2 | async-start | bytes 524288 | tf_op jit(solution)/shard_map/all_to_all | solution.py:466
  272.9 0.7 copy-start
  275.7 21.2 %all-to-all-start.3 = ((bf16[32,16,128]{2,1,0:T(8,128)(2,1)}), bf16[32,16,128]{2,1,0:T(8,128)(2,1)S(1)}, u32[]{:S(2)}, u32[]{:S(2)}) async-start(bf16[32,16,128]{2,1,0:T(8,128)(2,1)} %combine.1), calls=%async_computation.3 | async-start | bytes 262144 | tf_op jit(solution)/shard_map/all_to_all | solution.py:493
  296.9 0.6 copy-start.1

commit v2 on v1

v2 whole, which is shorter than its diff:
```python
import jax
import jax.numpy as jnp
from jax import lax
from jax.experimental import pallas as pl
from jax.experimental.pallas import tpu as pltpu
from jax.sharding import Mesh
from jax.sharding import PartitionSpec as P

D = 2048
HEAD = 64
PROPS = 16
ROWS = 384
SEQS = 24
LEN = 512
WIDTH = 128
N_KV = 32
N_TP = 8
STATS = 24
WINDOW = 32
KV = ("kv_0", "kv_1")

masked_score = -1e30
lowest_max = -1e20
norm_eps = 1e-06

VM = pl.BlockSpec(memory_space=pltpu.VMEM)
SM = pl.BlockSpec(memory_space=pltpu.SMEM)
ANY = pl.BlockSpec(memory_space=pl.ANY)
bf16 = jnp.bfloat16
f32 = jnp.float32


def iota(shape, dim):
    return lax.broadcasted_iota(jnp.int32, shape, dim)


def high_low(x):
    high = x.astype(bf16).astype(f32)
    return high, (x - high).astype(bf16).astype(f32)


def dot_t(a, b):
    return lax.dot_general(a, b, (((1,), (1,)), ((), ())), preferred_element_type=f32)


def project_kernel(
    prior, accepted, tokens, gain, w_q, w_k, w_v, w_gate, cum, out, bias, gate_rows, gates, sem
):
    kv, tp = lax.axis_index(KV), lax.axis_index("tp")
    columns = pl.ds(pl.multiple_of(lax.div(kv, 2) * WIDTH, WIDTH), WIDTH)
    copy = pltpu.make_async_copy(w_gate.at[:, columns], gate_rows, sem)
    copy.start()
    floats = tokens[...].astype(f32)
    same = iota((64, 64), 0) == iota((64, 64), 1)
    gain_column = jnp.sum(jnp.where(same, gain[...], 0.0), axis=1, keepdims=True)
    scaled = floats * gain_column
    rows = jnp.transpose(scaled).astype(bf16)
    scaled = scaled.astype(bf16)
    for n, w in enumerate((w_q, w_k, w_v)):
        part = jnp.dot(rows, w[...], preferred_element_type=f32).astype(bf16)
        out[0:SEQS, :, n * WIDTH : (n + 1) * WIDTH] = part.reshape(SEQS, PROPS, WIDTH)
    sq_high, sq_low = high_low(floats * floats)
    ones = jnp.ones((8, 64), bf16)
    square_sum = jnp.dot(ones, sq_high.astype(bf16), preferred_element_type=f32) + jnp.dot(
        ones, sq_low.astype(bf16), preferred_element_type=f32
    )
    lane = iota((2, WIDTH), 1)
    position = iota((2, LEN), 1)
    last = jnp.zeros((2, WIDTH), f32)
    for b in range(SEQS):
        at = prior[b] + accepted[b] - 1 - kv * LEN
        here = cum[b]
        bias[b] = jnp.where(position <= at, -here, masked_score)
        found = jnp.sum(jnp.where(position == at, here, 0.0), axis=1, keepdims=True)
        last = jnp.where(lane == b, found, last)
    last_high, last_low = high_low(last)
    rest = last - last_high - last_low
    odd = lax.rem(kv, 2)
    zero = jnp.zeros_like(scaled)
    both = jnp.concatenate(
        [jnp.where(odd == 0, scaled, zero), jnp.where(odd == 1, scaled, zero)], axis=0
    )
    copy.wait()
    gates[...] = jnp.dot(gate_rows[...], both, preferred_element_type=f32)
    row = iota((8, ROWS), 0)
    gate_0 = gates[pl.ds(2 * tp, 1), :]
    gate_1 = gates[pl.ds(2 * tp + 1, 1), :]
    stats = jnp.where(row == 0, gate_0, jnp.where(row == 1, gate_1, 0.0))
    stats = jnp.where(row == 2, square_sum, stats)
    wide = jnp.zeros((2, ROWS - WIDTH), f32)
    last = jnp.concatenate([last, wide], axis=1)
    rest = jnp.concatenate([rest, wide], axis=1)
    stats = jnp.where(row == 3, last[0:1], jnp.where(row == 4, last[1:2], stats))
    stats = jnp.where(row == 5, rest[0:1], jnp.where(row == 6, rest[1:2], stats))
    out[STATS] = jnp.concatenate(high_low(stats), axis=0).astype(bf16)
    out[STATS + 1 :] = jnp.zeros((N_KV - STATS - 1, PROPS, ROWS), bf16)


def share_kernel(bias, parts, after, after_w, out):
    kv, tp = lax.axis_index(KV), lax.axis_index("tp")
    total = jnp.zeros((PROPS, ROWS), f32)
    for k in range(N_KV):
        total = total + parts[k].astype(f32)
    stats = total[0:8] + total[8:16]
    row = iota((8, ROWS), 0)
    inv_rms = lax.rsqrt(stats[2:3] / D + norm_eps)
    logits = inv_rms * stats + jnp.where(row == 0, bias[2 * tp], bias[2 * tp + 1])
    log_gates = jnp.minimum(logits, 0.0) - jnp.log1p(jnp.exp(-jnp.abs(logits)))
    stats = jnp.where(row < 2, log_gates, jnp.where(row == 2, inv_rms, stats))
    stats = jnp.concatenate(high_low(stats), axis=0)
    block = jnp.where(kv == STATS, stats, total).astype(bf16)
    for k in range(N_KV):
        out[k] = block


def attention_kernel(
    ancestors,
    joined,
    biases,
    keys_far,
    values_far,
    out,
    columns,
    scores_buf,
    weights_buf,
    keys,
    values,
    sems,
):
    kv = lax.axis_index(KV)
    moves = []
    for n, (source, target) in enumerate(((keys_far, keys), (values_far, values))):
        for t in range(N_TP):
            three = pl.ds(3 * t, 3)
            moves.append(
                pltpu.make_async_copy(source.at[three], target.at[three], sems.at[n, t])
            )
    for move in moves:
        move.start()
    coded = joined[STATS].astype(f32)
    stats = coded[0:8] + coded[8:16]
    columns[...] = jnp.transpose(stats)
    lane = iota((PROPS, WIDTH), 1)
    first_head = lane < HEAD
    lane_out = iota((2 * PROPS, WIDTH), 1)
    row_out = iota((2 * PROPS, WIDTH), 0)
    own_lanes = (lane_out < HEAD) == (row_out < PROPS)
    stat_lane = jnp.where(row_out < PROPS, lane_out - HEAD, lane_out)
    scale = HEAD**-0.5

    def both_heads(b_rows, b_block):
        inv = columns[b_rows, 2:3]
        q = (inv * joined[b_block, :, 0:WIDTH].astype(f32)).astype(bf16).astype(f32) * scale
        zero = jnp.zeros_like(q)
        return jnp.concatenate(
            [jnp.where(first_head, q, zero), jnp.where(first_head, zero, q)], axis=0
        ).astype(bf16)

    def packed(v, top, total):
        top_high, top_low = high_low(top)
        sum_high, sum_low = high_low(total)
        stats = jnp.where(
            stat_lane == 0,
            top_high,
            jnp.where(stat_lane == 1, top_low, jnp.where(stat_lane == 2, sum_high, sum_low)),
        )
        return jnp.where(own_lanes, v, stats).astype(bf16)

    def sendable(top):
        high, low = high_low(jnp.maximum(top, lowest_max))
        return high + low

    own = jnp.minimum(kv, SEQS - 1)
    mine = pl.ds(pl.multiple_of(PROPS * own, PROPS), PROPS)
    pad = jnp.zeros((WIDTH - PROPS, WIDTH), f32)
    picks = (iota((ROWS, WIDTH), 0) == iota((ROWS, WIDTH), 1) + PROPS * own) & (
        iota((ROWS, WIDTH), 1) < PROPS
    )
    own_gates = jnp.dot(
        joined[STATS], jnp.where(picks, 1.0, 0.0).astype(bf16), preferred_element_type=f32
    ).astype(bf16)
    reached = ancestors[...]
    tree = dot_t(own_gates, jnp.concatenate([reached, pad], axis=0).astype(bf16))
    tree = tree[0:8] + tree[8:16]
    last = jnp.sum(
        jnp.where(iota((8, WIDTH), 1) == own, stats[:, 0:WIDTH], 0.0), axis=1, keepdims=True
    )
    tree_bias = jnp.concatenate(
        [
            jnp.broadcast_to(-(last[3:4] + last[5:6] + tree[0:1]), (PROPS, WIDTH)),
            jnp.broadcast_to(-(last[4:5] + last[6:7] + tree[1:2]), (PROPS, WIDTH)),
        ],
        axis=0,
    )
    own_inv = columns[mine, 2:3]
    new_keys = own_inv * joined[own, :, WIDTH : 2 * WIDTH].astype(f32)
    new_values = own_inv * joined[own, :, 2 * WIDTH : 3 * WIDTH].astype(f32)
    new_keys = jnp.concatenate([new_keys, pad], axis=0).astype(bf16)
    new_values = jnp.concatenate([new_values, pad], axis=0).astype(bf16)
    needed = jnp.where(kv < SEQS, 0.5, 2.0)
    live = jnp.concatenate([reached, reached], axis=0) > needed
    tree_scores = jnp.where(live, dot_t(both_heads(mine, own), new_keys) + tree_bias, masked_score)
    tree_top = jnp.max(tree_scores, axis=1, keepdims=True)

    for b in range(SEQS):
        if b % 3 == 0:
            moves[b // 3].wait()
        q = both_heads(pl.ds(PROPS * b, PROPS), b)
        bias = biases[b]
        bias = jnp.concatenate(
            [
                jnp.broadcast_to(bias[0:1], (PROPS, LEN)),
                jnp.broadcast_to(bias[1:2], (PROPS, LEN)),
            ],
            axis=0,
        )
        scores_buf[b] = dot_t(q, keys[b]) + bias
    tops = []
    totals = []
    for b in range(SEQS):
        scores = scores_buf[b]
        top = sendable(jnp.max(scores, axis=1, keepdims=True))
        weights = jnp.exp(scores - top)
        totals.append(jnp.sum(weights, axis=1, keepdims=True))
        tops.append(top)
        weights_buf[b] = weights.astype(bf16)
    for t in range(N_TP):
        moves[N_TP + t].wait()
    for b in range(SEQS):
        v = jnp.dot(weights_buf[b], values[b], preferred_element_type=f32)
        t, s = divmod(b, 3)
        out[t, 32 * s : 32 * s + 32, :] = packed(v, tops[b], totals[b])
    for t in range(N_TP):
        out[t, 96:128, :] = jnp.zeros((32, WIDTH), bf16)

    at = pl.ds(pl.multiple_of(32 * lax.rem(own, 3), 32), 32)
    held = out[lax.div(own, 3), at, :].astype(f32)

    def stat(n):
        pick = (stat_lane == n) & jnp.logical_not(own_lanes)
        return jnp.sum(jnp.where(pick, held, 0.0), axis=1, keepdims=True)

    old_top = stat(0) + stat(1)
    old_sum = stat(2) + stat(3)
    top = sendable(jnp.maximum(old_top, tree_top))
    weights = jnp.exp(tree_scores - top)
    keep = jnp.exp(old_top - top)
    total = keep * old_sum + jnp.sum(weights, axis=1, keepdims=True)
    v = keep * held + jnp.dot(weights.astype(bf16), new_values, preferred_element_type=f32)
    out[lax.div(own, 3), at, :] = packed(v, top, total)


def combine_kernel(parts, after_w, after, out):
    kv = lax.axis_index(KV)
    head = lax.rem(lax.div(kv, 4), 2)
    start = HEAD * (1 - head)
    row = iota((WIDTH, 2 * WIDTH), 0) - start
    row = row - jnp.where(iota((WIDTH, 2 * WIDTH), 1) < WIDTH, 0, 2)
    spread = jnp.where((row == 0) | (row == 1), 1.0, 0.0).astype(bf16)
    results = []
    for g in range(N_TP):
        block = parts[128 * g : 128 * g + 128]
        stats = jnp.dot(block, spread, preferred_element_type=f32)
        tops = stats[:, 0:WIDTH].reshape(16, 8, WIDTH)
        sums = stats[:, WIDTH:].reshape(16, 8, WIDTH)
        floats = block.astype(f32).reshape(16, 8, WIDTH)
        top = jnp.max(tops, axis=0)
        top = jnp.maximum(top, pltpu.roll(top, 4, 0))
        factor = jnp.exp(tops - top[None])
        above = jnp.sum(factor * floats, axis=0)
        below = jnp.sum(factor * sums, axis=0)
        above = above + pltpu.roll(above, 4, 0)
        below = below + pltpu.roll(below, 4, 0)
        results.append(above / below)
    lane = iota((8, WIDTH), 1)
    first = iota((8, WIDTH), 0) < 4
    pairs = []
    for p in range(4):
        even, odd = results[2 * p], results[2 * p + 1]
        even = jnp.where(head == 0, even, pltpu.roll(even, HEAD, 1))
        odd = jnp.where(head == 1, odd, pltpu.roll(odd, HEAD, 1))
        pairs.append(jnp.where(lane < HEAD, even, odd))
    block = jnp.concatenate(
        [jnp.where(first, pairs[0], pairs[1]), jnp.where(first, pairs[2], pairs[3])], axis=0
    ).astype(bf16)
    for k in range(N_KV):
        out[k] = block


def output_kernel(shared, w_0, w_1, w_2, w_4, out, rows):
    tp = lax.axis_index("tp")
    for s in range(3):
        for h in range(2):
            for i in range(4):
                block = shared[8 * s + 4 * h + i].astype(f32)
                for p in range(4):
                    rows[16 * s + 4 * i : 16 * s + 4 * i + 4, pl.ds((2 * p + h) * WIDTH, WIDTH)] = (
                        block[4 * p : 4 * p + 4]
                    )
    near = (w_0[...], w_1[...], w_2[0], w_2[1], w_4[0], w_4[1], w_4[2], w_4[3])
    near = [w.astype(f32) for w in near]
    for bit in (1, 2, 4):
        swap = (tp & bit) != 0
        near = [jnp.where(swap, near[g ^ bit], near[g]) for g in range(N_TP)]
    lane = iota((64, WIDTH), 1)
    total = jnp.zeros((48, 64), f32)
    for p in range(4):
        even, odd = near[2 * p], near[2 * p + 1]
        for h in range(2):
            if h == 0:
                weight = jnp.where(lane < HEAD, even, pltpu.roll(odd, HEAD, 1))
            else:
                weight = jnp.where(lane < HEAD, pltpu.roll(even, HEAD, 1), odd)
            block = rows[:, (2 * p + h) * WIDTH : (2 * p + h + 1) * WIDTH].astype(bf16)
            total = total + dot_t(block, weight.astype(bf16))
    out[...] = total.astype(bf16)


def join_kernel(first, second, out):
    count = first.shape[0]
    out[0:count] = first[...]
    out[count:] = second[...]


def copy_kernel(
    after, parents, keys, values, keys_out, values_out, ancestors, keys_near, values_near, sems
):
    moves = []
    for n, (source, near, target) in enumerate(
        ((keys, keys_near, keys_out), (values, values_near, values_out))
    ):
        for t in range(8):
            three = pl.ds(3 * t, 3)
            moves.append(
                (
                    pltpu.make_async_copy(source.at[three], near.at[three], sems.at[0, 8 * n + t]),
                    pltpu.make_async_copy(near.at[three], target.at[three], sems.at[1, 8 * n + t]),
                )
            )
    for move in moves:
        move[0].start()
    own = jnp.minimum(lax.axis_index(KV), SEQS - 1)
    row = iota((PROPS, WIDTH), 0)
    lane = iota((PROPS, WIDTH), 1)
    reached = jnp.where(lane == row, 1.0, 0.0)
    for i in range(PROPS):
        reached = jnp.where((row == i) & (lane == parents[i, own]), 1.0, reached)
    pad = jnp.zeros((WIDTH - PROPS, WIDTH), f32)
    for _ in range(4):
        other = jnp.concatenate([reached, pad], axis=0).astype(bf16)
        reached = jnp.minimum(jnp.dot(reached.astype(bf16), other, preferred_element_type=f32), 1.0)
    ancestors[...] = reached
    for move in moves:
        move[0].wait()
        move[1].start()
    for move in moves:
        move[1].wait()


def write_kernel(
    prior, accepted, joined, after, keys_in, values_in, keys, values, buf, columns, in_sem, out_sem
):
    offset = lax.axis_index(KV) * LEN
    coded = joined[STATS].astype(f32)
    columns[...] = jnp.transpose(coded[0:8] + coded[8:16])

    def place(b):
        start = prior[b] + accepted[b] - offset
        base = jnp.clip(lax.div(jnp.maximum(start, 0), 16) * 16, 0, LEN - WINDOW)
        hit = (start > -PROPS) & (start < LEN)
        return start, pl.multiple_of(base, 16), hit

    def copy_in(n, b, base):
        source = (keys, values)[n].at[b, pl.ds(base, WINDOW), :]
        return pltpu.make_async_copy(source, buf.at[n, b], in_sem.at[n, b])

    def copy_out(n, b, base):
        target = (keys, values)[n].at[b, pl.ds(base, WINDOW), :]
        return pltpu.make_async_copy(buf.at[n, b], target, out_sem.at[n, b])

    @pl.loop(0, SEQS)
    def _(b):
        start, base, hit = place(b)

        @pl.when(hit)
        def _():
            for n in range(2):
                copy_in(n, b, base).start()

    @pl.loop(0, SEQS)
    def _(b):
        start, base, hit = place(b)

        @pl.when(hit)
        def _():
            inv = columns[pl.ds(pl.multiple_of(PROPS * b, PROPS), PROPS), 2:3]
            slot = iota((WINDOW, PROPS), 0) + (base - start)
            selector = jnp.where(slot == iota((WINDOW, PROPS), 1), 1.0, 0.0).astype(bf16)
            slot = iota((WINDOW, WIDTH), 0) + (base - start)
            inside = (slot >= 0) & (slot < PROPS)
            for n in range(2):
                raw = joined[b, :, (n + 1) * WIDTH : (n + 2) * WIDTH].astype(f32)
                rows = jnp.dot(selector, (inv * raw).astype(bf16), preferred_element_type=f32)
                copy_in(n, b, base).wait()
                held = buf[n, b].astype(f32)
                buf[n, b] = jnp.where(inside, rows, held).astype(bf16)
                copy_out(n, b, base).start()

    @pl.loop(0, SEQS)
    def _(b):
        start, base, hit = place(b)

        @pl.when(hit)
        def _():
            for n in range(2):
                copy_out(n, b, base).wait()


def shards(
    tokens,
    norm_gain,
    w_query,
    w_key,
    w_value,
    w_gate,
    gate_bias,
    w_out,
    keys_cache,
    values_cache,
    cum_gates,
    prior_len,
    accepted,
    parents,
):
    cache = jax.ShapeDtypeStruct(keys_cache.shape, bf16)

    def near(*arrays):
        return [pltpu.with_memory_space_constraint(a, pltpu.VMEM) for a in arrays]

    def far(*arrays):
        return [pltpu.with_memory_space_constraint(a, pltpu.HBM) for a in arrays]

    def limit(mib):
        return pltpu.CompilerParams(vmem_limit_bytes=mib << 20)

    parts, biases = pl.pallas_call(
        project_kernel,
        out_shape=(
            jax.ShapeDtypeStruct((N_KV, PROPS, ROWS), bf16),
            pltpu.VMEM(cum_gates.shape, f32),
        ),
        in_specs=[SM, SM, VM, VM, VM, VM, VM, ANY, VM],
        out_specs=(VM, VM),
        scratch_shapes=[
            pltpu.VMEM((16, WIDTH), bf16),
            pltpu.VMEM((16, ROWS), f32),
            pltpu.SemaphoreType.DMA,
        ],
        name="project",
    )(
        prior_len,
        accepted,
        tokens.T,
        norm_gain[None],
        w_query,
        w_key,
        w_value,
        w_gate.T,
        cum_gates,
    )
    arrived = lax.all_to_all(parts, KV, 0, 0, tiled=True)

    keys_copy, values_copy, ancestors = pl.pallas_call(
        copy_kernel,
        out_shape=(
            cache,
            cache,
            pltpu.VMEM((PROPS, WIDTH), f32),
        ),
        in_specs=[ANY, SM, ANY, ANY],
        out_specs=(ANY, ANY, VM),
        scratch_shapes=[
            pltpu.VMEM(keys_cache.shape, bf16),
            pltpu.VMEM(keys_cache.shape, bf16),
            pltpu.SemaphoreType.DMA((2, 16)),
        ],
        compiler_params=limit(8),
        cost_estimate=pl.CostEstimate(
            flops=2_000_000_000, bytes_accessed=12_600_000, transcendentals=0
        ),
        name="copy",
    )(*far(parts), parents.T, *far(keys_cache, values_cache))

    tp_count = lax.axis_size("tp")

    def gathered(name, *pieces):
        return pl.pallas_call(
            join_kernel,
            out_shape=pltpu.VMEM((sum(len(p) for p in pieces), *pieces[0].shape[1:]), bf16),
            in_specs=[VM, VM],
            out_specs=VM,
            compiler_params=limit(2),
            name=name,
        )(*near(*pieces))

    def across(x, bit):
        return lax.ppermute(x, "tp", [(i, i ^ bit) for i in range(tp_count)])

    w_0 = w_out.T
    w_1 = across(w_0, 1)
    w_pair = gathered("pair", w_0[None], w_1[None])
    w_2 = across(w_pair, 2)
    w_4 = across(gathered("four", w_pair, w_2), 4)

    block = pl.pallas_call(
        share_kernel,
        out_shape=pltpu.VMEM((N_KV, PROPS, ROWS), bf16),
        in_specs=[SM, VM, VM, VM],
        out_specs=VM,
        compiler_params=limit(8),
        name="share",
    )(gate_bias, *near(arrived, ancestors, w_2))
    joined = lax.all_to_all(block, KV, 0, 0, tiled=True)

    sent = pl.pallas_call(
        attention_kernel,
        out_shape=jax.ShapeDtypeStruct((N_TP, 128, WIDTH), bf16),
        in_specs=[VM, VM, VM, ANY, ANY],
        out_specs=VM,
        scratch_shapes=[
            pltpu.VMEM((ROWS, 8), f32),
            pltpu.VMEM((SEQS, 2 * PROPS, LEN), f32),
            pltpu.VMEM((SEQS, 2 * PROPS, LEN), bf16),
            pltpu.VMEM(keys_cache.shape, bf16),
            pltpu.VMEM(keys_cache.shape, bf16),
            pltpu.SemaphoreType.DMA((2, N_TP)),
        ],
        compiler_params=limit(20),
        name="attention",
    )(*near(ancestors, joined, biases), *far(keys_cache, values_cache))
    pieces = lax.all_to_all(sent.reshape(256, 4, WIDTH), ("tp", *KV), 0, 0, tiled=True)

    keys_out, values_out = pl.pallas_call(
        write_kernel,
        out_shape=(cache, cache),
        in_specs=[SM, SM, VM, ANY, ANY, ANY],
        out_specs=(ANY, ANY),
        input_output_aliases={4: 0, 5: 1},
        scratch_shapes=[
            pltpu.VMEM((2, SEQS, WINDOW, WIDTH), bf16),
            pltpu.VMEM((ROWS, 8), f32),
            pltpu.SemaphoreType.DMA((2, SEQS)),
            pltpu.SemaphoreType.DMA((2, SEQS)),
        ],
        compiler_params=limit(8),
        cost_estimate=pl.CostEstimate(
            flops=2_000_000_000, bytes_accessed=100_000, transcendentals=0
        ),
        name="write",
    )(
        *far(prior_len, accepted),
        *near(joined),
        *far(sent, keys_copy, values_copy),
    )

    combined = pl.pallas_call(
        combine_kernel,
        out_shape=pltpu.VMEM((N_KV, PROPS, WIDTH), bf16),
        in_specs=[VM, VM, ANY],
        out_specs=VM,
        compiler_params=limit(8),
        name="combine",
    )(*near(pieces.reshape(1024, WIDTH), w_4), *far(keys_out))
    shared = lax.all_to_all(combined, KV, 0, 0, tiled=True)

    mixed_rows = pl.pallas_call(
        output_kernel,
        out_shape=jax.ShapeDtypeStruct((48, 64), bf16),
        in_specs=[VM] * 5,
        out_specs=VM,
        scratch_shapes=[pltpu.VMEM((48, 1024), f32)],
        compiler_params=limit(8),
        name="output",
    )(*near(shared, w_0, w_1, w_2, w_4))
    return (mixed_rows, keys_out, values_out)


def solution(mesh):
    torus = Mesh(mesh.devices.reshape(8, 4, mesh.shape["tp"]), ("kv_0", "kv_1", "tp"))
    in_specs = (
        P(None, KV),
        P(KV),
        P(KV, "tp"),
        P(KV, "tp"),
        P(KV, "tp"),
        P(),
        P(),
        P("tp", KV),
        P(None, KV, "tp"),
        P(None, KV, "tp"),
        P(None, "tp", KV),
        P(),
        P(),
        P(),
    )
    out_specs = (P("tp", KV), P(None, KV, "tp"), P(None, KV, "tp"))
    return jax.shard_map(
        shards, mesh=torus, in_specs=in_specs, out_specs=out_specs, check_vma=False
    )
```

time: 300 us -> 94.8 us (0.32)
  Pallas kernels: 215 us -> 19.4 us
  blocking collectives: 45.7 us -> 33.7 us
  waiting for transfers between devices: 7.73 us -> 16.6 us
  local copies, waits for them, and re-layouts: 6.92 us -> 1.42 us
    pallas_call x4 -> x6, Pallas kernels: 199 us -> 10.2 us  [the longest x1 6.17 us: shards(): pl.pallas_call(copy_kernel, out_shape=(cache, cache, pltpu.VMEM((PROPS, W...]
    all_to_all x1, blocking collectives: 26.7 us -> 14.4 us  [shards(): shared = lax.all_to_all(combined, KV, 0, 0, tiled=True)]
    all_to_all x1, waiting for transfers between devices: 0.01 us -> 8.21 us  [shards(): lax.all_to_all(sent.reshape(256, 4, WIDTH), ('tp', *KV), 0, 0, tiled=True)]
    pallas_call x1, Pallas kernels: 11.4 us -> 5.53 us  [shards(): pl.pallas_call(attention_kernel, out_shape=jax.ShapeDtypeStruct((N_TP, 12...]
    all_to_all x2 -> x1, starting transfers between devices: 15.4 us -> 11.3 us  [shards(): arrived = lax.all_to_all(parts, KV, 0, 0, tiled=True)]
    unnamed x11 -> x8, local copies, waits for them, and re-layouts: 5.41 us -> 1.42 us
    all_to_all x2 -> x1, waiting for transfers between devices: 7.73 us -> 5.75 us  [shards(): arrived = lax.all_to_all(parts, KV, 0, 0, tiled=True)]
  transfers between devices with their start and end apart: 3 -> 5, of which waited for: 1 -> 4; matrix products, arithmetic and copies ran while one was open for 1% -> 0% of each run, Pallas kernels for 69% -> 9%
where the time goes in v2:
time: 94.8 us; the launch traced here: 94.2 us
  blocking collectives  33.7 us (36%)
  starting transfers between devices  22.4 us (24%)
  Pallas kernels  19.4 us (20%)
  waiting for transfers between devices  16.6 us (18%)
  local copies, waits for them, and re-layouts  1.42 us (1%)
    all_to_all x1, blocking collectives, shards(): joined = lax.all_to_all(block, KV, 0, 0, tiled=True)  19.3 us
    all_to_all x1, blocking collectives, shards(): shared = lax.all_to_all(combined, KV, 0, 0, tiled=True)  14.4 us
    all_to_all x1, starting transfers between devices, shards(): arrived = lax.all_to_all(parts, KV, 0, 0, tiled=True)  11.3 us
    all_to_all x1, starting transfers between devices, shards(): lax.all_to_all(sent.reshape(256, 4, WIDTH), ('tp', *KV), 0, 0, tiled=True)  8.33 us
    all_to_all x1, waiting for transfers between devices, shards(): lax.all_to_all(sent.reshape(256, 4, WIDTH), ('tp', *KV), 0, 0, tiled=True)  8.21 us
    pallas_call x1, Pallas kernels, shards(): pl.pallas_call(copy_kernel, out_shape=(cache, cache, pltpu.VMEM((PROPS, W...  6.17 us
    all_to_all x1, waiting for transfers between devices, shards(): arrived = lax.all_to_all(parts, KV, 0, 0, tiled=True)  5.75 us
    pallas_call x1, Pallas kernels, shards(): pl.pallas_call(attention_kernel, out_shape=jax.ShapeDtypeStruct((N_TP, 12...  5.53 us
  transfers between devices with their start and end apart: 5, of which 4 were waited for; matrix products, arithmetic and copies ran while one was open for 0% of the time, Pallas kernels for 9%

profile of v2, /device:TPU:8, one launch (start us, length us, event | category | flops | bytes accessed | tf_op | source)
XLA Modules:
  0.0 94.2 jit_solution(12133784250007051390)
XLA Ops:
  0.6 2.9 %project.1 = (bf16[32,16,384]{2,1,0:T(8,128)(2,1)}, f32[24,2,512]{2,1,0:T(2,128)S(1)}) custom-call(s32[24]{0:T(128)} %prior.3, s32[24]{0:T(128)} %accepted.3, bf16[64,384]{1,0:T(8,128)(2,1)} %bitcast.17, f32[1,64]{1,0:T(1,128)} %bitcast.18, bf16[64,128]{1,0:T(8,128)(2,1)} %w_q.1, bf16[64,128]{1,0:T(8,128)(2,1)} %w_k.1, bf16[64,128]{1,0:T(8,128)(2,1)} %w_v.1, ...), custom_call_target="tpu_custom_call" | custom-call | tf_op jit(solution)/shard_map/project/pallas_call | solution.py:446
  3.6 11.3 %all-to-all-start = ((bf16[32,16,384]{2,1,0:T(8,128)(2,1)}), bf16[32,16,384]{2,1,0:T(8,128)(2,1)S(1)}, u32[]{:S(2)}, u32[]{:S(2)}) async-start(bf16[32,16,384]{2,1,0:T(8,128)(2,1)} %get-tuple-element.10.after), calls=%async_computation | async-start | bytes 786432 | tf_op jit(solution)/shard_map/all_to_all | solution.py:471
  14.9 0.1 collective-permute-start
  15.0 1.4 %collective-permute-done.w_1 = bf16[64,128]{1,0:T(8,128)(2,1)S(1)} collective-permute-done((bf16[64,128]{1,0:T(8,128)(2,1)}, bf16[64,128]{1,0:T(8,128)(2,1)S(1)}, u32[]{:S(2)}, u32[]{:S(2)}) %collective-permute-start) | collective-permute-done | bytes 16416 | tf_op jit(solution)/shard_map/ppermute | solution.py:507
  16.4 0.0 copy-start
  16.4 0.7 copy-done
  17.1 0.4 collective-permute-start.1
  17.6 0.0 copy-start.3
  17.6 0.7 copy-done.3
  18.3 0.0 copy-start.2
  18.3 6.2 %copy.22 = (bf16[24,512,128]{2,1,0:T(8,128)(2,1)}, bf16[24,512,128]{2,1,0:T(8,128)(2,1)}, f32[16,128]{1,0:T(8,128)S(1)}) custom-call(bf16[32,16,384]{2,1,0:T(8,128)(2,1)} %get-tuple-element.10.after, s32[16,24]{1,0:T(8,128)S(1)} %bitcast.15, bf16[24,512,128]{2,1,0:T(8,128)(2,1)} %keys_far.1, bf16[24,512,128]{2,1,0:T(8,128)(2,1)} %values_far.1), custom_call_target="tpu_custom_call" | custom-call | flops 2000000000 | bytes 12600000 | tf_op jit(solution)/shard_map/copy/pallas_call | solution.py:473
  24.4 0.0 collective-permute-done.1.after_w.second.w_2
  24.4 5.7 %all-to-all-done.parts = bf16[32,16,384]{2,1,0:T(8,128)(2,1)S(1)} async-done(((bf16[32,16,384]{2,1,0:T(8,128)(2,1)}), bf16[32,16,384]{2,1,0:T(8,128)(2,1)S(1)}, u32[]{:S(2)}, u32[]{:S(2)}) %all-to-all-start) | async-done | bytes 393248 | tf_op jit(solution)/shard_map/all_to_all | solution.py:471
  30.2 0.0 copy-done.2
  30.2 0.7 share.1
  30.9 19.3 %all_to_all.20.joined = bf16[32,16,384]{2,1,0:T(8,128)(2,1)S(1)} all-to-all(bf16[32,16,384]{2,1,0:T(8,128)(2,1)S(1)} %share.1), channel_id=1, replica_groups=mesh['kv_0'=8,'kv_1'=4,'tp'=8] {'kv_0','kv_1'}, dimensions={0} | all-to-all | bytes 786432 | tf_op jit(solution)/shard_map/all_to_all | solution.py:523
  50.2 5.5 %attention.1.after = bf16[8,128,128]{2,1,0:T(8,128)(2,1)} custom-call(f32[16,128]{1,0:T(8,128)S(1)} %get-tuple-element.11.after.ancestors, bf16[32,16,384]{2,1,0:T(8,128)(2,1)S(1)} %all_to_all.20.joined, f32[24,2,512]{2,1,0:T(2,128)S(1)} %get-tuple-element.12.biases, bf16[24,512,128]{2,1,0:T(8,128)(2,1)} %keys_far.1, bf16[24,512,128]{2,1,0:T(8,128)(2,1)} %values_far.1), custom_call_target="tpu_custom_call" | custom-call | tf_op jit(solution)/shard_map/attention/pallas_call | solution.py:525
  55.7 8.3 %all-to-all-start.2 = ((bf16[256,4,128]{2,1,0:T(4,128)(2,1)}), bf16[256,4,128]{2,1,0:T(4,128)(2,1)S(1)}, u32[]{:S(2)}, u32[]{:S(2)}) async-start(bf16[256,4,128]{2,1,0:T(4,128)(2,1)} %bitcast.7), calls=%async_computation.2 | async-start | bytes 524288 | tf_op jit(solution)/shard_map/all_to_all | solution.py:541
  64.0 2.2 %collective-permute-start.2 = (bf16[4,64,128]{2,1,0:T(8,128)(2,1)S(1)}, bf16[4,64,128]{2,1,0:T(8,128)(2,1)S(1)}, u32[]{:S(2)}, u32[]{:S(2)}) collective-permute-start(bf16[4,64,128]{2,1,0:T(8,128)(2,1)S(1)} %four.1), channel_id=1, source_target_pairs={{0,4},{1,5},{2,6},{3,7},{4,0},{5,1},{6,2},{7,3},{8,12},{9,13},{10,... | collective-permute-start | bytes 196616 | tf_op jit(solution)/shard_map/ppermute | solution.py:507
  66.2 2.7 %write.1 = (bf16[24,512,128]{2,1,0:T(8,128)(2,1)}, bf16[24,512,128]{2,1,0:T(8,128)(2,1)}) custom-call(s32[24]{0:T(128)} %prior.3, s32[24]{0:T(128)} %accepted.3, bf16[32,16,384]{2,1,0:T(8,128)(2,1)S(1)} %all_to_all.20.joined, bf16[8,128,128]{2,1,0:T(8,128)(2,1)} %attention.1.after, ...), custom_call_target="tpu_custom_call", output_to_operand_aliasing={{0}: (4, {}), {1}: (5, {})} | custom-call | flops 2000000000 | bytes 100000 | tf_op jit(solution)/shard_map/write/pallas_call | solution.py:543
  69.0 0.0 copy-start.1
  69.0 1.3 %collective-permute-done.2.after_w.w_4 = bf16[4,64,128]{2,1,0:T(8,128)(2,1)S(1)} collective-permute-done((bf16[4,64,128]{2,1,0:T(8,128)(2,1)S(1)}, bf16[4,64,128]{2,1,0:T(8,128)(2,1)S(1)}, u32[]{:S(2)}, u32[]{:S(2)}) %collective-permute-start.2) | collective-permute-done | bytes 65568 | tf_op jit(solution)/shard_map/ppermute | solution.py:507
  70.2 8.2 %all-to-all-done.2 = bf16[256,4,128]{2,1,0:T(4,128)(2,1)S(1)} async-done(((bf16[256,4,128]{2,1,0:T(4,128)(2,1)}), bf16[256,4,128]{2,1,0:T(4,128)(2,1)S(1)}, u32[]{:S(2)}, u32[]{:S(2)}) %all-to-all-start.2) | async-done | bytes 262176 | tf_op jit(solution)/shard_map/all_to_all | solution.py:541
  78.4 0.5 combine.1
  78.9 14.4 %all_to_all.21.shared = bf16[32,16,128]{2,1,0:T(8,128)(2,1)S(1)} all-to-all(bf16[32,16,128]{2,1,0:T(8,128)(2,1)S(1)} %combine.1), channel_id=1, replica_groups=mesh['kv_0'=8,'kv_1'=4,'tp'=8] {'kv_0','kv_1'}, dimensions={0} | all-to-all | bytes 262144 | tf_op jit(solution)/shard_map/all_to_all | solution.py:574
  93.3 0.0 copy-done.1
  93.3 0.9 output.1
  (2 shorter events, 0.0 us)
Async XLA Ops:
  3.6 26.6 %all-to-all-start = ((bf16[32,16,384]{2,1,0:T(8,128)(2,1)}), bf16[32,16,384]{2,1,0:T(8,128)(2,1)S(1)}, u32[]{:S(2)}, u32[]{:S(2)}) async-start(bf16[32,16,384]{2,1,0:T(8,128)(2,1)} %get-tuple-element.10.after), calls=%async_computation | async-start | bytes 786432 | tf_op jit(solution)/shard_map/all_to_all | solution.py:471
  14.9 1.5 %collective-permute-start = (bf16[64,128]{1,0:T(8,128)(2,1)}, bf16[64,128]{1,0:T(8,128)(2,1)S(1)}, u32[]{:S(2)}, u32[]{:S(2)}) collective-permute-start(bf16[64,128]{1,0:T(8,128)(2,1)} %bitcast.11), channel_id=1, source_target_pairs={{0,1},{1,0},{2,3},{3,2},{4,5},{5,4},{6,7},{7,6},{8,9},{9,8},{10,11... | collective-permute-start | bytes 49160 | tf_op jit(solution)/shard_map/ppermute | solution.py:507
  16.4 0.7 copy-start
  17.1 7.3 %collective-permute-start.1 = (bf16[2,64,128]{2,1,0:T(8,128)(2,1)S(1)}, bf16[2,64,128]{2,1,0:T(8,128)(2,1)S(1)}, u32[]{:S(2)}, u32[]{:S(2)}) collective-permute-start(bf16[2,64,128]{2,1,0:T(8,128)(2,1)S(1)} %pair.1.first), channel_id=1, source_target_pairs={{0,2},{1,3},{2,0},{3,1},{4,6},{5,7},{6,4},{7,5},{8,10},{9,11},{10,... | collective-permute-start | bytes 98312 | tf_op jit(solution)/shard_map/ppermute | solution.py:507
  17.6 0.7 copy-start.3
  18.3 11.9 %copy-start.2 = (f32[16]{0:T(128)S(1)}, f32[16]{0:T(128)}, u32[]{:S(2)}) copy-start(f32[16]{0:T(128)} %bias.1) | copy-start | bytes 196
  55.7 22.7 %all-to-all-start.2 = ((bf16[256,4,128]{2,1,0:T(4,128)(2,1)}), bf16[256,4,128]{2,1,0:T(4,128)(2,1)S(1)}, u32[]{:S(2)}, u32[]{:S(2)}) async-start(bf16[256,4,128]{2,1,0:T(4,128)(2,1)} %bitcast.7), calls=%async_computation.2 | async-start | bytes 524288 | tf_op jit(solution)/shard_map/all_to_all | solution.py:541
  64.0 6.2 %collective-permute-start.2 = (bf16[4,64,128]{2,1,0:T(8,128)(2,1)S(1)}, bf16[4,64,128]{2,1,0:T(8,128)(2,1)S(1)}, u32[]{:S(2)}, u32[]{:S(2)}) collective-permute-start(bf16[4,64,128]{2,1,0:T(8,128)(2,1)S(1)} %four.1), channel_id=1, source_target_pairs={{0,4},{1,5},{2,6},{3,7},{4,0},{5,1},{6,2},{7,3},{8,12},{9,13},{10,... | collective-permute-start | bytes 196616 | tf_op jit(solution)/shard_map/ppermute | solution.py:507
  69.0 24.3 %copy-start.1 = (bf16[128,64]{0,1:T(8,128)(2,1)S(1)}, bf16[128,64]{0,1:T(8,128)(2,1)}, u32[]{:S(2)}) copy-start(bf16[128,64]{0,1:T(8,128)(2,1)} %param.21) | copy-start | bytes 49156

commit v3 on v2

--- a/solution.py
+++ b/solution.py
@@ -125,6 +125,9 @@
     weights_buf,
     keys,
     values,
+    v_buf,
+    stat_buf,
+    mixed,
     sems,
 ):
     kv = lax.axis_index(KV)
@@ -143,9 +146,7 @@
     lane = iota((PROPS, WIDTH), 1)
     first_head = lane < HEAD
     lane_out = iota((2 * PROPS, WIDTH), 1)
-    row_out = iota((2 * PROPS, WIDTH), 0)
-    own_lanes = (lane_out < HEAD) == (row_out < PROPS)
-    stat_lane = jnp.where(row_out < PROPS, lane_out - HEAD, lane_out)
+    first_row = iota((2 * PROPS, WIDTH), 0) < PROPS
     scale = HEAD**-0.5
 
     def both_heads(b_rows, b_block):
@@ -156,15 +157,12 @@
             [jnp.where(first_head, q, zero), jnp.where(first_head, zero, q)], axis=0
         ).astype(bf16)
 
-    def packed(v, top, total):
+    def coded_stats(s, top, total):
+        place = lane_out - (HEAD + 4 * s)
         top_high, top_low = high_low(top)
         sum_high, sum_low = high_low(total)
-        stats = jnp.where(
-            stat_lane == 0,
-            top_high,
-            jnp.where(stat_lane == 1, top_low, jnp.where(stat_lane == 2, sum_high, sum_low)),
-        )
-        return jnp.where(own_lanes, v, stats).astype(bf16)
+        stats = jnp.where(place == 0, top_high, jnp.where(place == 1, top_low, 0.0))
+        return jnp.where(place == 2, sum_high, jnp.where(place == 3, sum_low, stats))
 
     def sendable(top):
         high, low = high_low(jnp.maximum(top, lowest_max))
@@ -215,104 +213,99 @@
             axis=0,
         )
         scores_buf[b] = dot_t(q, keys[b]) + bias
-    tops = []
-    totals = []
     for b in range(SEQS):
         scores = scores_buf[b]
         top = sendable(jnp.max(scores, axis=1, keepdims=True))
         weights = jnp.exp(scores - top)
-        totals.append(jnp.sum(weights, axis=1, keepdims=True))
-        tops.append(top)
+        total = jnp.sum(weights, axis=1, keepdims=True)
         weights_buf[b] = weights.astype(bf16)
+        stat_buf[b] = coded_stats(b % 3, top, total)
     for t in range(N_TP):
         moves[N_TP + t].wait()
     for b in range(SEQS):
-        v = jnp.dot(weights_buf[b], values[b], preferred_element_type=f32)
-        t, s = divmod(b, 3)
-        out[t, 32 * s : 32 * s + 32, :] = packed(v, tops[b], totals[b])
+        v_buf[b] = jnp.dot(weights_buf[b], values[b], preferred_element_type=f32)
+
+    scores = scores_buf[own]
+    top = jnp.maximum(jnp.max(scores, axis=1, keepdims=True), tree_top)
+    top = sendable(top)
+    weights = jnp.exp(scores - top)
+    tree_weights = jnp.exp(tree_scores - top)
+    total = jnp.sum(weights, axis=1, keepdims=True) + jnp.sum(tree_weights, axis=1, keepdims=True)
+    stat_buf[own] = coded_stats(lax.rem(own, 3), top, total)
+    v_buf[own] = jnp.dot(
+        weights.astype(bf16), values[own], preferred_element_type=f32
+    ) + jnp.dot(tree_weights.astype(bf16), new_values, preferred_element_type=f32)
+
+    low = lane_out < HEAD
     for t in range(N_TP):
-        out[t, 96:128, :] = jnp.zeros((32, WIDTH), bf16)
-
-    at = pl.ds(pl.multiple_of(32 * lax.rem(own, 3), 32), 32)
-    held = out[lax.div(own, 3), at, :].astype(f32)
-
-    def stat(n):
-        pick = (stat_lane == n) & jnp.logical_not(own_lanes)
-        return jnp.sum(jnp.where(pick, held, 0.0), axis=1, keepdims=True)
-
-    old_top = stat(0) + stat(1)
-    old_sum = stat(2) + stat(3)
-    top = sendable(jnp.maximum(old_top, tree_top))
-    weights = jnp.exp(tree_scores - top)
-    keep = jnp.exp(old_top - top)
-    total = keep * old_sum + jnp.sum(weights, axis=1, keepdims=True)
-    v = keep * held + jnp.dot(weights.astype(bf16), new_values, preferred_element_type=f32)
-    out[lax.div(own, 3), at, :] = packed(v, top, total)
-
-
-def combine_kernel(parts, after_w, after, out):
-    kv = lax.axis_index(KV)
-    head = lax.rem(lax.div(kv, 4), 2)
-    start = HEAD * (1 - head)
-    row = iota((WIDTH, 2 * WIDTH), 0) - start
-    row = row - jnp.where(iota((WIDTH, 2 * WIDTH), 1) < WIDTH, 0, 2)
+        v = [v_buf[3 * t + s] for s in range(3)]
+        turned = [pltpu.roll(x, HEAD, 1) for x in v]
+        first = jnp.where(first_row, v[0], turned[0])
+        second = jnp.where(first_row, turned[1], v[1])
+        third = jnp.where(first_row, v[2], turned[2])
+        stats = stat_buf[3 * t] + stat_buf[3 * t + 1] + stat_buf[3 * t + 2]
+        mixed[pl.ds(2 * t, N_KV, stride=16), :] = jnp.where(low, first, second)
+        mixed[pl.ds(2 * t + 1, N_KV, stride=16), :] = jnp.where(low, third, stats)
+    out[...] = mixed[...].astype(bf16)
+
+
+def combine_kernel(parts, after_w, after, out, tops, sums):
+    row = iota((WIDTH, 4 * WIDTH), 0) - HEAD
+    column = iota((WIDTH, 4 * WIDTH), 1)
+    unit = jnp.where(column < 2 * WIDTH, lax.rem(lax.div(column, HEAD), 2), 2)
+    kind = lax.rem(lax.div(column, WIDTH), 2)
+    row = row - 4 * unit - 2 * kind
     spread = jnp.where((row == 0) | (row == 1), 1.0, 0.0).astype(bf16)
+    even = lax.rem(iota((8, WIDTH), 0), 2) == 0
+    for n in range(4):
+        stats = jnp.dot(parts[128 * n : 128 * n + 128], spread, preferred_element_type=f32)
+        for v in range(16):
+            rows = stats[8 * v : 8 * v + 8]
+            near = pltpu.roll(rows[:, 0 : 2 * WIDTH], 7, 0)
+            tops[16 * n + v] = jnp.where(even, near[:, 0:WIDTH], rows[:, 2 * WIDTH : 3 * WIDTH])
+            sums[16 * n + v] = jnp.where(even, near[:, WIDTH:], rows[:, 3 * WIDTH :])
     results = []
-    for g in range(N_TP):
-        block = parts[128 * g : 128 * g + 128]
-        stats = jnp.dot(block, spread, preferred_element_type=f32)
-        tops = stats[:, 0:WIDTH].reshape(16, 8, WIDTH)
-        sums = stats[:, WIDTH:].reshape(16, 8, WIDTH)
-        floats = block.astype(f32).reshape(16, 8, WIDTH)
-        top = jnp.max(tops, axis=0)
-        top = jnp.maximum(top, pltpu.roll(top, 4, 0))
-        factor = jnp.exp(tops - top[None])
-        above = jnp.sum(factor * floats, axis=0)
-        below = jnp.sum(factor * sums, axis=0)
-        above = above + pltpu.roll(above, 4, 0)
-        below = below + pltpu.roll(below, 4, 0)
+    for half in range(2):
+        top = tops[half]
+        for k in range(1, N_KV):
+            top = jnp.maximum(top, tops[2 * k + half])
+        above = jnp.zeros((8, WIDTH), f32)
+        below = jnp.zeros((8, WIDTH), f32)
+        for k in range(N_KV):
+            v = 2 * k + half
+            factor = jnp.exp(tops[v] - top)
+            above = above + factor * parts[8 * v : 8 * v + 8, :].astype(f32)
+            below = below + factor * sums[v]
         results.append(above / below)
-    lane = iota((8, WIDTH), 1)
-    first = iota((8, WIDTH), 0) < 4
-    pairs = []
-    for p in range(4):
-        even, odd = results[2 * p], results[2 * p + 1]
-        even = jnp.where(head == 0, even, pltpu.roll(even, HEAD, 1))
-        odd = jnp.where(head == 1, odd, pltpu.roll(odd, HEAD, 1))
-        pairs.append(jnp.where(lane < HEAD, even, odd))
-    block = jnp.concatenate(
-        [jnp.where(first, pairs[0], pairs[1]), jnp.where(first, pairs[2], pairs[3])], axis=0
-    ).astype(bf16)
+    block = jnp.concatenate(results, axis=0).astype(bf16)
     for k in range(N_KV):
         out[k] = block
 
 
 def output_kernel(shared, w_0, w_1, w_2, w_4, out, rows):
     tp = lax.axis_index("tp")
-    for s in range(3):
-        for h in range(2):
-            for i in range(4):
-                block = shared[8 * s + 4 * h + i].astype(f32)
-                for p in range(4):
-                    rows[16 * s + 4 * i : 16 * s + 4 * i + 4, pl.ds((2 * p + h) * WIDTH, WIDTH)] = (
-                        block[4 * p : 4 * p + 4]
-                    )
+    rows[...] = shared[...].astype(f32)
     near = (w_0[...], w_1[...], w_2[0], w_2[1], w_4[0], w_4[1], w_4[2], w_4[3])
     near = [w.astype(f32) for w in near]
     for bit in (1, 2, 4):
         swap = (tp & bit) != 0
         near = [jnp.where(swap, near[g ^ bit], near[g]) for g in range(N_TP)]
-    lane = iota((64, WIDTH), 1)
+    low = iota((PROPS, WIDTH), 1) < HEAD
     total = jnp.zeros((48, 64), f32)
-    for p in range(4):
-        even, odd = near[2 * p], near[2 * p + 1]
-        for h in range(2):
-            if h == 0:
-                weight = jnp.where(lane < HEAD, even, pltpu.roll(odd, HEAD, 1))
-            else:
-                weight = jnp.where(lane < HEAD, pltpu.roll(even, HEAD, 1), odd)
-            block = rows[:, (2 * p + h) * WIDTH : (2 * p + h + 1) * WIDTH].astype(bf16)
-            total = total + dot_t(block, weight.astype(bf16))
+    for g in range(N_TP):
+        pair_0 = rows[pl.ds(2 * g, PROPS, stride=16), :]
+        pair_1 = rows[pl.ds(256 + 2 * g, PROPS, stride=16), :]
+        last_0 = rows[pl.ds(2 * g + 1, PROPS, stride=16), :]
+        last_1 = rows[pl.ds(257 + 2 * g, PROPS, stride=16), :]
+        block = jnp.concatenate(
+            [
+                jnp.where(low, pair_0, pltpu.roll(pair_1, HEAD, 1)),
+                jnp.where(low, pltpu.roll(pair_0, HEAD, 1), pair_1),
+                jnp.where(low, last_0, pltpu.roll(last_1, HEAD, 1)),
+            ],
+            axis=0,
+        )
+        total = total + dot_t(block.astype(bf16), near[g].astype(bf16))
     out[...] = total.astype(bf16)
 
 
@@ -322,21 +315,16 @@
     out[count:] = second[...]
 
 
-def copy_kernel(
-    after, parents, keys, values, keys_out, values_out, ancestors, keys_near, values_near, sems
-):
+def copy_kernel(after, parents, keys, keys_out, ancestors, keys_near, sems):
     moves = []
-    for n, (source, near, target) in enumerate(
-        ((keys, keys_near, keys_out), (values, values_near, values_out))
-    ):
-        for t in range(8):
-            three = pl.ds(3 * t, 3)
-            moves.append(
-                (
-                    pltpu.make_async_copy(source.at[three], near.at[three], sems.at[0, 8 * n + t]),
-                    pltpu.make_async_copy(near.at[three], target.at[three], sems.at[1, 8 * n + t]),
-                )
+    for t in range(8):
+        three = pl.ds(3 * t, 3)
+        moves.append(
+            (
+                pltpu.make_async_copy(keys.at[three], keys_near.at[three], sems.at[0, t]),
+                pltpu.make_async_copy(keys_near.at[three], keys_out.at[three], sems.at[1, t]),
             )
+        )
     for move in moves:
         move[0].start()
     own = jnp.minimum(lax.axis_index(KV), SEQS - 1)
@@ -358,11 +346,31 @@
 
 
 def write_kernel(
-    prior, accepted, joined, after, keys_in, values_in, keys, values, buf, columns, in_sem, out_sem
+    prior,
+    accepted,
+    joined,
+    after,
+    keys_in,
+    values_in,
+    keys,
+    values,
+    buf,
+    near,
+    columns,
+    in_sem,
+    out_sem,
+    near_sem,
 ):
+    moves = []
+    for t in range(8):
+        three = pl.ds(3 * t, 3)
+        moves.append(
+            (
+                pltpu.make_async_copy(values_in.at[three], near.at[three], near_sem.at[0, t]),
+                pltpu.make_async_copy(near.at[three], values.at[three], near_sem.at[1, t]),
+            )
+        )
     offset = lax.axis_index(KV) * LEN
-    coded = joined[STATS].astype(f32)
-    columns[...] = jnp.transpose(coded[0:8] + coded[8:16])
 
     def place(b):
         start = prior[b] + accepted[b] - offset
@@ -370,13 +378,15 @@
         hit = (start > -PROPS) & (start < LEN)
         return start, pl.multiple_of(base, 16), hit
 
-    def copy_in(n, b, base):
-        source = (keys, values)[n].at[b, pl.ds(base, WINDOW), :]
-        return pltpu.make_async_copy(source, buf.at[n, b], in_sem.at[n, b])
-
-    def copy_out(n, b, base):
-        target = (keys, values)[n].at[b, pl.ds(base, WINDOW), :]
-        return pltpu.make_async_copy(buf.at[n, b], target, out_sem.at[n, b])
+    def copy_in(b, base):
+        return pltpu.make_async_copy(
+            keys.at[b, pl.ds(base, WINDOW), :], buf.at[b], in_sem.at[b]
+        )
+
+    def copy_out(b, base):
+        return pltpu.make_async_copy(
+            buf.at[b], keys.at[b, pl.ds(base, WINDOW), :], out_sem.at[b]
+        )
 
     @pl.loop(0, SEQS)
     def _(b):
@@ -384,8 +394,43 @@
 
         @pl.when(hit)
         def _():
-            for n in range(2):
-                copy_in(n, b, base).start()
+            copy_in(b, base).start()
+
+    for move in moves:
+        move[0].start()
+    coded = joined[STATS].astype(f32)
+    columns[...] = jnp.transpose(coded[0:8] + coded[8:16])
+
+    def patched(b, start, base):
+        inv = columns[pl.ds(pl.multiple_of(PROPS * b, PROPS), PROPS), 2:3]
+        slot = iota((WINDOW, PROPS), 0) + (base - start)
+        selector = jnp.where(slot == iota((WINDOW, PROPS), 1), 1.0, 0.0).astype(bf16)
+        raw = joined[b, :, WIDTH:].astype(f32)
+        rows = jnp.dot(selector, (inv * raw).astype(bf16), preferred_element_type=f32)
+        slot = iota((WINDOW, WIDTH), 0) + (base - start)
+        return (slot >= 0) & (slot < PROPS), rows
+
+    for t in range(8):
+        moves[t][0].wait()
+
+        @pl.loop(3 * t, 3 * t + 3)
+        def _(b):
+            start, base, hit = place(b)
+
+            @pl.when(hit)
+            def _():
+                inside, rows = patched(b, start, base)
+                window = pl.ds(base, WINDOW)
+                held = near[b, window, :].astype(f32)
+                near[b, window, :] = jnp.where(inside, rows[:, WIDTH:], held).astype(bf16)
+                copy_in(b, base).wait()
+                held = buf[b].astype(f32)
+                buf[b] = jnp.where(inside, rows[:, 0:WIDTH], held).astype(bf16)
+                copy_out(b, base).start()
+
+        moves[t][1].start()
+    for move in moves:
+        move[1].wait()
 
     @pl.loop(0, SEQS)
     def _(b):
@@ -393,27 +438,7 @@
 
         @pl.when(hit)
         def _():
-            inv = columns[pl.ds(pl.multiple_of(PROPS * b, PROPS), PROPS), 2:3]
-            slot = iota((WINDOW, PROPS), 0) + (base - start)
-            selector = jnp.where(slot == iota((WINDOW, PROPS), 1), 1.0, 0.0).astype(bf16)
-            slot = iota((WINDOW, WIDTH), 0) + (base - start)
-            inside = (slot >= 0) & (slot < PROPS)
-            for n in range(2):
-                raw = joined[b, :, (n + 1) * WIDTH : (n + 2) * WIDTH].astype(f32)
-                rows = jnp.dot(selector, (inv * raw).astype(bf16), preferred_element_type=f32)
-                copy_in(n, b, base).wait()
-                held = buf[n, b].astype(f32)
-                buf[n, b] = jnp.where(inside, rows, held).astype(bf16)
-                copy_out(n, b, base).start()
-
-    @pl.loop(0, SEQS)
-    def _(b):
-        start, base, hit = place(b)
-
-        @pl.when(hit)
-        def _():
-            for n in range(2):
-                copy_out(n, b, base).wait()
+            copy_out(b, base).wait()
 
 
 def shards(
@@ -470,26 +495,24 @@
     )
     arrived = lax.all_to_all(parts, KV, 0, 0, tiled=True)
 
-    keys_copy, values_copy, ancestors = pl.pallas_call(
+    keys_copy, ancestors = pl.pallas_call(
         copy_kernel,
         out_shape=(
             cache,
-            cache,
             pltpu.VMEM((PROPS, WIDTH), f32),
         ),
-        in_specs=[ANY, SM, ANY, ANY],
-        out_specs=(ANY, ANY, VM),
+        in_specs=[ANY, SM, ANY],
+        out_specs=(ANY, VM),
         scratch_shapes=[
             pltpu.VMEM(keys_cache.shape, bf16),
-            pltpu.VMEM(keys_cache.shape, bf16),
-            pltpu.SemaphoreType.DMA((2, 16)),
+            pltpu.SemaphoreType.DMA((2, 8)),
         ],
         compiler_params=limit(8),
         cost_estimate=pl.CostEstimate(
             flops=2_000_000_000, bytes_accessed=12_600_000, transcendentals=0
         ),
         name="copy",
-    )(*far(parts), parents.T, *far(keys_cache, values_cache))
+    )(*far(parts), parents.T, *far(keys_cache))
 
     tp_count = lax.axis_size("tp")
 
@@ -524,7 +547,7 @@
 
     sent = pl.pallas_call(
         attention_kernel,
-        out_shape=jax.ShapeDtypeStruct((N_TP, 128, WIDTH), bf16),
+        out_shape=jax.ShapeDtypeStruct((512, WIDTH), bf16),
         in_specs=[VM, VM, VM, ANY, ANY],
         out_specs=VM,
         scratch_shapes=[
@@ -533,24 +556,29 @@
             pltpu.VMEM((SEQS, 2 * PROPS, LEN), bf16),
             pltpu.VMEM(keys_cache.shape, bf16),
             pltpu.VMEM(keys_cache.shape, bf16),
+            pltpu.VMEM((SEQS, 2 * PROPS, WIDTH), f32),
+            pltpu.VMEM((SEQS, 2 * PROPS, WIDTH), f32),
+            pltpu.VMEM((512, WIDTH), f32),
             pltpu.SemaphoreType.DMA((2, N_TP)),
         ],
         compiler_params=limit(20),
         name="attention",
     )(*near(ancestors, joined, biases), *far(keys_cache, values_cache))
-    pieces = lax.all_to_all(sent.reshape(256, 4, WIDTH), ("tp", *KV), 0, 0, tiled=True)
+    pieces = lax.all_to_all(sent.reshape(256, 2, WIDTH), (*KV, "tp"), 0, 0, tiled=True)
 
     keys_out, values_out = pl.pallas_call(
         write_kernel,
         out_shape=(cache, cache),
         in_specs=[SM, SM, VM, ANY, ANY, ANY],
         out_specs=(ANY, ANY),
-        input_output_aliases={4: 0, 5: 1},
+        input_output_aliases={4: 0},
         scratch_shapes=[
-            pltpu.VMEM((2, SEQS, WINDOW, WIDTH), bf16),
+            pltpu.VMEM((SEQS, WINDOW, WIDTH), bf16),
+            pltpu.VMEM(keys_cache.shape, bf16),
             pltpu.VMEM((ROWS, 8), f32),
-            pltpu.SemaphoreType.DMA((2, SEQS)),
-            pltpu.SemaphoreType.DMA((2, SEQS)),
+            pltpu.SemaphoreType.DMA((SEQS,)),
+            pltpu.SemaphoreType.DMA((SEQS,)),
+            pltpu.SemaphoreType.DMA((2, 8)),
         ],
         compiler_params=limit(8),
         cost_estimate=pl.CostEstimate(
@@ -560,7 +588,7 @@
     )(
         *far(prior_len, accepted),
         *near(joined),
-        *far(sent, keys_copy, values_copy),
+        *far(sent, keys_copy, values_cache),
     )
 
     combined = pl.pallas_call(
@@ -568,9 +596,10 @@
         out_shape=pltpu.VMEM((N_KV, PROPS, WIDTH), bf16),
         in_specs=[VM, VM, ANY],
         out_specs=VM,
+        scratch_shapes=[pltpu.VMEM((64, 8, WIDTH), f32), pltpu.VMEM((64, 8, WIDTH), f32)],
         compiler_params=limit(8),
         name="combine",
-    )(*near(pieces.reshape(1024, WIDTH), w_4), *far(keys_out))
+    )(*near(pieces.reshape(512, WIDTH), w_4), *far(keys_out))
     shared = lax.all_to_all(combined, KV, 0, 0, tiled=True)
 
     mixed_rows = pl.pallas_call(
@@ -578,10 +607,10 @@
         out_shape=jax.ShapeDtypeStruct((48, 64), bf16),
         in_specs=[VM] * 5,
         out_specs=VM,
-        scratch_shapes=[pltpu.VMEM((48, 1024), f32)],
+        scratch_shapes=[pltpu.VMEM((512, WIDTH), f32)],
         compiler_params=limit(8),
         name="output",
-    )(*near(shared, w_0, w_1, w_2, w_4))
+    )(*near(shared.reshape(512, WIDTH), w_0, w_1, w_2, w_4))
     return (mixed_rows, keys_out, values_out)
 
 

time: 94.8 us -> 92 us (0.970)
  Pallas kernels: 19.4 us -> 18 us
  waiting for transfers between devices: 16.6 us -> 15.4 us
    pallas_call x2, Pallas kernels: 11.7 us -> 8.84 us  [the longest x1 5.36 us: shards(): pl.pallas_call(attention_kernel, out_shape=jax.ShapeDtypeStruct((512, WID...]
    all_to_all x1, waiting for transfers between devices: 5.75 us -> 8.44 us  [shards(): arrived = lax.all_to_all(parts, KV, 0, 0, tiled=True)]
    all_to_all x1, waiting for transfers between devices: 8.21 us -> 5.6 us  [shards(): lax.all_to_all(sent.reshape(256, 2, WIDTH), (*KV, 'tp'), 0, 0, tiled=True)]
    pallas_call x1, Pallas kernels: 2.7 us -> 4.21 us  [shards(): pl.pallas_call(write_kernel, out_shape=(cache, cache), in_specs=[SM, SM,...]
    ppermute x3, waiting for transfers between devices: 2.64 us -> 1.38 us  [across(): return lax.ppermute(x, 'tp', [(i, i ^ bit) for i in range(tp_count)])]
  transfers between devices with their start and end apart: 5 -> 5, of which waited for: 4 -> 3; matrix products, arithmetic and copies ran while one was open for 0% -> 0% of each run, Pallas kernels for 9% -> 8%
where the time goes in v3:
time: 92 us; the launch traced here: 91.1 us
  blocking collectives  34 us (37%)
  starting transfers between devices  21.5 us (23%)
  Pallas kernels  18 us (20%)
  waiting for transfers between devices  15.4 us (17%)
  local copies, waits for them, and re-layouts  1.42 us (2%)
    all_to_all x1, blocking collectives, shards(): joined = lax.all_to_all(block, KV, 0, 0, tiled=True)  18.8 us
    all_to_all x1, blocking collectives, shards(): shared = lax.all_to_all(combined, KV, 0, 0, tiled=True)  15.2 us
    all_to_all x1, starting transfers between devices, shards(): arrived = lax.all_to_all(parts, KV, 0, 0, tiled=True)  11.3 us
    all_to_all x1, waiting for transfers between devices, shards(): arrived = lax.all_to_all(parts, KV, 0, 0, tiled=True)  8.44 us
    all_to_all x1, starting transfers between devices, shards(): lax.all_to_all(sent.reshape(256, 2, WIDTH), (*KV, 'tp'), 0, 0, tiled=True)  7.46 us
    all_to_all x1, waiting for transfers between devices, shards(): lax.all_to_all(sent.reshape(256, 2, WIDTH), (*KV, 'tp'), 0, 0, tiled=True)  5.6 us
    pallas_call x1, Pallas kernels, shards(): pl.pallas_call(attention_kernel, out_shape=jax.ShapeDtypeStruct((512, WID...  5.36 us
    pallas_call x1, Pallas kernels, shards(): pl.pallas_call(write_kernel, out_shape=(cache, cache), in_specs=[SM, SM,...  4.21 us
  transfers between devices with their start and end apart: 5, of which 3 were waited for; matrix products, arithmetic and copies ran while one was open for 0% of the time, Pallas kernels for 8%

profile of v3, /device:TPU:8, one launch (start us, length us, event | category | flops | bytes accessed | tf_op | source)
XLA Modules:
  0.0 91.1 jit_solution(6391423673516194472)
XLA Ops:
  0.6 2.9 %project.1 = (bf16[32,16,384]{2,1,0:T(8,128)(2,1)}, f32[24,2,512]{2,1,0:T(2,128)S(1)}) custom-call(s32[24]{0:T(128)} %prior.3, s32[24]{0:T(128)} %accepted.3, bf16[64,384]{1,0:T(8,128)(2,1)} %bitcast.19, f32[1,64]{1,0:T(1,128)} %bitcast.20, bf16[64,128]{1,0:T(8,128)(2,1)} %w_q.1, bf16[64,128]{1,0:T(8,128)(2,1)} %w_k.1, bf16[64,128]{1,0:T(8,128)(2,1)} %w_v.1, ...), custom_call_target="tpu_custom_call" | custom-call | tf_op jit(solution)/shard_map/project/pallas_call | solution.py:471
  3.6 11.3 %all-to-all-start = ((bf16[32,16,384]{2,1,0:T(8,128)(2,1)}), bf16[32,16,384]{2,1,0:T(8,128)(2,1)S(1)}, u32[]{:S(2)}, u32[]{:S(2)}) async-start(bf16[32,16,384]{2,1,0:T(8,128)(2,1)} %get-tuple-element.9.after), calls=%async_computation | async-start | bytes 786432 | tf_op jit(solution)/shard_map/all_to_all | solution.py:496
  14.9 0.1 collective-permute-start
  15.0 1.4 %collective-permute-done.w_1 = bf16[64,128]{1,0:T(8,128)(2,1)S(1)} collective-permute-done((bf16[64,128]{1,0:T(8,128)(2,1)}, bf16[64,128]{1,0:T(8,128)(2,1)S(1)}, u32[]{:S(2)}, u32[]{:S(2)}) %collective-permute-start) | collective-permute-done | bytes 16416 | tf_op jit(solution)/shard_map/ppermute | solution.py:530
  16.4 0.0 copy-start
  16.4 0.7 copy-done
  17.1 0.5 collective-permute-start.1
  17.6 0.0 copy-start.3
  17.6 0.7 copy-done.3
  18.3 0.0 copy-start.2
  18.3 3.5 %copy.20 = (bf16[24,512,128]{2,1,0:T(8,128)(2,1)}, f32[16,128]{1,0:T(8,128)S(1)}) custom-call(bf16[32,16,384]{2,1,0:T(8,128)(2,1)} %get-tuple-element.9.after, s32[16,24]{1,0:T(8,128)S(1)} %bitcast.17, bf16[24,512,128]{2,1,0:T(8,128)(2,1)} %keys_far.1), custom_call_target="tpu_custom_call" | custom-call | flops 2000000000 | bytes 12600000 | tf_op jit(solution)/shard_map/copy/pallas_call | solution.py:498
  21.7 0.0 collective-permute-done.1.after_w.second.w_2
  21.8 8.4 %all-to-all-done.parts = bf16[32,16,384]{2,1,0:T(8,128)(2,1)S(1)} async-done(((bf16[32,16,384]{2,1,0:T(8,128)(2,1)}), bf16[32,16,384]{2,1,0:T(8,128)(2,1)S(1)}, u32[]{:S(2)}, u32[]{:S(2)}) %all-to-all-start) | async-done | bytes 393248 | tf_op jit(solution)/shard_map/all_to_all | solution.py:496
  30.2 0.0 copy-done.2
  30.2 0.7 share.1
  30.9 18.8 %all_to_all.20.joined = bf16[32,16,384]{2,1,0:T(8,128)(2,1)S(1)} all-to-all(bf16[32,16,384]{2,1,0:T(8,128)(2,1)S(1)} %share.1), channel_id=1, replica_groups=mesh['kv_0'=8,'kv_1'=4,'tp'=8] {'kv_0','kv_1'}, dimensions={0} | all-to-all | bytes 786432 | tf_op jit(solution)/shard_map/all_to_all | solution.py:546
  49.7 5.4 %attention.1.after = bf16[512,128]{1,0:T(8,128)(2,1)} custom-call(f32[16,128]{1,0:T(8,128)S(1)} %get-tuple-element.10.after.ancestors, bf16[32,16,384]{2,1,0:T(8,128)(2,1)S(1)} %all_to_all.20.joined, f32[24,2,512]{2,1,0:T(2,128)S(1)} %get-tuple-element.11.biases, bf16[24,512,128]{2,1,0:T(8,128)(2,1)} %keys_far.1, bf16[24,512,128]{2,1,0:T(8,128)(2,1)} %values_in.1), custom_call_target="tpu_custom_call" | custom-call | tf_op jit(solution)/shard_map/attention/pallas_call | solution.py:548
  55.0 7.5 %all-to-all-start.2 = ((bf16[256,2,128]{2,1,0:T(2,128)(2,1)}), bf16[256,2,128]{2,1,0:T(2,128)(2,1)S(1)}, u32[]{:S(2)}, u32[]{:S(2)}) async-start(bf16[256,2,128]{2,1,0:T(2,128)(2,1)} %bitcast.7), calls=%async_computation.2 | async-start | bytes 262144 | tf_op jit(solution)/shard_map/all_to_all | solution.py:567
  62.5 2.2 %collective-permute-start.2 = (bf16[4,64,128]{2,1,0:T(8,128)(2,1)S(1)}, bf16[4,64,128]{2,1,0:T(8,128)(2,1)S(1)}, u32[]{:S(2)}, u32[]{:S(2)}) collective-permute-start(bf16[4,64,128]{2,1,0:T(8,128)(2,1)S(1)} %four.1), channel_id=1, source_target_pairs={{0,4},{1,5},{2,6},{3,7},{4,0},{5,1},{6,2},{7,3},{8,12},{9,13},{10,... | collective-permute-start | bytes 196616 | tf_op jit(solution)/shard_map/ppermute | solution.py:530
  64.7 4.2 %write.1 = (bf16[24,512,128]{2,1,0:T(8,128)(2,1)}, bf16[24,512,128]{2,1,0:T(8,128)(2,1)}) custom-call(s32[24]{0:T(128)} %prior.3, s32[24]{0:T(128)} %accepted.3, bf16[32,16,384]{2,1,0:T(8,128)(2,1)S(1)} %all_to_all.20.joined, bf16[512,128]{1,0:T(8,128)(2,1)} %attention.1.after, ...), custom_call_target="tpu_custom_call", output_to_operand_aliasing={{0}: (4, {})} | custom-call | flops 2000000000 | bytes 100000 | tf_op jit(solution)/shard_map/write/pallas_call | solution.py:569
  68.9 0.0 copy-start.1
  68.9 0.0 collective-permute-done.2.after_w.w_4
  69.0 5.6 %all-to-all-done.2 = bf16[256,2,128]{2,1,0:T(2,128)(2,1)S(1)} async-done(((bf16[256,2,128]{2,1,0:T(2,128)(2,1)}), bf16[256,2,128]{2,1,0:T(2,128)(2,1)S(1)}, u32[]{:S(2)}, u32[]{:S(2)}) %all-to-all-start.2) | async-done | bytes 131104 | tf_op jit(solution)/shard_map/all_to_all | solution.py:567
  74.5 0.4 combine.1
  75.0 15.2 %all_to_all.21 = bf16[32,16,128]{2,1,0:T(8,128)(2,1)S(1)} all-to-all(bf16[32,16,128]{2,1,0:T(8,128)(2,1)S(1)} %combine.1), channel_id=1, replica_groups=mesh['kv_0'=8,'kv_1'=4,'tp'=8] {'kv_0','kv_1'}, dimensions={0} | all-to-all | bytes 262144 | tf_op jit(solution)/shard_map/all_to_all | solution.py:603
  90.2 0.0 copy-done.1
  90.2 0.9 output.1
  (2 shorter events, 0.0 us)
Async XLA Ops:
  3.6 26.6 %all-to-all-start = ((bf16[32,16,384]{2,1,0:T(8,128)(2,1)}), bf16[32,16,384]{2,1,0:T(8,128)(2,1)S(1)}, u32[]{:S(2)}, u32[]{:S(2)}) async-start(bf16[32,16,384]{2,1,0:T(8,128)(2,1)} %get-tuple-element.9.after), calls=%async_computation | async-start | bytes 786432 | tf_op jit(solution)/shard_map/all_to_all | solution.py:496
  14.9 1.5 %collective-permute-start = (bf16[64,128]{1,0:T(8,128)(2,1)}, bf16[64,128]{1,0:T(8,128)(2,1)S(1)}, u32[]{:S(2)}, u32[]{:S(2)}) collective-permute-start(bf16[64,128]{1,0:T(8,128)(2,1)} %bitcast.13), channel_id=1, source_target_pairs={{0,1},{1,0},{2,3},{3,2},{4,5},{5,4},{6,7},{7,6},{8,9},{9,8},{10,11... | collective-permute-start | bytes 49160 | tf_op jit(solution)/shard_map/ppermute | solution.py:530
  16.4 0.7 copy-start
  17.1 4.6 %collective-permute-start.1 = (bf16[2,64,128]{2,1,0:T(8,128)(2,1)S(1)}, bf16[2,64,128]{2,1,0:T(8,128)(2,1)S(1)}, u32[]{:S(2)}, u32[]{:S(2)}) collective-permute-start(bf16[2,64,128]{2,1,0:T(8,128)(2,1)S(1)} %pair.1.first), channel_id=1, source_target_pairs={{0,2},{1,3},{2,0},{3,1},{4,6},{5,7},{6,4},{7,5},{8,10},{9,11},{10,... | collective-permute-start | bytes 98312 | tf_op jit(solution)/shard_map/ppermute | solution.py:530
  17.6 0.7 copy-start.3
  18.3 11.9 %copy-start.2 = (f32[16]{0:T(128)S(1)}, f32[16]{0:T(128)}, u32[]{:S(2)}) copy-start(f32[16]{0:T(128)} %bias.1) | copy-start | bytes 196
  55.0 19.5 %all-to-all-start.2 = ((bf16[256,2,128]{2,1,0:T(2,128)(2,1)}), bf16[256,2,128]{2,1,0:T(2,128)(2,1)S(1)}, u32[]{:S(2)}, u32[]{:S(2)}) async-start(bf16[256,2,128]{2,1,0:T(2,128)(2,1)} %bitcast.7), calls=%async_computation.2 | async-start | bytes 262144 | tf_op jit(solution)/shard_map/all_to_all | solution.py:567
  62.5 6.4 %collective-permute-start.2 = (bf16[4,64,128]{2,1,0:T(8,128)(2,1)S(1)}, bf16[4,64,128]{2,1,0:T(8,128)(2,1)S(1)}, u32[]{:S(2)}, u32[]{:S(2)}) collective-permute-start(bf16[4,64,128]{2,1,0:T(8,128)(2,1)S(1)} %four.1), channel_id=1, source_target_pairs={{0,4},{1,5},{2,6},{3,7},{4,0},{5,1},{6,2},{7,3},{8,12},{9,13},{10,... | collective-permute-start | bytes 196616 | tf_op jit(solution)/shard_map/ppermute | solution.py:530
  68.9 21.3 %copy-start.1 = (bf16[128,64]{0,1:T(8,128)(2,1)S(1)}, bf16[128,64]{0,1:T(8,128)(2,1)}, u32[]{:S(2)}) copy-start(bf16[128,64]{0,1:T(8,128)(2,1)} %param.21) | copy-start | bytes 49156

commit v4 on v3

--- a/solution.py
+++ b/solution.py
@@ -44,12 +44,10 @@
 
 
 def project_kernel(
-    prior, accepted, tokens, gain, w_q, w_k, w_v, w_gate, cum, out, bias, gate_rows, gates, sem
+    prior, accepted, tokens, gain, w_q, w_k, w_v, w_gate, cum, out, bias, gates
 ):
     kv, tp = lax.axis_index(KV), lax.axis_index("tp")
     columns = pl.ds(pl.multiple_of(lax.div(kv, 2) * WIDTH, WIDTH), WIDTH)
-    copy = pltpu.make_async_copy(w_gate.at[:, columns], gate_rows, sem)
-    copy.start()
     floats = tokens[...].astype(f32)
     same = iota((64, 64), 0) == iota((64, 64), 1)
     gain_column = jnp.sum(jnp.where(same, gain[...], 0.0), axis=1, keepdims=True)
@@ -80,8 +78,7 @@
     both = jnp.concatenate(
         [jnp.where(odd == 0, scaled, zero), jnp.where(odd == 1, scaled, zero)], axis=0
     )
-    copy.wait()
-    gates[...] = jnp.dot(gate_rows[...], both, preferred_element_type=f32)
+    gates[...] = jnp.dot(w_gate[:, columns], both, preferred_element_type=f32)
     row = iota((8, ROWS), 0)
     gate_0 = gates[pl.ds(2 * tp, 1), :]
     gate_1 = gates[pl.ds(2 * tp + 1, 1), :]
@@ -169,40 +166,9 @@
         return high + low
 
     own = jnp.minimum(kv, SEQS - 1)
-    mine = pl.ds(pl.multiple_of(PROPS * own, PROPS), PROPS)
-    pad = jnp.zeros((WIDTH - PROPS, WIDTH), f32)
-    picks = (iota((ROWS, WIDTH), 0) == iota((ROWS, WIDTH), 1) + PROPS * own) & (
-        iota((ROWS, WIDTH), 1) < PROPS
-    )
-    own_gates = jnp.dot(
-        joined[STATS], jnp.where(picks, 1.0, 0.0).astype(bf16), preferred_element_type=f32
-    ).astype(bf16)
-    reached = ancestors[...]
-    tree = dot_t(own_gates, jnp.concatenate([reached, pad], axis=0).astype(bf16))
-    tree = tree[0:8] + tree[8:16]
-    last = jnp.sum(
-        jnp.where(iota((8, WIDTH), 1) == own, stats[:, 0:WIDTH], 0.0), axis=1, keepdims=True
-    )
-    tree_bias = jnp.concatenate(
-        [
-            jnp.broadcast_to(-(last[3:4] + last[5:6] + tree[0:1]), (PROPS, WIDTH)),
-            jnp.broadcast_to(-(last[4:5] + last[6:7] + tree[1:2]), (PROPS, WIDTH)),
-        ],
-        axis=0,
-    )
-    own_inv = columns[mine, 2:3]
-    new_keys = own_inv * joined[own, :, WIDTH : 2 * WIDTH].astype(f32)
-    new_values = own_inv * joined[own, :, 2 * WIDTH : 3 * WIDTH].astype(f32)
-    new_keys = jnp.concatenate([new_keys, pad], axis=0).astype(bf16)
-    new_values = jnp.concatenate([new_values, pad], axis=0).astype(bf16)
-    needed = jnp.where(kv < SEQS, 0.5, 2.0)
-    live = jnp.concatenate([reached, reached], axis=0) > needed
-    tree_scores = jnp.where(live, dot_t(both_heads(mine, own), new_keys) + tree_bias, masked_score)
-    tree_top = jnp.max(tree_scores, axis=1, keepdims=True)
-
-    for b in range(SEQS):
-        if b % 3 == 0:
-            moves[b // 3].wait()
+    low = lane_out < HEAD
+
+    def score(b):
         q = both_heads(pl.ds(PROPS * b, PROPS), b)
         bias = biases[b]
         bias = jnp.concatenate(
@@ -213,31 +179,19 @@
             axis=0,
         )
         scores_buf[b] = dot_t(q, keys[b]) + bias
-    for b in range(SEQS):
+
+    def weigh(b):
         scores = scores_buf[b]
         top = sendable(jnp.max(scores, axis=1, keepdims=True))
         weights = jnp.exp(scores - top)
         total = jnp.sum(weights, axis=1, keepdims=True)
         weights_buf[b] = weights.astype(bf16)
         stat_buf[b] = coded_stats(b % 3, top, total)
-    for t in range(N_TP):
-        moves[N_TP + t].wait()
-    for b in range(SEQS):
+
+    def gather(b):
         v_buf[b] = jnp.dot(weights_buf[b], values[b], preferred_element_type=f32)
 
-    scores = scores_buf[own]
-    top = jnp.maximum(jnp.max(scores, axis=1, keepdims=True), tree_top)
-    top = sendable(top)
-    weights = jnp.exp(scores - top)
-    tree_weights = jnp.exp(tree_scores - top)
-    total = jnp.sum(weights, axis=1, keepdims=True) + jnp.sum(tree_weights, axis=1, keepdims=True)
-    stat_buf[own] = coded_stats(lax.rem(own, 3), top, total)
-    v_buf[own] = jnp.dot(
-        weights.astype(bf16), values[own], preferred_element_type=f32
-    ) + jnp.dot(tree_weights.astype(bf16), new_values, preferred_element_type=f32)
-
-    low = lane_out < HEAD
-    for t in range(N_TP):
+    def pack(t):
         v = [v_buf[3 * t + s] for s in range(3)]
         turned = [pltpu.roll(x, HEAD, 1) for x in v]
         first = jnp.where(first_row, v[0], turned[0])
@@ -246,10 +200,75 @@
         stats = stat_buf[3 * t] + stat_buf[3 * t + 1] + stat_buf[3 * t + 2]
         mixed[pl.ds(2 * t, N_KV, stride=16), :] = jnp.where(low, first, second)
         mixed[pl.ds(2 * t + 1, N_KV, stride=16), :] = jnp.where(low, third, stats)
+
+    def tree():
+        mine = pl.ds(pl.multiple_of(PROPS * own, PROPS), PROPS)
+        pad = jnp.zeros((WIDTH - PROPS, WIDTH), f32)
+        picks = (iota((ROWS, WIDTH), 0) == iota((ROWS, WIDTH), 1) + PROPS * own) & (
+            iota((ROWS, WIDTH), 1) < PROPS
+        )
+        own_gates = jnp.dot(
+            joined[STATS], jnp.where(picks, 1.0, 0.0).astype(bf16), preferred_element_type=f32
+        ).astype(bf16)
+        reached = ancestors[...]
+        tree = dot_t(own_gates, jnp.concatenate([reached, pad], axis=0).astype(bf16))
+        tree = tree[0:8] + tree[8:16]
+        last = jnp.sum(
+            jnp.where(iota((8, WIDTH), 1) == own, stats[:, 0:WIDTH], 0.0), axis=1, keepdims=True
+        )
+        tree_bias = jnp.concatenate(
+            [
+                jnp.broadcast_to(-(last[3:4] + last[5:6] + tree[0:1]), (PROPS, WIDTH)),
+                jnp.broadcast_to(-(last[4:5] + last[6:7] + tree[1:2]), (PROPS, WIDTH)),
+            ],
+            axis=0,
+        )
+        own_inv = columns[mine, 2:3]
+        new_keys = own_inv * joined[own, :, WIDTH : 2 * WIDTH].astype(f32)
+        new_values = own_inv * joined[own, :, 2 * WIDTH : 3 * WIDTH].astype(f32)
+        new_keys = jnp.concatenate([new_keys, pad], axis=0).astype(bf16)
+        new_values = jnp.concatenate([new_values, pad], axis=0).astype(bf16)
+        needed = jnp.where(kv < SEQS, 0.5, 2.0)
+        live = jnp.concatenate([reached, reached], axis=0) > needed
+        tree_scores = jnp.where(live, dot_t(both_heads(mine, own), new_keys) + tree_bias, masked_score)
+        tree_top = jnp.max(tree_scores, axis=1, keepdims=True)
+        return tree_scores, tree_top, new_values
+
+    for step in range(N_TP + 2):
+        if step < N_TP:
+            moves[step].wait()
+        if step >= 2:
+            moves[N_TP + step - 2].wait()
+        for s in range(3):
+            if step < N_TP:
+                score(3 * step + s)
+            if 1 <= step <= N_TP:
+                weigh(3 * step - 3 + s)
+            if step >= 2:
+                gather(3 * step - 6 + s)
+        if step == 3:
+            tree_scores, tree_top, new_values = tree()
+        if step == N_TP:
+            scores = scores_buf[own]
+            top = jnp.maximum(jnp.max(scores, axis=1, keepdims=True), tree_top)
+            top = sendable(top)
+            own_weights = jnp.exp(scores - top)
+            tree_weights = jnp.exp(tree_scores - top)
+            own_total = jnp.sum(own_weights, axis=1, keepdims=True) + jnp.sum(
+                tree_weights, axis=1, keepdims=True
+            )
+            own_stats = coded_stats(lax.rem(own, 3), top, own_total)
+    own_v = jnp.dot(
+        own_weights.astype(bf16), values[own], preferred_element_type=f32
+    ) + jnp.dot(tree_weights.astype(bf16), new_values, preferred_element_type=f32)
+    stat_buf[own] = own_stats
+    v_buf[own] = own_v
+    for t in range(N_TP):
+        pack(t)
     out[...] = mixed[...].astype(bf16)
 
 
-def combine_kernel(parts, after_w, after, out, tops, sums):
+def combine_kernel(parts, out, tops, sums):
     row = iota((WIDTH, 4 * WIDTH), 0) - HEAD
     column = iota((WIDTH, 4 * WIDTH), 1)
     unit = jnp.where(column < 2 * WIDTH, lax.rem(lax.div(column, HEAD), 2), 2)
@@ -474,13 +493,9 @@
             jax.ShapeDtypeStruct((N_KV, PROPS, ROWS), bf16),
             pltpu.VMEM(cum_gates.shape, f32),
         ),
-        in_specs=[SM, SM, VM, VM, VM, VM, VM, ANY, VM],
+        in_specs=[SM, SM, VM, VM, VM, VM, VM, VM, VM],
         out_specs=(VM, VM),
-        scratch_shapes=[
-            pltpu.VMEM((16, WIDTH), bf16),
-            pltpu.VMEM((16, ROWS), f32),
-            pltpu.SemaphoreType.DMA,
-        ],
+        scratch_shapes=[pltpu.VMEM((16, ROWS), f32)],
         name="project",
     )(
         prior_len,
@@ -512,7 +527,7 @@
             flops=2_000_000_000, bytes_accessed=12_600_000, transcendentals=0
         ),
         name="copy",
-    )(*far(parts), parents.T, *far(keys_cache))
+    )(*far(parts, parents.T, keys_cache))
 
     tp_count = lax.axis_size("tp")
 
@@ -524,16 +539,16 @@
             out_specs=VM,
             compiler_params=limit(2),
             name=name,
-        )(*near(*pieces))
+        )(*pieces)
 
     def across(x, bit):
         return lax.ppermute(x, "tp", [(i, i ^ bit) for i in range(tp_count)])
 
     w_0 = w_out.T
     w_1 = across(w_0, 1)
-    w_pair = gathered("pair", w_0[None], w_1[None])
+    w_pair = gathered("pair", *far(w_0[None]), *near(w_1[None]))
     w_2 = across(w_pair, 2)
-    w_4 = across(gathered("four", w_pair, w_2), 4)
+    w_4 = across(gathered("four", *near(w_pair, w_2)), 4)
 
     block = pl.pallas_call(
         share_kernel,
@@ -542,12 +557,12 @@
         out_specs=VM,
         compiler_params=limit(8),
         name="share",
-    )(gate_bias, *near(arrived, ancestors, w_2))
+    )(gate_bias, *near(arrived, ancestors, w_4))
     joined = lax.all_to_all(block, KV, 0, 0, tiled=True)
 
     sent = pl.pallas_call(
         attention_kernel,
-        out_shape=jax.ShapeDtypeStruct((512, WIDTH), bf16),
+        out_shape=pltpu.VMEM((512, WIDTH), bf16),
         in_specs=[VM, VM, VM, ANY, ANY],
         out_specs=VM,
         scratch_shapes=[
@@ -565,6 +580,17 @@
         name="attention",
     )(*near(ancestors, joined, biases), *far(keys_cache, values_cache))
     pieces = lax.all_to_all(sent.reshape(256, 2, WIDTH), (*KV, "tp"), 0, 0, tiled=True)
+
+    combined = pl.pallas_call(
+        combine_kernel,
+        out_shape=jax.ShapeDtypeStruct((N_KV, PROPS, WIDTH), bf16),
+        in_specs=[VM],
+        out_specs=VM,
+        scratch_shapes=[pltpu.VMEM((64, 8, WIDTH), f32), pltpu.VMEM((64, 8, WIDTH), f32)],
+        compiler_params=limit(8),
+        name="combine",
+    )(*near(pieces.reshape(512, WIDTH)))
+    shared = lax.all_to_all(combined, KV, 0, 0, tiled=True)
 
     keys_out, values_out = pl.pallas_call(
         write_kernel,
@@ -588,19 +614,8 @@
     )(
         *far(prior_len, accepted),
         *near(joined),
-        *far(sent, keys_copy, values_cache),
+        *far(combined, keys_copy, values_cache),
     )
-
-    combined = pl.pallas_call(
-        combine_kernel,
-        out_shape=pltpu.VMEM((N_KV, PROPS, WIDTH), bf16),
-        in_specs=[VM, VM, ANY],
-        out_specs=VM,
-        scratch_shapes=[pltpu.VMEM((64, 8, WIDTH), f32), pltpu.VMEM((64, 8, WIDTH), f32)],
-        compiler_params=limit(8),
-        name="combine",
-    )(*near(pieces.reshape(512, WIDTH), w_4), *far(keys_out))
-    shared = lax.all_to_all(combined, KV, 0, 0, tiled=True)
 
     mixed_rows = pl.pallas_call(
         output_kernel,

time: 92 us -> 92.6 us (level)
  blocking collectives: 34 us -> 39.3 us
  starting transfers between devices: 21.5 us -> 18 us
  local copies, waits for them, and re-layouts: 1.42 us -> 0.01 us
    all_to_all x1, waiting for transfers between devices: 8.44 us -> 3.12 us  [shards(): arrived = lax.all_to_all(parts, KV, 0, 0, tiled=True)]
    all_to_all x1, starting transfers between devices: 7.46 us -> 3.84 us  [shards(): shared = lax.all_to_all(combined, KV, 0, 0, tiled=True)]
    ppermute x3, waiting for transfers between devices: 1.38 us -> 4.85 us  [across(): return lax.ppermute(x, 'tp', [(i, i ^ bit) for i in range(tp_count)])]
    all_to_all x1, blocking collectives: 15.2 us -> 18.3 us  [shards(): lax.all_to_all(sent.reshape(256, 2, WIDTH), (*KV, 'tp'), 0, 0, tiled=True)]
    all_to_all x1, blocking collectives: 18.8 us -> 21 us  [shards(): joined = lax.all_to_all(block, KV, 0, 0, tiled=True)]
    unnamed x8 -> x4, local copies, waits for them, and re-layouts: 1.42 us -> 0.01 us
    all_to_all x1, waiting for transfers between devices: 5.6 us -> 6.66 us  [shards(): shared = lax.all_to_all(combined, KV, 0, 0, tiled=True)]
  transfers between devices with their start and end apart: 5 -> 5, of which waited for: 3 -> 4; matrix products, arithmetic and copies ran while one was open for 0% -> 0% of each run, Pallas kernels for 8% -> 10%
where the time goes in v4:
time: 92.6 us; the launch traced here: 91.4 us
  blocking collectives  39.3 us (42%)
  Pallas kernels  18.8 us (20%)
  starting transfers between devices  18 us (19%)
  waiting for transfers between devices  14.6 us (16%)
    all_to_all x1, blocking collectives, shards(): joined = lax.all_to_all(block, KV, 0, 0, tiled=True)  21 us
    all_to_all x1, blocking collectives, shards(): lax.all_to_all(sent.reshape(256, 2, WIDTH), (*KV, 'tp'), 0, 0, tiled=True)  18.3 us
    all_to_all x1, starting transfers between devices, shards(): arrived = lax.all_to_all(parts, KV, 0, 0, tiled=True)  11.3 us
    all_to_all x1, waiting for transfers between devices, shards(): shared = lax.all_to_all(combined, KV, 0, 0, tiled=True)  6.66 us
    pallas_call x1, Pallas kernels, shards(): pl.pallas_call(attention_kernel, out_shape=pltpu.VMEM((512, WIDTH), bf16)...  5.14 us
    ppermute x3, waiting for transfers between devices, across(): return lax.ppermute(x, 'tp', [(i, i ^ bit) for i in range(tp_count)])  4.85 us
    pallas_call x1, Pallas kernels, shards(): pl.pallas_call(write_kernel, out_shape=(cache, cache), in_specs=[SM, SM,...  4.34 us
    all_to_all x1, starting transfers between devices, shards(): shared = lax.all_to_all(combined, KV, 0, 0, tiled=True)  3.84 us
  transfers between devices with their start and end apart: 5, of which 4 were waited for; matrix products, arithmetic and copies ran while one was open for 0% of the time, Pallas kernels for 10%

profile of v4, /device:TPU:8, one launch (start us, length us, event | category | flops | bytes accessed | tf_op | source)
XLA Modules:
  0.0 91.4 jit_solution(16117107431974785654)
XLA Ops:
  0.6 2.2 %project.1 = (bf16[32,16,384]{2,1,0:T(8,128)(2,1)}, f32[24,2,512]{2,1,0:T(2,128)S(1)}) custom-call(s32[24]{0:T(128)} %prior.3, s32[24]{0:T(128)} %accepted.3, bf16[64,384]{1,0:T(8,128)(2,1)} %bitcast.19, f32[1,64]{1,0:T(1,128)} %bitcast.20, bf16[64,128]{1,0:T(8,128)(2,1)} %w_q.1, bf16[64,128]{1,0:T(8,128)(2,1)} %w_k.1, bf16[64,128]{1,0:T(8,128)(2,1)} %w_v.1, ...), custom_call_target="tpu_custom_call" | custom-call | tf_op jit(solution)/shard_map/project/pallas_call | solution.py:490
  2.9 11.3 %all-to-all-start = ((bf16[32,16,384]{2,1,0:T(8,128)(2,1)}), bf16[32,16,384]{2,1,0:T(8,128)(2,1)S(1)}, u32[]{:S(2)}, u32[]{:S(2)}) async-start(bf16[32,16,384]{2,1,0:T(8,128)(2,1)} %get-tuple-element.9.after), calls=%async_computation | async-start | bytes 786432 | tf_op jit(solution)/shard_map/all_to_all | solution.py:511
  14.2 0.1 collective-permute-start
  14.3 1.4 %collective-permute-done.w_1 = bf16[64,128]{1,0:T(8,128)(2,1)S(1)} collective-permute-done((bf16[64,128]{1,0:T(8,128)(2,1)}, bf16[64,128]{1,0:T(8,128)(2,1)S(1)}, u32[]{:S(2)}, u32[]{:S(2)}) %collective-permute-start) | collective-permute-done | bytes 16416 | tf_op jit(solution)/shard_map/ppermute | solution.py:545
  15.7 0.7 pair.1.first
  16.4 0.4 collective-permute-start.1
  16.8 3.5 %collective-permute-done.1.second.w_2 = bf16[2,64,128]{2,1,0:T(8,128)(2,1)S(1)} collective-permute-done((bf16[2,64,128]{2,1,0:T(8,128)(2,1)S(1)}, bf16[2,64,128]{2,1,0:T(8,128)(2,1)S(1)}, u32[]{:S(2)}, u32[]{:S(2)}) %collective-permute-start.1) | collective-permute-done | bytes 32800 | tf_op jit(solution)/shard_map/ppermute | solution.py:545
  20.3 2.3 %collective-permute-start.2 = (bf16[4,64,128]{2,1,0:T(8,128)(2,1)S(1)}, bf16[4,64,128]{2,1,0:T(8,128)(2,1)S(1)}, u32[]{:S(2)}, u32[]{:S(2)}) collective-permute-start(bf16[4,64,128]{2,1,0:T(8,128)(2,1)S(1)} %four.1), channel_id=1, source_target_pairs={{0,4},{1,5},{2,6},{3,7},{4,0},{5,1},{6,2},{7,3},{8,12},{9,13},{10,... | collective-permute-start | bytes 196616 | tf_op jit(solution)/shard_map/ppermute | solution.py:545
  22.6 0.0 copy-start.1
  22.6 3.7 %copy.20 = (bf16[24,512,128]{2,1,0:T(8,128)(2,1)}, f32[16,128]{1,0:T(8,128)S(1)}) custom-call(bf16[32,16,384]{2,1,0:T(8,128)(2,1)} %get-tuple-element.9.after, s32[16,24]{1,0:T(8,128)} %bitcast.21, bf16[24,512,128]{2,1,0:T(8,128)(2,1)} %keys_far.1), custom_call_target="tpu_custom_call" | custom-call | flops 2000000000 | bytes 12600000 | tf_op jit(solution)/shard_map/copy/pallas_call | solution.py:513
  26.3 0.0 collective-permute-done.2.after_w.w_4
  26.3 3.1 %all-to-all-done.parts = bf16[32,16,384]{2,1,0:T(8,128)(2,1)S(1)} async-done(((bf16[32,16,384]{2,1,0:T(8,128)(2,1)}), bf16[32,16,384]{2,1,0:T(8,128)(2,1)S(1)}, u32[]{:S(2)}, u32[]{:S(2)}) %all-to-all-start) | async-done | bytes 393248 | tf_op jit(solution)/shard_map/all_to_all | solution.py:511
  29.5 0.0 copy-done.1
  29.5 0.7 share.1
  30.1 21.0 %all_to_all.20.joined = bf16[32,16,384]{2,1,0:T(8,128)(2,1)S(1)} all-to-all(bf16[32,16,384]{2,1,0:T(8,128)(2,1)S(1)} %share.1), channel_id=1, replica_groups=mesh['kv_0'=8,'kv_1'=4,'tp'=8] {'kv_0','kv_1'}, dimensions={0} | all-to-all | bytes 786432 | tf_op jit(solution)/shard_map/all_to_all | solution.py:561
  51.1 5.1 %attention.1 = bf16[512,128]{1,0:T(8,128)(2,1)S(1)} custom-call(f32[16,128]{1,0:T(8,128)S(1)} %get-tuple-element.10.after.ancestors, bf16[32,16,384]{2,1,0:T(8,128)(2,1)S(1)} %all_to_all.20.joined, f32[24,2,512]{2,1,0:T(2,128)S(1)} %get-tuple-element.11.biases, bf16[24,512,128]{2,1,0:T(8,128)(2,1)} %keys_far.1, bf16[24,512,128]{2,1,0:T(8,128)(2,1)} %values_in.1), custom_call_target="tpu_custom_call" | custom-call | tf_op jit(solution)/shard_map/attention/pallas_call | solution.py:563
  56.2 18.3 %all_to_all.21 = bf16[256,2,128]{2,1,0:T(2,128)(2,1)S(1)} all-to-all(bf16[256,2,128]{2,1,0:T(2,128)(2,1)S(1)} %bitcast.13), channel_id=1, replica_groups=mesh['kv_0'=8,'kv_1'=4,'tp'=8] {'kv_0','kv_1','tp'}, dimensions={0} | all-to-all | bytes 262144 | tf_op jit(solution)/shard_map/all_to_all | solution.py:582
  74.5 1.1 %combine.1.after = bf16[32,16,128]{2,1,0:T(8,128)(2,1)} custom-call(bf16[512,128]{1,0:T(8,128)(2,1)S(1)} %bitcast.12), custom_call_target="tpu_custom_call" | custom-call | tf_op jit(solution)/shard_map/combine/pallas_call | solution.py:584
  75.6 3.8 %all-to-all-start.3 = ((bf16[32,16,128]{2,1,0:T(8,128)(2,1)}), bf16[32,16,128]{2,1,0:T(8,128)(2,1)S(1)}, u32[]{:S(2)}, u32[]{:S(2)}) async-start(bf16[32,16,128]{2,1,0:T(8,128)(2,1)} %combine.1.after), calls=%async_computation.3 | async-start | bytes 262144 | tf_op jit(solution)/shard_map/all_to_all | solution.py:593
  79.5 0.0 copy-start
  79.5 4.3 %write.1 = (bf16[24,512,128]{2,1,0:T(8,128)(2,1)}, bf16[24,512,128]{2,1,0:T(8,128)(2,1)}) custom-call(s32[24]{0:T(128)} %prior.3, s32[24]{0:T(128)} %accepted.3, bf16[32,16,384]{2,1,0:T(8,128)(2,1)S(1)} %all_to_all.20.joined, bf16[32,16,128]{2,1,0:T(8,128)(2,1)} %combine.1.after, ...), custom_call_target="tpu_custom_call", output_to_operand_aliasing={{0}: (4, {})} | custom-call | flops 2000000000 | bytes 100000 | tf_op jit(solution)/shard_map/write/pallas_call | solution.py:595
  83.8 6.7 %all-to-all-done.3 = bf16[32,16,128]{2,1,0:T(8,128)(2,1)S(1)} async-done(((bf16[32,16,128]{2,1,0:T(8,128)(2,1)}), bf16[32,16,128]{2,1,0:T(8,128)(2,1)S(1)}, u32[]{:S(2)}, u32[]{:S(2)}) %all-to-all-start.3) | async-done | bytes 131104 | tf_op jit(solution)/shard_map/all_to_all | solution.py:593
  90.5 0.0 copy-done
  90.5 0.9 output.1
  (1 shorter events, 0.0 us)
Async XLA Ops:
  2.9 26.6 %all-to-all-start = ((bf16[32,16,384]{2,1,0:T(8,128)(2,1)}), bf16[32,16,384]{2,1,0:T(8,128)(2,1)S(1)}, u32[]{:S(2)}, u32[]{:S(2)}) async-start(bf16[32,16,384]{2,1,0:T(8,128)(2,1)} %get-tuple-element.9.after), calls=%async_computation | async-start | bytes 786432 | tf_op jit(solution)/shard_map/all_to_all | solution.py:511
  14.2 1.5 %collective-permute-start = (bf16[64,128]{1,0:T(8,128)(2,1)}, bf16[64,128]{1,0:T(8,128)(2,1)S(1)}, u32[]{:S(2)}, u32[]{:S(2)}) collective-permute-start(bf16[64,128]{1,0:T(8,128)(2,1)} %bitcast.14), channel_id=1, source_target_pairs={{0,1},{1,0},{2,3},{3,2},{4,5},{5,4},{6,7},{7,6},{8,9},{9,8},{10,11... | collective-permute-start | bytes 49160 | tf_op jit(solution)/shard_map/ppermute | solution.py:545
  16.4 3.9 %collective-permute-start.1 = (bf16[2,64,128]{2,1,0:T(8,128)(2,1)S(1)}, bf16[2,64,128]{2,1,0:T(8,128)(2,1)S(1)}, u32[]{:S(2)}, u32[]{:S(2)}) collective-permute-start(bf16[2,64,128]{2,1,0:T(8,128)(2,1)S(1)} %pair.1.first), channel_id=1, source_target_pairs={{0,2},{1,3},{2,0},{3,1},{4,6},{5,7},{6,4},{7,5},{8,10},{9,11},{10,... | collective-permute-start | bytes 98312 | tf_op jit(solution)/shard_map/ppermute | solution.py:545
  20.3 6.0 %collective-permute-start.2 = (bf16[4,64,128]{2,1,0:T(8,128)(2,1)S(1)}, bf16[4,64,128]{2,1,0:T(8,128)(2,1)S(1)}, u32[]{:S(2)}, u32[]{:S(2)}) collective-permute-start(bf16[4,64,128]{2,1,0:T(8,128)(2,1)S(1)} %four.1), channel_id=1, source_target_pairs={{0,4},{1,5},{2,6},{3,7},{4,0},{5,1},{6,2},{7,3},{8,12},{9,13},{10,... | collective-permute-start | bytes 196616 | tf_op jit(solution)/shard_map/ppermute | solution.py:545
  22.6 6.9 %copy-start.1 = (f32[16]{0:T(128)S(1)}, f32[16]{0:T(128)}, u32[]{:S(2)}) copy-start(f32[16]{0:T(128)} %bias.1) | copy-start | bytes 196
  75.6 14.9 %all-to-all-start.3 = ((bf16[32,16,128]{2,1,0:T(8,128)(2,1)}), bf16[32,16,128]{2,1,0:T(8,128)(2,1)S(1)}, u32[]{:S(2)}, u32[]{:S(2)}) async-start(bf16[32,16,128]{2,1,0:T(8,128)(2,1)} %combine.1.after), calls=%async_computation.3 | async-start | bytes 262144 | tf_op jit(solution)/shard_map/all_to_all | solution.py:593
  79.5 11.0 %copy-start = (bf16[128,64]{0,1:T(8,128)(2,1)S(1)}, bf16[128,64]{0,1:T(8,128)(2,1)}, u32[]{:S(2)}) copy-start(bf16[128,64]{0,1:T(8,128)(2,1)} %param.21) | copy-start | bytes 49156

commit v5 on v4

--- a/solution.py
+++ b/solution.py
@@ -93,7 +93,7 @@
     out[STATS + 1 :] = jnp.zeros((N_KV - STATS - 1, PROPS, ROWS), bf16)
 
 
-def share_kernel(bias, parts, after, after_w, out):
+def share_kernel(bias, parts, out):
     kv, tp = lax.axis_index(KV), lax.axis_index("tp")
     total = jnp.zeros((PROPS, ROWS), f32)
     for k in range(N_KV):
@@ -111,17 +111,17 @@
 
 
 def attention_kernel(
-    ancestors,
+    parents,
     joined,
     biases,
-    keys_far,
-    values_far,
+    keys,
+    values,
     out,
+    keys_out,
+    values_out,
     columns,
     scores_buf,
     weights_buf,
-    keys,
-    values,
     v_buf,
     stat_buf,
     mixed,
@@ -129,12 +129,10 @@
 ):
     kv = lax.axis_index(KV)
     moves = []
-    for n, (source, target) in enumerate(((keys_far, keys), (values_far, values))):
-        for t in range(N_TP):
-            three = pl.ds(3 * t, 3)
-            moves.append(
-                pltpu.make_async_copy(source.at[three], target.at[three], sems.at[n, t])
-            )
+    for n, (source, target) in enumerate(((keys, keys_out), (values, values_out))):
+        for t in range(4):
+            six = pl.ds(6 * t, 6)
+            moves.append(pltpu.make_async_copy(source.at[six], target.at[six], sems.at[n, t]))
     for move in moves:
         move.start()
     coded = joined[STATS].astype(f32)
@@ -201,7 +199,19 @@
         mixed[pl.ds(2 * t, N_KV, stride=16), :] = jnp.where(low, first, second)
         mixed[pl.ds(2 * t + 1, N_KV, stride=16), :] = jnp.where(low, third, stats)
 
-    def tree():
+    def lineage():
+        row = iota((PROPS, WIDTH), 0)
+        linked = jnp.where(lane == row, 1.0, 0.0)
+        for i in range(PROPS):
+            linked = jnp.where((row == i) & (lane == parents[i, own]), 1.0, linked)
+        return linked
+
+    def squared(linked):
+        other = jnp.concatenate([linked, jnp.zeros((WIDTH - PROPS, WIDTH), f32)], axis=0)
+        product = jnp.dot(linked.astype(bf16), other.astype(bf16), preferred_element_type=f32)
+        return jnp.minimum(product, 1.0)
+
+    def tree(reached):
         mine = pl.ds(pl.multiple_of(PROPS * own, PROPS), PROPS)
         pad = jnp.zeros((WIDTH - PROPS, WIDTH), f32)
         picks = (iota((ROWS, WIDTH), 0) == iota((ROWS, WIDTH), 1) + PROPS * own) & (
@@ -210,7 +220,6 @@
         own_gates = jnp.dot(
             joined[STATS], jnp.where(picks, 1.0, 0.0).astype(bf16), preferred_element_type=f32
         ).astype(bf16)
-        reached = ancestors[...]
         tree = dot_t(own_gates, jnp.concatenate([reached, pad], axis=0).astype(bf16))
         tree = tree[0:8] + tree[8:16]
         last = jnp.sum(
@@ -235,10 +244,6 @@
         return tree_scores, tree_top, new_values
 
     for step in range(N_TP + 2):
-        if step < N_TP:
-            moves[step].wait()
-        if step >= 2:
-            moves[N_TP + step - 2].wait()
         for s in range(3):
             if step < N_TP:
                 score(3 * step + s)
@@ -246,8 +251,12 @@
                 weigh(3 * step - 3 + s)
             if step >= 2:
                 gather(3 * step - 6 + s)
-        if step == 3:
-            tree_scores, tree_top, new_values = tree()
+        if step == 0:
+            reached = lineage()
+        if 1 <= step <= 4:
+            reached = squared(reached)
+        if step == 5:
+            tree_scores, tree_top, new_values = tree(reached)
         if step == N_TP:
             scores = scores_buf[own]
             top = jnp.maximum(jnp.max(scores, axis=1, keepdims=True), tree_top)
@@ -266,9 +275,11 @@
     for t in range(N_TP):
         pack(t)
     out[...] = mixed[...].astype(bf16)
-
-
-def combine_kernel(parts, out, tops, sums):
+    for move in moves:
+        move.wait()
+
+
+def combine_kernel(parts, after_w, out, tops, sums):
     row = iota((WIDTH, 4 * WIDTH), 0) - HEAD
     column = iota((WIDTH, 4 * WIDTH), 1)
     unit = jnp.where(column < 2 * WIDTH, lax.rem(lax.div(column, HEAD), 2), 2)
@@ -334,62 +345,12 @@
     out[count:] = second[...]
 
 
-def copy_kernel(after, parents, keys, keys_out, ancestors, keys_near, sems):
-    moves = []
-    for t in range(8):
-        three = pl.ds(3 * t, 3)
-        moves.append(
-            (
-                pltpu.make_async_copy(keys.at[three], keys_near.at[three], sems.at[0, t]),
-                pltpu.make_async_copy(keys_near.at[three], keys_out.at[three], sems.at[1, t]),
-            )
-        )
-    for move in moves:
-        move[0].start()
-    own = jnp.minimum(lax.axis_index(KV), SEQS - 1)
-    row = iota((PROPS, WIDTH), 0)
-    lane = iota((PROPS, WIDTH), 1)
-    reached = jnp.where(lane == row, 1.0, 0.0)
-    for i in range(PROPS):
-        reached = jnp.where((row == i) & (lane == parents[i, own]), 1.0, reached)
-    pad = jnp.zeros((WIDTH - PROPS, WIDTH), f32)
-    for _ in range(4):
-        other = jnp.concatenate([reached, pad], axis=0).astype(bf16)
-        reached = jnp.minimum(jnp.dot(reached.astype(bf16), other, preferred_element_type=f32), 1.0)
-    ancestors[...] = reached
-    for move in moves:
-        move[0].wait()
-        move[1].start()
-    for move in moves:
-        move[1].wait()
-
-
 def write_kernel(
-    prior,
-    accepted,
-    joined,
-    after,
-    keys_in,
-    values_in,
-    keys,
-    values,
-    buf,
-    near,
-    columns,
-    in_sem,
-    out_sem,
-    near_sem,
+    prior, accepted, joined, after, keys_in, values_in, keys, values, buf, columns, in_sem, out_sem
 ):
-    moves = []
-    for t in range(8):
-        three = pl.ds(3 * t, 3)
-        moves.append(
-            (
-                pltpu.make_async_copy(values_in.at[three], near.at[three], near_sem.at[0, t]),
-                pltpu.make_async_copy(near.at[three], values.at[three], near_sem.at[1, t]),
-            )
-        )
     offset = lax.axis_index(KV) * LEN
+    coded = joined[STATS].astype(f32)
+    columns[...] = jnp.transpose(coded[0:8] + coded[8:16])
 
     def place(b):
         start = prior[b] + accepted[b] - offset
@@ -397,15 +358,13 @@
         hit = (start > -PROPS) & (start < LEN)
         return start, pl.multiple_of(base, 16), hit
 
-    def copy_in(b, base):
-        return pltpu.make_async_copy(
-            keys.at[b, pl.ds(base, WINDOW), :], buf.at[b], in_sem.at[b]
-        )
-
-    def copy_out(b, base):
-        return pltpu.make_async_copy(
-            buf.at[b], keys.at[b, pl.ds(base, WINDOW), :], out_sem.at[b]
-        )
+    def copy_in(n, b, base):
+        source = (keys, values)[n].at[b, pl.ds(base, WINDOW), :]
+        return pltpu.make_async_copy(source, buf.at[n, b], in_sem.at[n, b])
+
+    def copy_out(n, b, base):
+        target = (keys, values)[n].at[b, pl.ds(base, WINDOW), :]
+        return pltpu.make_async_copy(buf.at[n, b], target, out_sem.at[n, b])
 
     @pl.loop(0, SEQS)
     def _(b):
@@ -413,43 +372,8 @@
 
         @pl.when(hit)
         def _():
-            copy_in(b, base).start()
-
-    for move in moves:
-        move[0].start()
-    coded = joined[STATS].astype(f32)
-    columns[...] = jnp.transpose(coded[0:8] + coded[8:16])
-
-    def patched(b, start, base):
-        inv = columns[pl.ds(pl.multiple_of(PROPS * b, PROPS), PROPS), 2:3]
-        slot = iota((WINDOW, PROPS), 0) + (base - start)
-        selector = jnp.where(slot == iota((WINDOW, PROPS), 1), 1.0, 0.0).astype(bf16)
-        raw = joined[b, :, WIDTH:].astype(f32)
-        rows = jnp.dot(selector, (inv * raw).astype(bf16), preferred_element_type=f32)
-        slot = iota((WINDOW, WIDTH), 0) + (base - start)
-        return (slot >= 0) & (slot < PROPS), rows
-
-    for t in range(8):
-        moves[t][0].wait()
-
-        @pl.loop(3 * t, 3 * t + 3)
-        def _(b):
-            start, base, hit = place(b)
-
-            @pl.when(hit)
-            def _():
-                inside, rows = patched(b, start, base)
-                window = pl.ds(base, WINDOW)
-                held = near[b, window, :].astype(f32)
-                near[b, window, :] = jnp.where(inside, rows[:, WIDTH:], held).astype(bf16)
-                copy_in(b, base).wait()
-                held = buf[b].astype(f32)
-                buf[b] = jnp.where(inside, rows[:, 0:WIDTH], held).astype(bf16)
-                copy_out(b, base).start()
-
-        moves[t][1].start()
-    for move in moves:
-        move[1].wait()
+            for n in range(2):
+                copy_in(n, b, base).start()
 
     @pl.loop(0, SEQS)
     def _(b):
@@ -457,7 +381,27 @@
 
         @pl.when(hit)
         def _():
-            copy_out(b, base).wait()
+            inv = columns[pl.ds(pl.multiple_of(PROPS * b, PROPS), PROPS), 2:3]
+            slot = iota((WINDOW, PROPS), 0) + (base - start)
+            selector = jnp.where(slot == iota((WINDOW, PROPS), 1), 1.0, 0.0).astype(bf16)
+            slot = iota((WINDOW, WIDTH), 0) + (base - start)
+            inside = (slot >= 0) & (slot < PROPS)
+            for n in range(2):
+                raw = joined[b, :, (n + 1) * WIDTH : (n + 2) * WIDTH].astype(f32)
+                rows = jnp.dot(selector, (inv * raw).astype(bf16), preferred_element_type=f32)
+                copy_in(n, b, base).wait()
+                held = buf[n, b].astype(f32)
+                buf[n, b] = jnp.where(inside, rows, held).astype(bf16)
+                copy_out(n, b, base).start()
+
+    @pl.loop(0, SEQS)
+    def _(b):
+        start, base, hit = place(b)
+
+        @pl.when(hit)
+        def _():
+            for n in range(2):
+                copy_out(n, b, base).wait()
 
 
 def shards(
@@ -490,7 +434,7 @@
     parts, biases = pl.pallas_call(
         project_kernel,
         out_shape=(
-            jax.ShapeDtypeStruct((N_KV, PROPS, ROWS), bf16),
+            pltpu.VMEM((N_KV, PROPS, ROWS), bf16),
             pltpu.VMEM(cum_gates.shape, f32),
         ),
         in_specs=[SM, SM, VM, VM, VM, VM, VM, VM, VM],
@@ -510,25 +454,6 @@
     )
     arrived = lax.all_to_all(parts, KV, 0, 0, tiled=True)
 
-    keys_copy, ancestors = pl.pallas_call(
-        copy_kernel,
-        out_shape=(
-            cache,
-            pltpu.VMEM((PROPS, WIDTH), f32),
-        ),
-        in_specs=[ANY, SM, ANY],
-        out_specs=(ANY, VM),
-        scratch_shapes=[
-            pltpu.VMEM(keys_cache.shape, bf16),
-            pltpu.SemaphoreType.DMA((2, 8)),
-        ],
-        compiler_params=limit(8),
-        cost_estimate=pl.CostEstimate(
-            flops=2_000_000_000, bytes_accessed=12_600_000, transcendentals=0
-        ),
-        name="copy",
-    )(*far(parts, parents.T, keys_cache))
-
     tp_count = lax.axis_size("tp")
 
     def gathered(name, *pieces):
@@ -553,43 +478,44 @@
     block = pl.pallas_call(
         share_kernel,
         out_shape=pltpu.VMEM((N_KV, PROPS, ROWS), bf16),
-        in_specs=[SM, VM, VM, VM],
+        in_specs=[SM, VM],
         out_specs=VM,
         compiler_params=limit(8),
+        cost_estimate=pl.CostEstimate(
+            flops=10_000_000_000, bytes_accessed=800_000, transcendentals=0
+        ),
         name="share",
-    )(gate_bias, *near(arrived, ancestors, w_4))
+    )(*far(gate_bias), *near(arrived))
     joined = lax.all_to_all(block, KV, 0, 0, tiled=True)
 
-    sent = pl.pallas_call(
+    sent, keys_copy, values_copy = pl.pallas_call(
         attention_kernel,
-        out_shape=pltpu.VMEM((512, WIDTH), bf16),
-        in_specs=[VM, VM, VM, ANY, ANY],
-        out_specs=VM,
+        out_shape=(jax.ShapeDtypeStruct((512, WIDTH), bf16), cache, cache),
+        in_specs=[SM, VM, VM, VM, VM],
+        out_specs=(VM, ANY, ANY),
         scratch_shapes=[
             pltpu.VMEM((ROWS, 8), f32),
             pltpu.VMEM((SEQS, 2 * PROPS, LEN), f32),
             pltpu.VMEM((SEQS, 2 * PROPS, LEN), bf16),
-            pltpu.VMEM(keys_cache.shape, bf16),
-            pltpu.VMEM(keys_cache.shape, bf16),
             pltpu.VMEM((SEQS, 2 * PROPS, WIDTH), f32),
             pltpu.VMEM((SEQS, 2 * PROPS, WIDTH), f32),
             pltpu.VMEM((512, WIDTH), f32),
-            pltpu.SemaphoreType.DMA((2, N_TP)),
+            pltpu.SemaphoreType.DMA((2, 4)),
         ],
-        compiler_params=limit(20),
+        compiler_params=limit(12),
         name="attention",
-    )(*near(ancestors, joined, biases), *far(keys_cache, values_cache))
+    )(*far(parents.T), *near(joined, biases, keys_cache, values_cache))
     pieces = lax.all_to_all(sent.reshape(256, 2, WIDTH), (*KV, "tp"), 0, 0, tiled=True)
 
     combined = pl.pallas_call(
         combine_kernel,
         out_shape=jax.ShapeDtypeStruct((N_KV, PROPS, WIDTH), bf16),
-        in_specs=[VM],
+        in_specs=[VM, VM],
         out_specs=VM,
         scratch_shapes=[pltpu.VMEM((64, 8, WIDTH), f32), pltpu.VMEM((64, 8, WIDTH), f32)],
         compiler_params=limit(8),
         name="combine",
-    )(*near(pieces.reshape(512, WIDTH)))
+    )(*near(pieces.reshape(512, WIDTH), w_4))
     shared = lax.all_to_all(combined, KV, 0, 0, tiled=True)
 
     keys_out, values_out = pl.pallas_call(
@@ -597,14 +523,12 @@
         out_shape=(cache, cache),
         in_specs=[SM, SM, VM, ANY, ANY, ANY],
         out_specs=(ANY, ANY),
-        input_output_aliases={4: 0},
+        input_output_aliases={4: 0, 5: 1},
         scratch_shapes=[
-            pltpu.VMEM((SEQS, WINDOW, WIDTH), bf16),
-            pltpu.VMEM(keys_cache.shape, bf16),
+            pltpu.VMEM((2, SEQS, WINDOW, WIDTH), bf16),
             pltpu.VMEM((ROWS, 8), f32),
-            pltpu.SemaphoreType.DMA((SEQS,)),
-            pltpu.SemaphoreType.DMA((SEQS,)),
-            pltpu.SemaphoreType.DMA((2, 8)),
+            pltpu.SemaphoreType.DMA((2, SEQS)),
+            pltpu.SemaphoreType.DMA((2, SEQS)),
         ],
         compiler_params=limit(8),
         cost_estimate=pl.CostEstimate(
@@ -614,7 +538,7 @@
     )(
         *far(prior_len, accepted),
         *near(joined),
-        *far(combined, keys_copy, values_cache),
+        *far(combined, keys_copy, values_copy),
     )
 
     mixed_rows = pl.pallas_call(

time: 92.6 us -> 97.1 us (1.049)
  blocking collectives: 39.3 us -> 45.5 us
  Pallas kernels: 18.8 us -> 13.7 us
  starting transfers between devices: 18 us -> 21.9 us
    all_to_all x1, blocking collectives: 18.3 us -> 26.4 us  [shards(): arrived = lax.all_to_all(parts, KV, 0, 0, tiled=True)]
    all_to_all x1, starting transfers between devices: 3.84 us -> 10.1 us  [shards(): shared = lax.all_to_all(combined, KV, 0, 0, tiled=True)]
    pallas_call x3 -> x2, Pallas kernels: 11.1 us -> 7.23 us  [the longest x1 5.76 us: shards(): pl.pallas_call(attention_kernel, out_shape=(jax.ShapeDtypeStruct((512, WI...]
    all_to_all x1, starting transfers between devices: 11.3 us -> 7.47 us  [shards(): lax.all_to_all(sent.reshape(256, 2, WIDTH), (*KV, 'tp'), 0, 0, tiled=True)]
    all_to_all x1, waiting for transfers between devices: 3.12 us -> 0.07 us  [shards(): lax.all_to_all(sent.reshape(256, 2, WIDTH), (*KV, 'tp'), 0, 0, tiled=True)]
    ppermute x3, waiting for transfers between devices: 4.85 us -> 6.96 us  [across(): return lax.ppermute(x, 'tp', [(i, i ^ bit) for i in range(tp_count)])]
    all_to_all x1, blocking collectives: 21 us -> 19.1 us  [shards(): joined = lax.all_to_all(block, KV, 0, 0, tiled=True)]
    pallas_call x1, Pallas kernels: 4.34 us -> 2.83 us  [shards(): pl.pallas_call(write_kernel, out_shape=(cache, cache), in_specs=[SM, SM,...]
  transfers between devices with their start and end apart: 5 -> 5, of which waited for: 4 -> 5; matrix products, arithmetic and copies ran while one was open for 0% -> 0% of each run, Pallas kernels for 10% -> 4%
where the time goes in v5:
time: 97.1 us; the launch traced here: 96.5 us
  blocking collectives  45.5 us (47%)
  starting transfers between devices  21.9 us (23%)
  waiting for transfers between devices  14.8 us (15%)
  Pallas kernels  13.7 us (14%)
    all_to_all x1, blocking collectives, shards(): arrived = lax.all_to_all(parts, KV, 0, 0, tiled=True)  26.4 us
    all_to_all x1, blocking collectives, shards(): joined = lax.all_to_all(block, KV, 0, 0, tiled=True)  19.1 us
    all_to_all x1, starting transfers between devices, shards(): shared = lax.all_to_all(combined, KV, 0, 0, tiled=True)  10.1 us
    all_to_all x1, waiting for transfers between devices, shards(): shared = lax.all_to_all(combined, KV, 0, 0, tiled=True)  7.78 us
    all_to_all x1, starting transfers between devices, shards(): lax.all_to_all(sent.reshape(256, 2, WIDTH), (*KV, 'tp'), 0, 0, tiled=True)  7.47 us
    ppermute x3, waiting for transfers between devices, across(): return lax.ppermute(x, 'tp', [(i, i ^ bit) for i in range(tp_count)])  6.96 us
    pallas_call x1, Pallas kernels, shards(): pl.pallas_call(attention_kernel, out_shape=(jax.ShapeDtypeStruct((512, WI...  5.76 us
    ppermute x3, starting transfers between devices, across(): return lax.ppermute(x, 'tp', [(i, i ^ bit) for i in range(tp_count)])  4.29 us
  transfers between devices with their start and end apart: 5, of which 5 were waited for; matrix products, arithmetic and copies ran while one was open for 0% of the time, Pallas kernels for 4%

profile of v5, /device:TPU:8, one launch (start us, length us, event | category | flops | bytes accessed | tf_op | source)
XLA Modules:
  0.0 96.5 jit_solution(1779458953657567062)
XLA Ops:
  0.6 1.5 %project.1 = (bf16[32,16,384]{2,1,0:T(8,128)(2,1)S(1)}, f32[24,2,512]{2,1,0:T(2,128)S(1)}) custom-call(s32[24]{0:T(128)} %prior.3, s32[24]{0:T(128)} %accepted.3, bf16[64,384]{1,0:T(8,128)(2,1)} %bitcast.18, f32[1,64]{1,0:T(1,128)} %bitcast.20, bf16[64,128]{1,0:T(8,128)(2,1)} %w_q.1, bf16[64,128]{1,0:T(8,128)(2,1)} %w_k.1, bf16[64,128]{1,0:T(8,128)(2,1)} %w_v.1, ...), custom_call_target="tpu_custom_call" | custom-call | tf_op jit(solution)/shard_map/project/pallas_call | solution.py:434
  2.1 26.4 %all_to_all.20.parts = bf16[32,16,384]{2,1,0:T(8,128)(2,1)S(1)} all-to-all(bf16[32,16,384]{2,1,0:T(8,128)(2,1)S(1)} %get-tuple-element.10), channel_id=1, replica_groups=mesh['kv_0'=8,'kv_1'=4,'tp'=8] {'kv_0','kv_1'}, dimensions={0} | all-to-all | bytes 786432 | tf_op jit(solution)/shard_map/all_to_all | solution.py:455
  28.5 0.0 copy-start
  28.5 0.0 copy-start.1
  28.5 0.9 share.1
  29.4 19.1 %all_to_all.21.joined = bf16[32,16,384]{2,1,0:T(8,128)(2,1)S(1)} all-to-all(bf16[32,16,384]{2,1,0:T(8,128)(2,1)S(1)} %share.1), channel_id=1, replica_groups=mesh['kv_0'=8,'kv_1'=4,'tp'=8] {'kv_0','kv_1'}, dimensions={0} | all-to-all | bytes 786432 | tf_op jit(solution)/shard_map/all_to_all | solution.py:489
  48.5 0.0 copy-done
  48.5 0.0 copy-done.1
  48.5 0.0 copy-start.2
  48.5 5.8 %attention.1 = (bf16[512,128]{1,0:T(8,128)(2,1)}, bf16[24,512,128]{2,1,0:T(8,128)(2,1)}, bf16[24,512,128]{2,1,0:T(8,128)(2,1)}) custom-call(s32[16,24]{1,0:T(8,128)} %bitcast.19, bf16[32,16,384]{2,1,0:T(8,128)(2,1)S(1)} %all_to_all.21.joined, f32[24,2,512]{2,1,0:T(2,128)S(1)} %get-tuple-element.11.biases, bf16[24,512,128]{2,1,0:T(8,128)(2,1)S(1)} %copy-done, ...), custom_call_target="tpu_custom_call" | custom-call | tf_op jit(solution)/shard_map/attention/pallas_call | solution.py:491
  54.3 7.5 %all-to-all-start.2 = ((bf16[256,2,128]{2,1,0:T(2,128)(2,1)}), bf16[256,2,128]{2,1,0:T(2,128)(2,1)S(1)}, u32[]{:S(2)}, u32[]{:S(2)}) async-start(bf16[256,2,128]{2,1,0:T(2,128)(2,1)} %bitcast.4), calls=%async_computation.2 | async-start | bytes 262144 | tf_op jit(solution)/shard_map/all_to_all | solution.py:508
  61.7 0.0 copy-done.2
  61.7 0.2 collective-permute-start
  62.0 1.1 %collective-permute-done.w_1 = bf16[64,128]{1,0:T(8,128)(2,1)S(1)} collective-permute-done((bf16[64,128]{1,0:T(8,128)(2,1)S(1)}, bf16[64,128]{1,0:T(8,128)(2,1)S(1)}, u32[]{:S(2)}, u32[]{:S(2)}) %collective-permute-start) | collective-permute-done | bytes 16416 | tf_op jit(solution)/shard_map/ppermute | solution.py:470
  63.0 0.7 pair.1.first
  63.7 2.1 %collective-permute-start.1 = (bf16[2,64,128]{2,1,0:T(8,128)(2,1)S(1)}, bf16[2,64,128]{2,1,0:T(8,128)(2,1)S(1)}, u32[]{:S(2)}, u32[]{:S(2)}) collective-permute-start(bf16[2,64,128]{2,1,0:T(8,128)(2,1)S(1)} %pair.1.first), channel_id=1, source_target_pairs={{0,2},{1,3},{2,0},{3,1},{4,6},{5,7},{6,4},{7,5},{8,10},{9,11},{10,... | collective-permute-start | bytes 98312 | tf_op jit(solution)/shard_map/ppermute | solution.py:470
  65.9 2.0 %collective-permute-done.1.second.w_2 = bf16[2,64,128]{2,1,0:T(8,128)(2,1)S(1)} collective-permute-done((bf16[2,64,128]{2,1,0:T(8,128)(2,1)S(1)}, bf16[2,64,128]{2,1,0:T(8,128)(2,1)S(1)}, u32[]{:S(2)}, u32[]{:S(2)}) %collective-permute-start.1) | collective-permute-done | bytes 32800 | tf_op jit(solution)/shard_map/ppermute | solution.py:470
  67.9 1.9 %collective-permute-start.2 = (bf16[4,64,128]{2,1,0:T(8,128)(2,1)S(1)}, bf16[4,64,128]{2,1,0:T(8,128)(2,1)S(1)}, u32[]{:S(2)}, u32[]{:S(2)}) collective-permute-start(bf16[4,64,128]{2,1,0:T(8,128)(2,1)S(1)} %four.1), channel_id=1, source_target_pairs={{0,4},{1,5},{2,6},{3,7},{4,0},{5,1},{6,2},{7,3},{8,12},{9,13},{10,... | collective-permute-start | bytes 196616 | tf_op jit(solution)/shard_map/ppermute | solution.py:470
  69.9 3.9 %collective-permute-done.2.after_w.w_4 = bf16[4,64,128]{2,1,0:T(8,128)(2,1)S(1)} collective-permute-done((bf16[4,64,128]{2,1,0:T(8,128)(2,1)S(1)}, bf16[4,64,128]{2,1,0:T(8,128)(2,1)S(1)}, u32[]{:S(2)}, u32[]{:S(2)}) %collective-permute-start.2) | collective-permute-done | bytes 65568 | tf_op jit(solution)/shard_map/ppermute | solution.py:470
  73.7 0.1 all-to-all-done.2
  73.8 1.1 %combine.1.after = bf16[32,16,128]{2,1,0:T(8,128)(2,1)} custom-call(bf16[512,128]{1,0:T(8,128)(2,1)S(1)} %bitcast.11, bf16[4,64,128]{2,1,0:T(8,128)(2,1)S(1)} %collective-permute-done.2.after_w.w_4), custom_call_target="tpu_custom_call" | custom-call | tf_op jit(solution)/shard_map/combine/pallas_call | solution.py:510
  74.9 10.1 %all-to-all-start.3 = ((bf16[32,16,128]{2,1,0:T(8,128)(2,1)}), bf16[32,16,128]{2,1,0:T(8,128)(2,1)S(1)}, u32[]{:S(2)}, u32[]{:S(2)}) async-start(bf16[32,16,128]{2,1,0:T(8,128)(2,1)} %combine.1.after), calls=%async_computation.3 | async-start | bytes 262144 | tf_op jit(solution)/shard_map/all_to_all | solution.py:519
  85.0 0.0 copy-start.3
  85.0 2.8 %write.1 = (bf16[24,512,128]{2,1,0:T(8,128)(2,1)}, bf16[24,512,128]{2,1,0:T(8,128)(2,1)}) custom-call(s32[24]{0:T(128)} %prior.3, s32[24]{0:T(128)} %accepted.3, bf16[32,16,384]{2,1,0:T(8,128)(2,1)S(1)} %all_to_all.21.joined, bf16[32,16,128]{2,1,0:T(8,128)(2,1)} %combine.1.after, ...), custom_call_target="tpu_custom_call", output_to_operand_aliasing={{0}: (4, {}), {1}: (5, {})} | custom-call | flops 2000000000 | bytes 100000 | tf_op jit(solution)/shard_map/write/pallas_call | solution.py:521
  87.8 7.8 %all-to-all-done.3 = bf16[32,16,128]{2,1,0:T(8,128)(2,1)S(1)} async-done(((bf16[32,16,128]{2,1,0:T(8,128)(2,1)}), bf16[32,16,128]{2,1,0:T(8,128)(2,1)S(1)}, u32[]{:S(2)}, u32[]{:S(2)}) %all-to-all-start.3) | async-done | bytes 131104 | tf_op jit(solution)/shard_map/all_to_all | solution.py:519
  95.6 0.0 copy-done.3
  95.6 0.9 output.1
  (1 shorter events, 0.0 us)
Async XLA Ops:
  28.5 20.0 %copy-start = (bf16[24,512,128]{2,1,0:T(8,128)(2,1)S(1)}, bf16[24,512,128]{2,1,0:T(8,128)(2,1)}, u32[]{:S(2)}) copy-start(bf16[24,512,128]{2,1,0:T(8,128)(2,1)} %keys.1) | copy-start | bytes 9437188
  28.5 20.0 %copy-start.1 = (bf16[24,512,128]{2,1,0:T(8,128)(2,1)S(1)}, bf16[24,512,128]{2,1,0:T(8,128)(2,1)}, u32[]{:S(2)}) copy-start(bf16[24,512,128]{2,1,0:T(8,128)(2,1)} %values.1) | copy-start | bytes 9437188
  48.5 13.2 %copy-start.2 = (bf16[128,64]{0,1:T(8,128)(2,1)S(1)}, bf16[128,64]{0,1:T(8,128)(2,1)}, u32[]{:S(2)}) copy-start(bf16[128,64]{0,1:T(8,128)(2,1)} %param.21) | copy-start | bytes 49156
  54.3 19.5 %all-to-all-start.2 = ((bf16[256,2,128]{2,1,0:T(2,128)(2,1)}), bf16[256,2,128]{2,1,0:T(2,128)(2,1)S(1)}, u32[]{:S(2)}, u32[]{:S(2)}) async-start(bf16[256,2,128]{2,1,0:T(2,128)(2,1)} %bitcast.4), calls=%async_computation.2 | async-start | bytes 262144 | tf_op jit(solution)/shard_map/all_to_all | solution.py:508
  61.7 1.3 %collective-permute-start = (bf16[64,128]{1,0:T(8,128)(2,1)S(1)}, bf16[64,128]{1,0:T(8,128)(2,1)S(1)}, u32[]{:S(2)}, u32[]{:S(2)}) collective-permute-start(bf16[64,128]{1,0:T(8,128)(2,1)S(1)} %bitcast.14), channel_id=1, source_target_pairs={{0,1},{1,0},{2,3},{3,2},{4,5},{5,4},{6,7},{7,6},{8,9},{9,8},{10,11... | collective-permute-start | bytes 49160 | tf_op jit(solution)/shard_map/ppermute | solution.py:470
  63.7 4.2 %collective-permute-start.1 = (bf16[2,64,128]{2,1,0:T(8,128)(2,1)S(1)}, bf16[2,64,128]{2,1,0:T(8,128)(2,1)S(1)}, u32[]{:S(2)}, u32[]{:S(2)}) collective-permute-start(bf16[2,64,128]{2,1,0:T(8,128)(2,1)S(1)} %pair.1.first), channel_id=1, source_target_pairs={{0,2},{1,3},{2,0},{3,1},{4,6},{5,7},{6,4},{7,5},{8,10},{9,11},{10,... | collective-permute-start | bytes 98312 | tf_op jit(solution)/shard_map/ppermute | solution.py:470
  67.9 5.8 %collective-permute-start.2 = (bf16[4,64,128]{2,1,0:T(8,128)(2,1)S(1)}, bf16[4,64,128]{2,1,0:T(8,128)(2,1)S(1)}, u32[]{:S(2)}, u32[]{:S(2)}) collective-permute-start(bf16[4,64,128]{2,1,0:T(8,128)(2,1)S(1)} %four.1), channel_id=1, source_target_pairs={{0,4},{1,5},{2,6},{3,7},{4,0},{5,1},{6,2},{7,3},{8,12},{9,13},{10,... | collective-permute-start | bytes 196616 | tf_op jit(solution)/shard_map/ppermute | solution.py:470
  74.9 20.7 %all-to-all-start.3 = ((bf16[32,16,128]{2,1,0:T(8,128)(2,1)}), bf16[32,16,128]{2,1,0:T(8,128)(2,1)S(1)}, u32[]{:S(2)}, u32[]{:S(2)}) async-start(bf16[32,16,128]{2,1,0:T(8,128)(2,1)} %combine.1.after), calls=%async_computation.3 | async-start | bytes 262144 | tf_op jit(solution)/shard_map/all_to_all | solution.py:519
  85.0 10.6 %copy-start.3 = (bf16[128,64]{0,1:T(8,128)(2,1)S(1)}, bf16[128,64]{0,1:T(8,128)(2,1)}, u32[]{:S(2)}) copy-start(bf16[128,64]{0,1:T(8,128)(2,1)} %param.21) | copy-start | bytes 49156

commit v6 on v4

--- a/solution.py
+++ b/solution.py
@@ -93,7 +93,7 @@
     out[STATS + 1 :] = jnp.zeros((N_KV - STATS - 1, PROPS, ROWS), bf16)
 
 
-def share_kernel(bias, parts, after, after_w, out):
+def share_kernel(bias, parts, after_w, out):
     kv, tp = lax.axis_index(KV), lax.axis_index("tp")
     total = jnp.zeros((PROPS, ROWS), f32)
     for k in range(N_KV):
@@ -111,17 +111,16 @@
 
 
 def attention_kernel(
-    ancestors,
+    parents,
     joined,
     biases,
-    keys_far,
-    values_far,
+    keys,
+    values,
     out,
+    keys_out,
     columns,
     scores_buf,
     weights_buf,
-    keys,
-    values,
     v_buf,
     stat_buf,
     mixed,
@@ -129,12 +128,9 @@
 ):
     kv = lax.axis_index(KV)
     moves = []
-    for n, (source, target) in enumerate(((keys_far, keys), (values_far, values))):
-        for t in range(N_TP):
-            three = pl.ds(3 * t, 3)
-            moves.append(
-                pltpu.make_async_copy(source.at[three], target.at[three], sems.at[n, t])
-            )
+    for t in range(4):
+        six = pl.ds(6 * t, 6)
+        moves.append(pltpu.make_async_copy(keys.at[six], keys_out.at[six], sems.at[t]))
     for move in moves:
         move.start()
     coded = joined[STATS].astype(f32)
@@ -201,7 +197,19 @@
         mixed[pl.ds(2 * t, N_KV, stride=16), :] = jnp.where(low, first, second)
         mixed[pl.ds(2 * t + 1, N_KV, stride=16), :] = jnp.where(low, third, stats)
 
-    def tree():
+    def lineage():
+        row = iota((PROPS, WIDTH), 0)
+        linked = jnp.where(lane == row, 1.0, 0.0)
+        for i in range(PROPS):
+            linked = jnp.where((row == i) & (lane == parents[i, own]), 1.0, linked)
+        return linked
+
+    def squared(linked):
+        other = jnp.concatenate([linked, jnp.zeros((WIDTH - PROPS, WIDTH), f32)], axis=0)
+        product = jnp.dot(linked.astype(bf16), other.astype(bf16), preferred_element_type=f32)
+        return jnp.minimum(product, 1.0)
+
+    def tree(reached):
         mine = pl.ds(pl.multiple_of(PROPS * own, PROPS), PROPS)
         pad = jnp.zeros((WIDTH - PROPS, WIDTH), f32)
         picks = (iota((ROWS, WIDTH), 0) == iota((ROWS, WIDTH), 1) + PROPS * own) & (
@@ -210,7 +218,6 @@
         own_gates = jnp.dot(
             joined[STATS], jnp.where(picks, 1.0, 0.0).astype(bf16), preferred_element_type=f32
         ).astype(bf16)
-        reached = ancestors[...]
         tree = dot_t(own_gates, jnp.concatenate([reached, pad], axis=0).astype(bf16))
         tree = tree[0:8] + tree[8:16]
         last = jnp.sum(
@@ -235,10 +242,6 @@
         return tree_scores, tree_top, new_values
 
     for step in range(N_TP + 2):
-        if step < N_TP:
-            moves[step].wait()
-        if step >= 2:
-            moves[N_TP + step - 2].wait()
         for s in range(3):
             if step < N_TP:
                 score(3 * step + s)
@@ -246,8 +249,12 @@
                 weigh(3 * step - 3 + s)
             if step >= 2:
                 gather(3 * step - 6 + s)
-        if step == 3:
-            tree_scores, tree_top, new_values = tree()
+        if step == 0:
+            reached = lineage()
+        if 1 <= step <= 4:
+            reached = squared(reached)
+        if step == 5:
+            tree_scores, tree_top, new_values = tree(reached)
         if step == N_TP:
             scores = scores_buf[own]
             top = jnp.maximum(jnp.max(scores, axis=1, keepdims=True), tree_top)
@@ -266,6 +273,8 @@
     for t in range(N_TP):
         pack(t)
     out[...] = mixed[...].astype(bf16)
+    for move in moves:
+        move.wait()
 
 
 def combine_kernel(parts, out, tops, sums):
@@ -334,36 +343,6 @@
     out[count:] = second[...]
 
 
-def copy_kernel(after, parents, keys, keys_out, ancestors, keys_near, sems):
-    moves = []
-    for t in range(8):
-        three = pl.ds(3 * t, 3)
-        moves.append(
-            (
-                pltpu.make_async_copy(keys.at[three], keys_near.at[three], sems.at[0, t]),
-                pltpu.make_async_copy(keys_near.at[three], keys_out.at[three], sems.at[1, t]),
-            )
-        )
-    for move in moves:
-        move[0].start()
-    own = jnp.minimum(lax.axis_index(KV), SEQS - 1)
-    row = iota((PROPS, WIDTH), 0)
-    lane = iota((PROPS, WIDTH), 1)
-    reached = jnp.where(lane == row, 1.0, 0.0)
-    for i in range(PROPS):
-        reached = jnp.where((row == i) & (lane == parents[i, own]), 1.0, reached)
-    pad = jnp.zeros((WIDTH - PROPS, WIDTH), f32)
-    for _ in range(4):
-        other = jnp.concatenate([reached, pad], axis=0).astype(bf16)
-        reached = jnp.minimum(jnp.dot(reached.astype(bf16), other, preferred_element_type=f32), 1.0)
-    ancestors[...] = reached
-    for move in moves:
-        move[0].wait()
-        move[1].start()
-    for move in moves:
-        move[1].wait()
-
-
 def write_kernel(
     prior,
     accepted,
@@ -510,25 +489,6 @@
     )
     arrived = lax.all_to_all(parts, KV, 0, 0, tiled=True)
 
-    keys_copy, ancestors = pl.pallas_call(
-        copy_kernel,
-        out_shape=(
-            cache,
-            pltpu.VMEM((PROPS, WIDTH), f32),
-        ),
-        in_specs=[ANY, SM, ANY],
-        out_specs=(ANY, VM),
-        scratch_shapes=[
-            pltpu.VMEM(keys_cache.shape, bf16),
-            pltpu.SemaphoreType.DMA((2, 8)),
-        ],
-        compiler_params=limit(8),
-        cost_estimate=pl.CostEstimate(
-            flops=2_000_000_000, bytes_accessed=12_600_000, transcendentals=0
-        ),
-        name="copy",
-    )(*far(parts, parents.T, keys_cache))
-
     tp_count = lax.axis_size("tp")
 
     def gathered(name, *pieces):
@@ -553,32 +513,33 @@
     block = pl.pallas_call(
         share_kernel,
         out_shape=pltpu.VMEM((N_KV, PROPS, ROWS), bf16),
-        in_specs=[SM, VM, VM, VM],
+        in_specs=[SM, VM, ANY],
         out_specs=VM,
         compiler_params=limit(8),
+        cost_estimate=pl.CostEstimate(
+            flops=10_000_000_000, bytes_accessed=800_000, transcendentals=0
+        ),
         name="share",
-    )(gate_bias, *near(arrived, ancestors, w_4))
+    )(*far(gate_bias), *near(arrived), *far(w_4))
     joined = lax.all_to_all(block, KV, 0, 0, tiled=True)
 
-    sent = pl.pallas_call(
+    sent, keys_copy = pl.pallas_call(
         attention_kernel,
-        out_shape=pltpu.VMEM((512, WIDTH), bf16),
-        in_specs=[VM, VM, VM, ANY, ANY],
-        out_specs=VM,
+        out_shape=(pltpu.VMEM((512, WIDTH), bf16), cache),
+        in_specs=[SM, VM, VM, VM, VM],
+        out_specs=(VM, ANY),
         scratch_shapes=[
             pltpu.VMEM((ROWS, 8), f32),
             pltpu.VMEM((SEQS, 2 * PROPS, LEN), f32),
             pltpu.VMEM((SEQS, 2 * PROPS, LEN), bf16),
-            pltpu.VMEM(keys_cache.shape, bf16),
-            pltpu.VMEM(keys_cache.shape, bf16),
             pltpu.VMEM((SEQS, 2 * PROPS, WIDTH), f32),
             pltpu.VMEM((SEQS, 2 * PROPS, WIDTH), f32),
             pltpu.VMEM((512, WIDTH), f32),
-            pltpu.SemaphoreType.DMA((2, N_TP)),
+            pltpu.SemaphoreType.DMA((4,)),
         ],
-        compiler_params=limit(20),
+        compiler_params=limit(12),
         name="attention",
-    )(*near(ancestors, joined, biases), *far(keys_cache, values_cache))
+    )(*far(parents.T), *near(joined, biases, keys_cache, values_cache))
     pieces = lax.all_to_all(sent.reshape(256, 2, WIDTH), (*KV, "tp"), 0, 0, tiled=True)
 
     combined = pl.pallas_call(

time: 92.6 us -> 93 us (level)
  Pallas kernels: 18.8 us -> 15 us
  waiting for transfers between devices: 14.6 us -> 18.3 us
    pallas_call x2 -> x1, Pallas kernels: 8.87 us -> 4.02 us  [shards(): pl.pallas_call(attention_kernel, out_shape=(pltpu.VMEM((512, WIDTH), bf16...]
    ppermute x3, waiting for transfers between devices: 4.85 us -> 8.43 us  [across(): return lax.ppermute(x, 'tp', [(i, i ^ bit) for i in range(tp_count)])]
    all_to_all x1, blocking collectives: 18.3 us -> 19.4 us  [shards(): lax.all_to_all(sent.reshape(256, 2, WIDTH), (*KV, 'tp'), 0, 0, tiled=True)]
  transfers between devices with their start and end apart: 5 -> 5, of which waited for: 4 -> 5; matrix products, arithmetic and copies ran while one was open for 0% -> 0% of each run, Pallas kernels for 10% -> 6%
where the time goes in v6:
time: 93 us; the launch traced here: 91.8 us
  blocking collectives  39.6 us (43%)
  waiting for transfers between devices  18.3 us (20%)
  starting transfers between devices  18.1 us (19%)
  Pallas kernels  15 us (16%)
    all_to_all x1, blocking collectives, shards(): joined = lax.all_to_all(block, KV, 0, 0, tiled=True)  20.2 us
    all_to_all x1, blocking collectives, shards(): lax.all_to_all(sent.reshape(256, 2, WIDTH), (*KV, 'tp'), 0, 0, tiled=True)  19.4 us
    all_to_all x1, starting transfers between devices, shards(): arrived = lax.all_to_all(parts, KV, 0, 0, tiled=True)  11.3 us
    ppermute x3, waiting for transfers between devices, across(): return lax.ppermute(x, 'tp', [(i, i ^ bit) for i in range(tp_count)])  8.43 us
    all_to_all x1, waiting for transfers between devices, shards(): shared = lax.all_to_all(combined, KV, 0, 0, tiled=True)  6.65 us
    pallas_call x1, Pallas kernels, shards(): pl.pallas_call(write_kernel, out_shape=(cache, cache), in_specs=[SM, SM,...  4.34 us
    pallas_call x1, Pallas kernels, shards(): pl.pallas_call(attention_kernel, out_shape=(pltpu.VMEM((512, WIDTH), bf16...  4.02 us
    all_to_all x1, starting transfers between devices, shards(): shared = lax.all_to_all(combined, KV, 0, 0, tiled=True)  3.85 us
  transfers between devices with their start and end apart: 5, of which 5 were waited for; matrix products, arithmetic and copies ran while one was open for 0% of the time, Pallas kernels for 6%

profile of v6, /device:TPU:8, one launch (start us, length us, event | category | flops | bytes accessed | tf_op | source)
XLA Modules:
  0.0 91.8 jit_solution(14309155309966284764)
XLA Ops:
  0.6 2.2 %project.1 = (bf16[32,16,384]{2,1,0:T(8,128)(2,1)}, f32[24,2,512]{2,1,0:T(2,128)S(1)}) custom-call(s32[24]{0:T(128)} %prior.3, s32[24]{0:T(128)} %accepted.3, bf16[64,384]{1,0:T(8,128)(2,1)} %bitcast.19, f32[1,64]{1,0:T(1,128)} %bitcast.21, bf16[64,128]{1,0:T(8,128)(2,1)} %w_q.1, bf16[64,128]{1,0:T(8,128)(2,1)} %w_k.1, bf16[64,128]{1,0:T(8,128)(2,1)} %w_v.1, ...), custom_call_target="tpu_custom_call" | custom-call | tf_op jit(solution)/shard_map/project/pallas_call | solution.py:469
  2.9 0.0 copy-start.4
  2.9 11.3 %all-to-all-start = ((bf16[32,16,384]{2,1,0:T(8,128)(2,1)}), bf16[32,16,384]{2,1,0:T(8,128)(2,1)S(1)}, u32[]{:S(2)}, u32[]{:S(2)}) async-start(bf16[32,16,384]{2,1,0:T(8,128)(2,1)} %get-tuple-element.9), calls=%async_computation | async-start | bytes 786432 | tf_op jit(solution)/shard_map/all_to_all | solution.py:490
  14.2 0.1 collective-permute-start
  14.3 1.4 %collective-permute-done.w_1 = bf16[64,128]{1,0:T(8,128)(2,1)S(1)} collective-permute-done((bf16[64,128]{1,0:T(8,128)(2,1)}, bf16[64,128]{1,0:T(8,128)(2,1)S(1)}, u32[]{:S(2)}, u32[]{:S(2)}) %collective-permute-start) | collective-permute-done | bytes 16416 | tf_op jit(solution)/shard_map/ppermute | solution.py:505
  15.7 0.7 pair.1.first
  16.4 0.4 collective-permute-start.1
  16.8 3.5 %collective-permute-done.1.second.w_2 = bf16[2,64,128]{2,1,0:T(8,128)(2,1)S(1)} collective-permute-done((bf16[2,64,128]{2,1,0:T(8,128)(2,1)S(1)}, bf16[2,64,128]{2,1,0:T(8,128)(2,1)S(1)}, u32[]{:S(2)}, u32[]{:S(2)}) %collective-permute-start.1) | collective-permute-done | bytes 32800 | tf_op jit(solution)/shard_map/ppermute | solution.py:505
  20.3 0.0 copy-done.4
  20.3 0.0 copy-start.2
  20.3 0.0 copy-start
  20.3 2.4 %collective-permute-start.2 = (bf16[4,64,128]{2,1,0:T(8,128)(2,1)S(1)}, bf16[4,64,128]{2,1,0:T(8,128)(2,1)}, u32[]{:S(2)}, u32[]{:S(2)}) collective-permute-start(bf16[4,64,128]{2,1,0:T(8,128)(2,1)S(1)} %four.1), channel_id=1, source_target_pairs={{0,4},{1,5},{2,6},{3,7},{4,0},{5,1},{6,2},{7,3},{8,12},{9,13},{10,... | collective-permute-start | bytes 196616 | tf_op jit(solution)/shard_map/ppermute | solution.py:505
  22.7 0.0 copy-done.2
  22.7 3.6 %collective-permute-done.2.after_w.w_4 = bf16[4,64,128]{2,1,0:T(8,128)(2,1)} collective-permute-done((bf16[4,64,128]{2,1,0:T(8,128)(2,1)S(1)}, bf16[4,64,128]{2,1,0:T(8,128)(2,1)}, u32[]{:S(2)}, u32[]{:S(2)}) %collective-permute-start.2) | collective-permute-done | bytes 65568 | tf_op jit(solution)/shard_map/ppermute | solution.py:505
  26.3 3.2 %all-to-all-done.parts = bf16[32,16,384]{2,1,0:T(8,128)(2,1)S(1)} async-done(((bf16[32,16,384]{2,1,0:T(8,128)(2,1)}), bf16[32,16,384]{2,1,0:T(8,128)(2,1)S(1)}, u32[]{:S(2)}, u32[]{:S(2)}) %all-to-all-start) | async-done | bytes 393248 | tf_op jit(solution)/shard_map/all_to_all | solution.py:490
  29.5 0.0 copy-start.1
  29.5 0.0 copy-start.5
  29.5 0.9 share.1
  30.4 20.2 %all_to_all.20.joined = bf16[32,16,384]{2,1,0:T(8,128)(2,1)S(1)} all-to-all(bf16[32,16,384]{2,1,0:T(8,128)(2,1)S(1)} %share.1), channel_id=1, replica_groups=mesh['kv_0'=8,'kv_1'=4,'tp'=8] {'kv_0','kv_1'}, dimensions={0} | all-to-all | bytes 786432 | tf_op jit(solution)/shard_map/all_to_all | solution.py:524
  50.6 0.0 copy-done
  50.6 0.0 copy-done.1
  50.6 0.0 copy-done.5
  50.6 4.0 %attention.1 = (bf16[512,128]{1,0:T(8,128)(2,1)S(1)}, bf16[24,512,128]{2,1,0:T(8,128)(2,1)}) custom-call(s32[16,24]{1,0:T(8,128)} %bitcast.20, bf16[32,16,384]{2,1,0:T(8,128)(2,1)S(1)} %all_to_all.20.joined, f32[24,2,512]{2,1,0:T(2,128)S(1)} %copy-done.5, bf16[24,512,128]{2,1,0:T(8,128)(2,1)S(1)} %copy-done, bf16[24,512,128]{2,1,0:T(8,128)(2,1)S(1)} %copy-done.1), custom_call_target="tpu_custom_call" | custom-call | tf_op jit(solution)/shard_map/attention/pallas_call | solution.py:526
  54.7 19.4 %all_to_all.21 = bf16[256,2,128]{2,1,0:T(2,128)(2,1)S(1)} all-to-all(bf16[256,2,128]{2,1,0:T(2,128)(2,1)S(1)} %bitcast.13), channel_id=1, replica_groups=mesh['kv_0'=8,'kv_1'=4,'tp'=8] {'kv_0','kv_1','tp'}, dimensions={0} | all-to-all | bytes 262144 | tf_op jit(solution)/shard_map/all_to_all | solution.py:543
  74.0 1.1 %combine.1.after = bf16[32,16,128]{2,1,0:T(8,128)(2,1)} custom-call(bf16[512,128]{1,0:T(8,128)(2,1)S(1)} %bitcast.12), custom_call_target="tpu_custom_call" | custom-call | tf_op jit(solution)/shard_map/combine/pallas_call | solution.py:545
  75.1 3.9 %all-to-all-start.3 = ((bf16[32,16,128]{2,1,0:T(8,128)(2,1)}), bf16[32,16,128]{2,1,0:T(8,128)(2,1)S(1)}, u32[]{:S(2)}, u32[]{:S(2)}) async-start(bf16[32,16,128]{2,1,0:T(8,128)(2,1)} %combine.1.after), calls=%async_computation.3 | async-start | bytes 262144 | tf_op jit(solution)/shard_map/all_to_all | solution.py:554
  79.0 0.0 copy-start.3
  79.0 0.0 copy-start.6
  79.0 4.3 %write.1 = (bf16[24,512,128]{2,1,0:T(8,128)(2,1)}, bf16[24,512,128]{2,1,0:T(8,128)(2,1)}) custom-call(s32[24]{0:T(128)} %prior.3, s32[24]{0:T(128)} %accepted.3, bf16[32,16,384]{2,1,0:T(8,128)(2,1)S(1)} %all_to_all.20.joined, bf16[32,16,128]{2,1,0:T(8,128)(2,1)} %combine.1.after, ...), custom_call_target="tpu_custom_call", output_to_operand_aliasing={{0}: (4, {})} | custom-call | flops 2000000000 | bytes 100000 | tf_op jit(solution)/shard_map/write/pallas_call | solution.py:556
  83.4 6.7 %all-to-all-done.3 = bf16[32,16,128]{2,1,0:T(8,128)(2,1)S(1)} async-done(((bf16[32,16,128]{2,1,0:T(8,128)(2,1)}), bf16[32,16,128]{2,1,0:T(8,128)(2,1)S(1)}, u32[]{:S(2)}, u32[]{:S(2)}) %all-to-all-start.3) | async-done | bytes 131104 | tf_op jit(solution)/shard_map/all_to_all | solution.py:554
  90.0 0.0 copy-done.3
  90.0 0.0 copy-done.6
  90.0 1.7 %output.1 = bf16[48,64]{1,0:T(8,128)(2,1)} custom-call(bf16[512,128]{1,0:T(8,128)(2,1)S(1)} %bitcast.11, bf16[64,128]{1,0:T(8,128)(2,1)S(1)} %bitcast.16, bf16[64,128]{1,0:T(8,128)(2,1)S(1)} %collective-permute-done.w_1, bf16[2,64,128]{2,1,0:T(8,128)(2,1)S(1)} %copy-done.3, bf16[4,64,128]{2,1,0:T(8,128)(2,1)} %collective-permute-done.2.after_w.w_4), custom_call_target="tpu_custom_call" | custom-call | tf_op jit(solution)/shard_map/output/pallas_call | solution.py:581
  (1 shorter events, 0.0 us)
Async XLA Ops:
  2.9 17.4 %copy-start.4 = (f32[24,2,512]{2,1,0:T(2,128)}, f32[24,2,512]{2,1,0:T(2,128)S(1)}, u32[]{:S(2)}) copy-start(f32[24,2,512]{2,1,0:T(2,128)S(1)} %get-tuple-element.10.biases) | copy-start | bytes 294916
  2.9 26.6 %all-to-all-start = ((bf16[32,16,384]{2,1,0:T(8,128)(2,1)}), bf16[32,16,384]{2,1,0:T(8,128)(2,1)S(1)}, u32[]{:S(2)}, u32[]{:S(2)}) async-start(bf16[32,16,384]{2,1,0:T(8,128)(2,1)} %get-tuple-element.9), calls=%async_computation | async-start | bytes 786432 | tf_op jit(solution)/shard_map/all_to_all | solution.py:490
  14.2 1.5 %collective-permute-start = (bf16[64,128]{1,0:T(8,128)(2,1)}, bf16[64,128]{1,0:T(8,128)(2,1)S(1)}, u32[]{:S(2)}, u32[]{:S(2)}) collective-permute-start(bf16[64,128]{1,0:T(8,128)(2,1)} %bitcast.14), channel_id=1, source_target_pairs={{0,1},{1,0},{2,3},{3,2},{4,5},{5,4},{6,7},{7,6},{8,9},{9,8},{10,11... | collective-permute-start | bytes 49160 | tf_op jit(solution)/shard_map/ppermute | solution.py:505
  16.4 3.9 %collective-permute-start.1 = (bf16[2,64,128]{2,1,0:T(8,128)(2,1)S(1)}, bf16[2,64,128]{2,1,0:T(8,128)(2,1)S(1)}, u32[]{:S(2)}, u32[]{:S(2)}) collective-permute-start(bf16[2,64,128]{2,1,0:T(8,128)(2,1)S(1)} %pair.1.first), channel_id=1, source_target_pairs={{0,2},{1,3},{2,0},{3,1},{4,6},{5,7},{6,4},{7,5},{8,10},{9,11},{10,... | collective-permute-start | bytes 98312 | tf_op jit(solution)/shard_map/ppermute | solution.py:505
  20.3 2.4 %copy-start.2 = (bf16[2,64,128]{2,1,0:T(8,128)(2,1)}, bf16[2,64,128]{2,1,0:T(8,128)(2,1)S(1)}, u32[]{:S(2)}) copy-start(bf16[2,64,128]{2,1,0:T(8,128)(2,1)S(1)} %collective-permute-done.1.second.w_2) | copy-start | bytes 98308
  20.3 30.3 %copy-start = (bf16[24,512,128]{2,1,0:T(8,128)(2,1)S(1)}, bf16[24,512,128]{2,1,0:T(8,128)(2,1)}, u32[]{:S(2)}) copy-start(bf16[24,512,128]{2,1,0:T(8,128)(2,1)} %keys.1) | copy-start | bytes 9437188
  20.3 6.0 %collective-permute-start.2 = (bf16[4,64,128]{2,1,0:T(8,128)(2,1)S(1)}, bf16[4,64,128]{2,1,0:T(8,128)(2,1)}, u32[]{:S(2)}, u32[]{:S(2)}) collective-permute-start(bf16[4,64,128]{2,1,0:T(8,128)(2,1)S(1)} %four.1), channel_id=1, source_target_pairs={{0,4},{1,5},{2,6},{3,7},{4,0},{5,1},{6,2},{7,3},{8,12},{9,13},{10,... | collective-permute-start | bytes 196616 | tf_op jit(solution)/shard_map/ppermute | solution.py:505
  29.5 21.2 %copy-start.1 = (bf16[24,512,128]{2,1,0:T(8,128)(2,1)S(1)}, bf16[24,512,128]{2,1,0:T(8,128)(2,1)}, u32[]{:S(2)}) copy-start(bf16[24,512,128]{2,1,0:T(8,128)(2,1)} %values_in.1) | copy-start | bytes 9437188
  29.5 21.2 %copy-start.5 = (f32[24,2,512]{2,1,0:T(2,128)S(1)}, f32[24,2,512]{2,1,0:T(2,128)}, u32[]{:S(2)}) copy-start(f32[24,2,512]{2,1,0:T(2,128)} %copy-done.4) | copy-start | bytes 294916
  75.1 14.9 %all-to-all-start.3 = ((bf16[32,16,128]{2,1,0:T(8,128)(2,1)}), bf16[32,16,128]{2,1,0:T(8,128)(2,1)S(1)}, u32[]{:S(2)}, u32[]{:S(2)}) async-start(bf16[32,16,128]{2,1,0:T(8,128)(2,1)} %combine.1.after), calls=%async_computation.3 | async-start | bytes 262144 | tf_op jit(solution)/shard_map/all_to_all | solution.py:554
  79.0 11.0 %copy-start.3 = (bf16[2,64,128]{2,1,0:T(8,128)(2,1)S(1)}, bf16[2,64,128]{2,1,0:T(8,128)(2,1)}, u32[]{:S(2)}) copy-start(bf16[2,64,128]{2,1,0:T(8,128)(2,1)} %copy-done.2) | copy-start | bytes 98308
  79.0 11.0 %copy-start.6 = (bf16[128,64]{0,1:T(8,128)(2,1)S(1)}, bf16[128,64]{0,1:T(8,128)(2,1)}, u32[]{:S(2)}) copy-start(bf16[128,64]{0,1:T(8,128)(2,1)} %param.21) | copy-start | bytes 49156

commit v7 on v6

--- a/solution.py
+++ b/solution.py
@@ -93,7 +93,7 @@
     out[STATS + 1 :] = jnp.zeros((N_KV - STATS - 1, PROPS, ROWS), bf16)
 
 
-def share_kernel(bias, parts, after_w, out):
+def share_kernel(bias, parts, after_1, after_3, after_5, after_7, out):
     kv, tp = lax.axis_index(KV), lax.axis_index("tp")
     total = jnp.zeros((PROPS, ROWS), f32)
     for k in range(N_KV):
@@ -310,14 +310,8 @@
         out[k] = block
 
 
-def output_kernel(shared, w_0, w_1, w_2, w_4, out, rows):
-    tp = lax.axis_index("tp")
+def output_kernel(shared, w_all, out, rows):
     rows[...] = shared[...].astype(f32)
-    near = (w_0[...], w_1[...], w_2[0], w_2[1], w_4[0], w_4[1], w_4[2], w_4[3])
-    near = [w.astype(f32) for w in near]
-    for bit in (1, 2, 4):
-        swap = (tp & bit) != 0
-        near = [jnp.where(swap, near[g ^ bit], near[g]) for g in range(N_TP)]
     low = iota((PROPS, WIDTH), 1) < HEAD
     total = jnp.zeros((48, 64), f32)
     for g in range(N_TP):
@@ -333,25 +327,28 @@
             ],
             axis=0,
         )
-        total = total + dot_t(block.astype(bf16), near[g].astype(bf16))
+        total = total + dot_t(block.astype(bf16), w_all[g])
     out[...] = total.astype(bf16)
-
-
-def join_kernel(first, second, out):
-    count = first.shape[0]
-    out[0:count] = first[...]
-    out[count:] = second[...]
 
 
 def write_kernel(
     prior,
     accepted,
     joined,
+    w_0,
+    w_1,
+    w_2,
+    w_3,
+    w_4,
+    w_5,
+    w_6,
+    w_7,
     after,
     keys_in,
     values_in,
     keys,
     values,
+    w_all,
     buf,
     near,
     columns,
@@ -396,6 +393,9 @@
 
     for move in moves:
         move[0].start()
+    tp = lax.axis_index("tp")
+    for distance, w in enumerate((w_0, w_1, w_2, w_3, w_4, w_5, w_6, w_7)):
+        w_all[tp ^ distance] = w[...]
     coded = joined[STATS].astype(f32)
     columns[...] = jnp.transpose(coded[0:8] + coded[8:16])
 
@@ -491,36 +491,25 @@
 
     tp_count = lax.axis_size("tp")
 
-    def gathered(name, *pieces):
-        return pl.pallas_call(
-            join_kernel,
-            out_shape=pltpu.VMEM((sum(len(p) for p in pieces), *pieces[0].shape[1:]), bf16),
-            in_specs=[VM, VM],
-            out_specs=VM,
-            compiler_params=limit(2),
-            name=name,
-        )(*pieces)
-
     def across(x, bit):
         return lax.ppermute(x, "tp", [(i, i ^ bit) for i in range(tp_count)])
 
-    w_0 = w_out.T
-    w_1 = across(w_0, 1)
-    w_pair = gathered("pair", *far(w_0[None]), *near(w_1[None]))
-    w_2 = across(w_pair, 2)
-    w_4 = across(gathered("four", *near(w_pair, w_2)), 4)
-
+    all_w = [w_out.T]
+    for bit in (4, 2, 1):
+        all_w = all_w + [across(w, bit) for w in all_w]
+    order = {distance: n for n, distance in enumerate((0, 4, 2, 6, 1, 5, 3, 7))}
+    all_w = [all_w[order[distance]] for distance in range(tp_count)]
     block = pl.pallas_call(
         share_kernel,
         out_shape=pltpu.VMEM((N_KV, PROPS, ROWS), bf16),
-        in_specs=[SM, VM, ANY],
+        in_specs=[SM, VM] + [ANY] * 4,
         out_specs=VM,
         compiler_params=limit(8),
         cost_estimate=pl.CostEstimate(
             flops=10_000_000_000, bytes_accessed=800_000, transcendentals=0
         ),
         name="share",
-    )(*far(gate_bias), *near(arrived), *far(w_4))
+    )(*far(gate_bias), *near(arrived), *far(*all_w[1::2]))
     joined = lax.all_to_all(block, KV, 0, 0, tiled=True)
 
     sent, keys_copy = pl.pallas_call(
@@ -553,12 +542,12 @@
     )(*near(pieces.reshape(512, WIDTH)))
     shared = lax.all_to_all(combined, KV, 0, 0, tiled=True)
 
-    keys_out, values_out = pl.pallas_call(
+    keys_out, values_out, w_all = pl.pallas_call(
         write_kernel,
-        out_shape=(cache, cache),
-        in_specs=[SM, SM, VM, ANY, ANY, ANY],
-        out_specs=(ANY, ANY),
-        input_output_aliases={4: 0},
+        out_shape=(cache, cache, pltpu.VMEM((N_TP, 64, WIDTH), bf16)),
+        in_specs=[SM, SM] + [VM] * 9 + [ANY] * 3,
+        out_specs=(ANY, ANY, VM),
+        input_output_aliases={12: 0},
         scratch_shapes=[
             pltpu.VMEM((SEQS, WINDOW, WIDTH), bf16),
             pltpu.VMEM(keys_cache.shape, bf16),
@@ -575,18 +564,19 @@
     )(
         *far(prior_len, accepted),
         *near(joined),
+        *far(*all_w),
         *far(combined, keys_copy, values_cache),
     )
 
     mixed_rows = pl.pallas_call(
         output_kernel,
         out_shape=jax.ShapeDtypeStruct((48, 64), bf16),
-        in_specs=[VM] * 5,
+        in_specs=[VM, VM],
         out_specs=VM,
         scratch_shapes=[pltpu.VMEM((512, WIDTH), f32)],
         compiler_params=limit(8),
         name="output",
-    )(*near(shared.reshape(512, WIDTH), w_0, w_1, w_2, w_4))
+    )(*near(shared.reshape(512, WIDTH), w_all))
     return (mixed_rows, keys_out, values_out)
 
 

time: 93 us -> 92.9 us (level)
  waiting for transfers between devices: 18.3 us -> 15.9 us
  starting transfers between devices: 18.1 us -> 19.9 us
  Pallas kernels: 15 us -> 13.5 us
  local copies, waits for them, and re-layouts: 0.03 us -> 1.21 us
    ppermute x3 -> x7, waiting for transfers between devices: 8.43 us -> 4.57 us  [across(): return lax.ppermute(x, 'tp', [(i, i ^ bit) for i in range(tp_count)])]
    ppermute x3 -> x7, starting transfers between devices: 2.92 us -> 4.79 us  [across(): return lax.ppermute(x, 'tp', [(i, i ^ bit) for i in range(tp_count)])]
    all_to_all x1, waiting for transfers between devices: 3.18 us -> 4.67 us  [shards(): arrived = lax.all_to_all(parts, KV, 0, 0, tiled=True)]
    unnamed x14 -> x20, local copies, waits for them, and re-layouts: 0.03 us -> 1.21 us
    pallas_call x3 -> x1, Pallas kernels: 5.07 us -> 4.39 us  [shards(): pl.pallas_call(write_kernel, out_shape=(cache, cache, pltpu.VMEM((N_TP, 6...]
  transfers between devices with their start and end apart: 5 -> 9, of which waited for: 5 -> 5; matrix products, arithmetic and copies ran while one was open for 0% -> 0% of each run, Pallas kernels for 6% -> 5%
where the time goes in v7:
time: 92.9 us; the launch traced here: 91.7 us
  blocking collectives  40.4 us (43%)
  starting transfers between devices  19.9 us (21%)
  waiting for transfers between devices  15.9 us (17%)
  Pallas kernels  13.5 us (15%)
  local copies, waits for them, and re-layouts  1.21 us (1%)
    all_to_all x1, blocking collectives, shards(): joined = lax.all_to_all(block, KV, 0, 0, tiled=True)  21 us
    all_to_all x1, blocking collectives, shards(): lax.all_to_all(sent.reshape(256, 2, WIDTH), (*KV, 'tp'), 0, 0, tiled=True)  19.4 us
    all_to_all x1, starting transfers between devices, shards(): arrived = lax.all_to_all(parts, KV, 0, 0, tiled=True)  11.3 us
    all_to_all x1, waiting for transfers between devices, shards(): shared = lax.all_to_all(combined, KV, 0, 0, tiled=True)  6.63 us
    ppermute x7, starting transfers between devices, across(): return lax.ppermute(x, 'tp', [(i, i ^ bit) for i in range(tp_count)])  4.79 us
    all_to_all x1, waiting for transfers between devices, shards(): arrived = lax.all_to_all(parts, KV, 0, 0, tiled=True)  4.67 us
    ppermute x7, waiting for transfers between devices, across(): return lax.ppermute(x, 'tp', [(i, i ^ bit) for i in range(tp_count)])  4.57 us
    pallas_call x1, Pallas kernels, shards(): pl.pallas_call(write_kernel, out_shape=(cache, cache, pltpu.VMEM((N_TP, 6...  4.39 us
  transfers between devices with their start and end apart: 9, of which 5 were waited for; matrix products, arithmetic and copies ran while one was open for 0% of the time, Pallas kernels for 5%

profile of v7, /device:TPU:8, one launch (start us, length us, event | category | flops | bytes accessed | tf_op | source)
XLA Modules:
  0.0 91.7 jit_solution(9185141806756701680)
XLA Ops:
  0.6 2.2 %project.1 = (bf16[32,16,384]{2,1,0:T(8,128)(2,1)}, f32[24,2,512]{2,1,0:T(2,128)S(1)}) custom-call(s32[24]{0:T(128)} %prior.3, s32[24]{0:T(128)} %accepted.3, bf16[64,384]{1,0:T(8,128)(2,1)} %bitcast.12, f32[1,64]{1,0:T(1,128)} %bitcast.14, bf16[64,128]{1,0:T(8,128)(2,1)} %w_q.1, bf16[64,128]{1,0:T(8,128)(2,1)} %w_k.1, bf16[64,128]{1,0:T(8,128)(2,1)} %w_v.1, ...), custom_call_target="tpu_custom_call" | custom-call | tf_op jit(solution)/shard_map/project/pallas_call | solution.py:469
  2.8 0.0 copy-start.2
  2.9 11.3 %all-to-all-start = ((bf16[32,16,384]{2,1,0:T(8,128)(2,1)}), bf16[32,16,384]{2,1,0:T(8,128)(2,1)S(1)}, u32[]{:S(2)}, u32[]{:S(2)}) async-start(bf16[32,16,384]{2,1,0:T(8,128)(2,1)} %get-tuple-element.10), calls=%async_computation | async-start | bytes 786432 | tf_op jit(solution)/shard_map/all_to_all | solution.py:490
  14.2 0.0 copy-done.2
  14.2 0.0 copy-start
  14.2 2.4 %collective-permute-start.3 = (bf16[64,128]{1,0:T(8,128)(2,1)}, bf16[64,128]{1,0:T(8,128)(2,1)S(1)}, u32[]{:S(2)}, u32[]{:S(2)}) collective-permute-start(bf16[64,128]{1,0:T(8,128)(2,1)} %bitcast.15), channel_id=1, source_target_pairs={{0,4},{1,5},{2,6},{3,7},{4,0},{5,1},{6,2},{7,3},{8,12},{9,13},{10,... | collective-permute-start | bytes 49160 | tf_op jit(solution)/shard_map/ppermute | solution.py:495
  16.6 1.3 %collective-permute-start.1 = (bf16[64,128]{1,0:T(8,128)(2,1)}, bf16[64,128]{1,0:T(8,128)(2,1)S(1)}, u32[]{:S(2)}, u32[]{:S(2)}) collective-permute-start(bf16[64,128]{1,0:T(8,128)(2,1)} %bitcast.16), channel_id=1, source_target_pairs={{0,2},{1,3},{2,0},{3,1},{4,6},{5,7},{6,4},{7,5},{8,10},{9,11},{10,... | collective-permute-start | bytes 49160 | tf_op jit(solution)/shard_map/ppermute | solution.py:495
  17.9 1.8 %collective-permute-done.3.w_4 = bf16[64,128]{1,0:T(8,128)(2,1)S(1)} collective-permute-done((bf16[64,128]{1,0:T(8,128)(2,1)}, bf16[64,128]{1,0:T(8,128)(2,1)S(1)}, u32[]{:S(2)}, u32[]{:S(2)}) %collective-permute-start.3) | collective-permute-done | bytes 16416 | tf_op jit(solution)/shard_map/ppermute | solution.py:495
  19.7 0.0 copy-start.4
  19.7 0.5 collective-permute-start.5
  20.2 0.0 collective-permute-start
  20.2 0.5 collective-permute-start.4
  20.7 0.0 collective-permute-done.1.w_2
  20.7 0.0 copy-start.5
  20.7 0.1 collective-permute-start.2
  20.8 2.7 %collective-permute-done.5.w_6 = bf16[64,128]{1,0:T(8,128)(2,1)S(1)} collective-permute-done((bf16[64,128]{1,0:T(8,128)(2,1)S(1)}, bf16[64,128]{1,0:T(8,128)(2,1)S(1)}, u32[]{:S(2)}, u32[]{:S(2)}) %collective-permute-start.5) | collective-permute-done | bytes 16416 | tf_op jit(solution)/shard_map/ppermute | solution.py:495
  23.5 0.0 copy-start.6
  23.5 0.0 collective-permute-start.6
  23.5 0.0 collective-permute-done.after_1.w_1
  23.5 0.0 copy-start.7
  23.5 0.0 collective-permute-done.4.after_5.w_5
  23.5 0.0 copy-start.8
  23.5 0.0 collective-permute-done.2.after_3.w_3
  23.5 0.0 copy-done.5
  23.5 0.5 copy-done.6
  24.1 0.0 copy-done.7
  24.1 0.0 copy-done.8
  24.1 0.0 copy-start.9
  24.1 0.6 copy-done.9
  24.7 0.1 collective-permute-done.6.after_7.w_7
  24.8 4.7 %all-to-all-done.parts = bf16[32,16,384]{2,1,0:T(8,128)(2,1)S(1)} async-done(((bf16[32,16,384]{2,1,0:T(8,128)(2,1)}), bf16[32,16,384]{2,1,0:T(8,128)(2,1)S(1)}, u32[]{:S(2)}, u32[]{:S(2)}) %all-to-all-start) | async-done | bytes 393248 | tf_op jit(solution)/shard_map/all_to_all | solution.py:490
  29.5 0.0 copy-start.1
  29.5 0.0 copy-start.3
  29.5 0.9 share.1
  30.4 0.0 copy-done.4
  30.4 21.0 %all_to_all.20.joined = bf16[32,16,384]{2,1,0:T(8,128)(2,1)S(1)} all-to-all(bf16[32,16,384]{2,1,0:T(8,128)(2,1)S(1)} %share.1), channel_id=1, replica_groups=mesh['kv_0'=8,'kv_1'=4,'tp'=8] {'kv_0','kv_1'}, dimensions={0} | all-to-all | bytes 786432 | tf_op jit(solution)/shard_map/all_to_all | solution.py:513
  51.4 0.0 copy-done
  51.4 0.0 copy-done.1
  51.4 0.0 copy-done.3
  51.4 4.0 %attention.1 = (bf16[512,128]{1,0:T(8,128)(2,1)S(1)}, bf16[24,512,128]{2,1,0:T(8,128)(2,1)}) custom-call(s32[16,24]{1,0:T(8,128)} %bitcast.13, bf16[32,16,384]{2,1,0:T(8,128)(2,1)S(1)} %all_to_all.20.joined, f32[24,2,512]{2,1,0:T(2,128)S(1)} %copy-done.3, bf16[24,512,128]{2,1,0:T(8,128)(2,1)S(1)} %copy-done, bf16[24,512,128]{2,1,0:T(8,128)(2,1)S(1)} %copy-done.1), custom_call_target="tpu_custom_call" | custom-call | tf_op jit(solution)/shard_map/attention/pallas_call | solution.py:515
  55.4 19.4 %all_to_all.21 = bf16[256,2,128]{2,1,0:T(2,128)(2,1)S(1)} all-to-all(bf16[256,2,128]{2,1,0:T(2,128)(2,1)S(1)} %bitcast.10), channel_id=1, replica_groups=mesh['kv_0'=8,'kv_1'=4,'tp'=8] {'kv_0','kv_1','tp'}, dimensions={0} | all-to-all | bytes 262144 | tf_op jit(solution)/shard_map/all_to_all | solution.py:532
  74.8 1.1 %combine.1.after = bf16[32,16,128]{2,1,0:T(8,128)(2,1)} custom-call(bf16[512,128]{1,0:T(8,128)(2,1)S(1)} %bitcast.9), custom_call_target="tpu_custom_call" | custom-call | tf_op jit(solution)/shard_map/combine/pallas_call | solution.py:534
  75.9 3.8 %all-to-all-start.3 = ((bf16[32,16,128]{2,1,0:T(8,128)(2,1)}), bf16[32,16,128]{2,1,0:T(8,128)(2,1)S(1)}, u32[]{:S(2)}, u32[]{:S(2)}) async-start(bf16[32,16,128]{2,1,0:T(8,128)(2,1)} %combine.1.after), calls=%async_computation.3 | async-start | bytes 262144 | tf_op jit(solution)/shard_map/all_to_all | solution.py:543
  79.8 4.4 %write.1 = (bf16[24,512,128]{2,1,0:T(8,128)(2,1)}, bf16[24,512,128]{2,1,0:T(8,128)(2,1)}, bf16[8,64,128]{2,1,0:T(8,128)(2,1)S(1)}) custom-call(s32[24]{0:T(128)} %prior.3, s32[24]{0:T(128)} %accepted.3, bf16[32,16,384]{2,1,0:T(8,128)(2,1)S(1)} %all_to_all.20.joined, bf16[64,128]{1,0:T(8,128)(2,1)} %bitcast.18, ...), custom_call_target="tpu_custom_call", output_to_operand_aliasing={{0}: (12, {})} | custom-call | flops 2000000000 | bytes 100000 | tf_op jit(solution)/shard_map/write/pallas_call | solution.py:545
  84.2 6.6 %all-to-all-done.3 = bf16[32,16,128]{2,1,0:T(8,128)(2,1)S(1)} async-done(((bf16[32,16,128]{2,1,0:T(8,128)(2,1)}), bf16[32,16,128]{2,1,0:T(8,128)(2,1)S(1)}, u32[]{:S(2)}, u32[]{:S(2)}) %all-to-all-start.3) | async-done | bytes 131104 | tf_op jit(solution)/shard_map/all_to_all | solution.py:543
  90.8 0.9 output.1
Async XLA Ops:
  2.8 11.3 %copy-start.2 = (f32[24,2,512]{2,1,0:T(2,128)}, f32[24,2,512]{2,1,0:T(2,128)S(1)}, u32[]{:S(2)}) copy-start(f32[24,2,512]{2,1,0:T(2,128)S(1)} %get-tuple-element.11.biases) | copy-start | bytes 294916
  2.9 26.6 %all-to-all-start = ((bf16[32,16,384]{2,1,0:T(8,128)(2,1)}), bf16[32,16,384]{2,1,0:T(8,128)(2,1)S(1)}, u32[]{:S(2)}, u32[]{:S(2)}) async-start(bf16[32,16,384]{2,1,0:T(8,128)(2,1)} %get-tuple-element.10), calls=%async_computation | async-start | bytes 786432 | tf_op jit(solution)/shard_map/all_to_all | solution.py:490
  14.2 37.2 %copy-start = (bf16[24,512,128]{2,1,0:T(8,128)(2,1)S(1)}, bf16[24,512,128]{2,1,0:T(8,128)(2,1)}, u32[]{:S(2)}) copy-start(bf16[24,512,128]{2,1,0:T(8,128)(2,1)} %keys.1) | copy-start | bytes 9437188
  14.2 5.5 %collective-permute-start.3 = (bf16[64,128]{1,0:T(8,128)(2,1)}, bf16[64,128]{1,0:T(8,128)(2,1)S(1)}, u32[]{:S(2)}, u32[]{:S(2)}) collective-permute-start(bf16[64,128]{1,0:T(8,128)(2,1)} %bitcast.15), channel_id=1, source_target_pairs={{0,4},{1,5},{2,6},{3,7},{4,0},{5,1},{6,2},{7,3},{8,12},{9,13},{10,... | collective-permute-start | bytes 49160 | tf_op jit(solution)/shard_map/ppermute | solution.py:495
  16.6 4.1 %collective-permute-start.1 = (bf16[64,128]{1,0:T(8,128)(2,1)}, bf16[64,128]{1,0:T(8,128)(2,1)S(1)}, u32[]{:S(2)}, u32[]{:S(2)}) collective-permute-start(bf16[64,128]{1,0:T(8,128)(2,1)} %bitcast.16), channel_id=1, source_target_pairs={{0,2},{1,3},{2,0},{3,1},{4,6},{5,7},{6,4},{7,5},{8,10},{9,11},{10,... | collective-permute-start | bytes 49160 | tf_op jit(solution)/shard_map/ppermute | solution.py:495
  19.7 10.7 %copy-start.4 = (bf16[64,128]{1,0:T(8,128)(2,1)}, bf16[64,128]{1,0:T(8,128)(2,1)S(1)}, u32[]{:S(2)}) copy-start(bf16[64,128]{1,0:T(8,128)(2,1)S(1)} %collective-permute-done.3.w_4) | copy-start | bytes 49156
  19.7 3.7 %collective-permute-start.5 = (bf16[64,128]{1,0:T(8,128)(2,1)S(1)}, bf16[64,128]{1,0:T(8,128)(2,1)S(1)}, u32[]{:S(2)}, u32[]{:S(2)}) collective-permute-start(bf16[64,128]{1,0:T(8,128)(2,1)S(1)} %collective-permute-done.3.w_4), channel_id=1, source_target_pairs={{0,2},{1,3},{2,0},{3,1},{4,6},{5,7},{6,4},{7,5},{8,10},{9,11},{10,... | collective-permute-start | bytes 49160 | tf_op jit(solution)/shard_map/ppermute | solution.py:495
  20.2 3.3 %collective-permute-start = (bf16[64,128]{1,0:T(8,128)(2,1)}, bf16[64,128]{1,0:T(8,128)(2,1)S(1)}, u32[]{:S(2)}, u32[]{:S(2)}) collective-permute-start(bf16[64,128]{1,0:T(8,128)(2,1)} %bitcast.17), channel_id=1, source_target_pairs={{0,1},{1,0},{2,3},{3,2},{4,5},{5,4},{6,7},{7,6},{8,9},{9,8},{10,11... | collective-permute-start | bytes 49160 | tf_op jit(solution)/shard_map/ppermute | solution.py:495
  20.2 3.3 %collective-permute-start.4 = (bf16[64,128]{1,0:T(8,128)(2,1)S(1)}, bf16[64,128]{1,0:T(8,128)(2,1)S(1)}, u32[]{:S(2)}, u32[]{:S(2)}) collective-permute-start(bf16[64,128]{1,0:T(8,128)(2,1)S(1)} %collective-permute-done.3.w_4), channel_id=1, source_target_pairs={{0,1},{1,0},{2,3},{3,2},{4,5},{5,4},{6,7},{7,6},{8,9},{9,8},{10,11... | collective-permute-start | bytes 49160 | tf_op jit(solution)/shard_map/ppermute | solution.py:495
  20.7 2.8 %copy-start.5 = (bf16[64,128]{1,0:T(8,128)(2,1)}, bf16[64,128]{1,0:T(8,128)(2,1)S(1)}, u32[]{:S(2)}) copy-start(bf16[64,128]{1,0:T(8,128)(2,1)S(1)} %collective-permute-done.1.w_2) | copy-start | bytes 49156
  20.7 2.8 %collective-permute-start.2 = (bf16[64,128]{1,0:T(8,128)(2,1)S(1)}, bf16[64,128]{1,0:T(8,128)(2,1)S(1)}, u32[]{:S(2)}, u32[]{:S(2)}) collective-permute-start(bf16[64,128]{1,0:T(8,128)(2,1)S(1)} %collective-permute-done.1.w_2), channel_id=1, source_target_pairs={{0,1},{1,0},{2,3},{3,2},{4,5},{5,4},{6,7},{7,6},{8,9},{9,8},{10,11... | collective-permute-start | bytes 49160 | tf_op jit(solution)/shard_map/ppermute | solution.py:495
  23.5 0.6 copy-start.6
  23.5 1.3 %collective-permute-start.6 = (bf16[64,128]{1,0:T(8,128)(2,1)S(1)}, bf16[64,128]{1,0:T(8,128)(2,1)}, u32[]{:S(2)}, u32[]{:S(2)}) collective-permute-start(bf16[64,128]{1,0:T(8,128)(2,1)S(1)} %collective-permute-done.5.w_6), channel_id=1, source_target_pairs={{0,1},{1,0},{2,3},{3,2},{4,5},{5,4},{6,7},{7,6},{8,9},{9,8},{10,11... | collective-permute-start | bytes 49160 | tf_op jit(solution)/shard_map/ppermute | solution.py:495
  23.5 0.6 copy-start.7
  23.5 0.6 copy-start.8
  24.1 0.6 copy-start.9
  29.5 21.9 %copy-start.1 = (bf16[24,512,128]{2,1,0:T(8,128)(2,1)S(1)}, bf16[24,512,128]{2,1,0:T(8,128)(2,1)}, u32[]{:S(2)}) copy-start(bf16[24,512,128]{2,1,0:T(8,128)(2,1)} %values_in.1) | copy-start | bytes 9437188
  29.5 21.9 %copy-start.3 = (f32[24,2,512]{2,1,0:T(2,128)S(1)}, f32[24,2,512]{2,1,0:T(2,128)}, u32[]{:S(2)}) copy-start(f32[24,2,512]{2,1,0:T(2,128)} %copy-done.2) | copy-start | bytes 294916
  75.9 14.9 %all-to-all-start.3 = ((bf16[32,16,128]{2,1,0:T(8,128)(2,1)}), bf16[32,16,128]{2,1,0:T(8,128)(2,1)S(1)}, u32[]{:S(2)}, u32[]{:S(2)}) async-start(bf16[32,16,128]{2,1,0:T(8,128)(2,1)} %combine.1.after), calls=%async_computation.3 | async-start | bytes 262144 | tf_op jit(solution)/shard_map/all_to_all | solution.py:543

commit v8 on v6

--- a/solution.py
+++ b/solution.py
@@ -310,10 +310,10 @@
         out[k] = block
 
 
-def output_kernel(shared, w_0, w_1, w_2, w_4, out, rows):
+def output_kernel(shared, w_even, w_odd, out, rows):
     tp = lax.axis_index("tp")
     rows[...] = shared[...].astype(f32)
-    near = (w_0[...], w_1[...], w_2[0], w_2[1], w_4[0], w_4[1], w_4[2], w_4[3])
+    near = (w_even[0], w_odd[0], w_even[2], w_odd[2], w_even[1], w_odd[1], w_even[3], w_odd[3])
     near = [w.astype(f32) for w in near]
     for bit in (1, 2, 4):
         swap = (tp & bit) != 0
@@ -337,7 +337,7 @@
     out[...] = total.astype(bf16)
 
 
-def join_kernel(first, second, out):
+def join_kernel(first, second, after, out):
     count = first.shape[0]
     out[0:count] = first[...]
     out[count:] = second[...]
@@ -491,24 +491,23 @@
 
     tp_count = lax.axis_size("tp")
 
-    def gathered(name, *pieces):
+    def gathered(name, first, second, after, out_shape):
         return pl.pallas_call(
             join_kernel,
-            out_shape=pltpu.VMEM((sum(len(p) for p in pieces), *pieces[0].shape[1:]), bf16),
-            in_specs=[VM, VM],
+            out_shape=out_shape((2 * len(first), *first.shape[1:]), bf16),
+            in_specs=[VM, VM, ANY],
             out_specs=VM,
             compiler_params=limit(2),
             name=name,
-        )(*pieces)
+        )(*far(first, second, after))
 
     def across(x, bit):
         return lax.ppermute(x, "tp", [(i, i ^ bit) for i in range(tp_count)])
 
     w_0 = w_out.T
-    w_1 = across(w_0, 1)
-    w_pair = gathered("pair", *far(w_0[None]), *near(w_1[None]))
+    w_4 = across(w_0, 4)
+    w_pair = gathered("pair", w_0[None], w_4[None], parts, jax.ShapeDtypeStruct)
     w_2 = across(w_pair, 2)
-    w_4 = across(gathered("four", *near(w_pair, w_2)), 4)
 
     block = pl.pallas_call(
         share_kernel,
@@ -520,7 +519,7 @@
             flops=10_000_000_000, bytes_accessed=800_000, transcendentals=0
         ),
         name="share",
-    )(*far(gate_bias), *near(arrived), *far(w_4))
+    )(*far(gate_bias), *near(arrived), *far(w_2))
     joined = lax.all_to_all(block, KV, 0, 0, tiled=True)
 
     sent, keys_copy = pl.pallas_call(
@@ -552,6 +551,8 @@
         name="combine",
     )(*near(pieces.reshape(512, WIDTH)))
     shared = lax.all_to_all(combined, KV, 0, 0, tiled=True)
+    w_even = gathered("four", w_pair, w_2, combined, pltpu.VMEM)
+    w_odd = across(w_even, 1)
 
     keys_out, values_out = pl.pallas_call(
         write_kernel,
@@ -581,12 +582,12 @@
     mixed_rows = pl.pallas_call(
         output_kernel,
         out_shape=jax.ShapeDtypeStruct((48, 64), bf16),
-        in_specs=[VM] * 5,
+        in_specs=[VM] * 3,
         out_specs=VM,
         scratch_shapes=[pltpu.VMEM((512, WIDTH), f32)],
         compiler_params=limit(8),
         name="output",
-    )(*near(shared.reshape(512, WIDTH), w_0, w_1, w_2, w_4))
+    )(*near(shared.reshape(512, WIDTH), w_even, w_odd))
     return (mixed_rows, keys_out, values_out)
 
 

time: 93 us -> 90.6 us (0.974)
  waiting for transfers between devices: 18.3 us -> 16.9 us
  blocking collectives: 39.6 us -> 38.3 us
    ppermute x3, waiting for transfers between devices: 8.43 us -> 6.66 us  [across(): return lax.ppermute(x, 'tp', [(i, i ^ bit) for i in range(tp_count)])]
    all_to_all x1, waiting for transfers between devices: 3.18 us -> 4.31 us  [shards(): arrived = lax.all_to_all(parts, KV, 0, 0, tiled=True)]
    all_to_all x1, blocking collectives: 20.2 us -> 19.3 us  [shards(): joined = lax.all_to_all(block, KV, 0, 0, tiled=True)]
  transfers between devices with their start and end apart: 5 -> 5, of which waited for: 5 -> 4; matrix products, arithmetic and copies ran while one was open for 0% -> 0% of each run, Pallas kernels for 6% -> 6%
where the time goes in v8:
time: 90.6 us; the launch traced here: 89.6 us
  blocking collectives  38.3 us (42%)
  starting transfers between devices  18.1 us (20%)
  waiting for transfers between devices  16.9 us (19%)
  Pallas kernels  14.9 us (16%)
    all_to_all x1, blocking collectives, shards(): joined = lax.all_to_all(block, KV, 0, 0, tiled=True)  19.3 us
    all_to_all x1, blocking collectives, shards(): lax.all_to_all(sent.reshape(256, 2, WIDTH), (*KV, 'tp'), 0, 0, tiled=True)  19 us
    all_to_all x1, starting transfers between devices, shards(): arrived = lax.all_to_all(parts, KV, 0, 0, tiled=True)  11.3 us
    ppermute x3, waiting for transfers between devices, across(): return lax.ppermute(x, 'tp', [(i, i ^ bit) for i in range(tp_count)])  6.66 us
    all_to_all x1, waiting for transfers between devices, shards(): shared = lax.all_to_all(combined, KV, 0, 0, tiled=True)  5.98 us
    all_to_all x1, waiting for transfers between devices, shards(): arrived = lax.all_to_all(parts, KV, 0, 0, tiled=True)  4.31 us
    pallas_call x1, Pallas kernels, shards(): pl.pallas_call(write_kernel, out_shape=(cache, cache), in_specs=[SM, SM,...  4.21 us
    pallas_call x1, Pallas kernels, shards(): pl.pallas_call(attention_kernel, out_shape=(pltpu.VMEM((512, WIDTH), bf16...  4.02 us
  transfers between devices with their start and end apart: 5, of which 4 were waited for; matrix products, arithmetic and copies ran while one was open for 0% of the time, Pallas kernels for 6%

profile of v8, /device:TPU:8, one launch (start us, length us, event | category | flops | bytes accessed | tf_op | source)
XLA Modules:
  0.0 89.6 jit_solution(17365116192938033825)
XLA Ops:
  0.6 2.2 %project.1 = (bf16[32,16,384]{2,1,0:T(8,128)(2,1)}, f32[24,2,512]{2,1,0:T(2,128)S(1)}) custom-call(s32[24]{0:T(128)} %prior.3, s32[24]{0:T(128)} %accepted.3, bf16[64,384]{1,0:T(8,128)(2,1)} %bitcast.15, f32[1,64]{1,0:T(1,128)} %bitcast.20, bf16[64,128]{1,0:T(8,128)(2,1)} %w_q.1, bf16[64,128]{1,0:T(8,128)(2,1)} %w_k.1, bf16[64,128]{1,0:T(8,128)(2,1)} %w_v.1, ...), custom_call_target="tpu_custom_call" | custom-call | tf_op jit(solution)/shard_map/project/pallas_call | solution.py:469
  2.9 0.0 copy-start.3
  2.9 11.3 %all-to-all-start = ((bf16[32,16,384]{2,1,0:T(8,128)(2,1)}), bf16[32,16,384]{2,1,0:T(8,128)(2,1)S(1)}, u32[]{:S(2)}, u32[]{:S(2)}) async-start(bf16[32,16,384]{2,1,0:T(8,128)(2,1)} %get-tuple-element.9.after), calls=%async_computation | async-start | bytes 786432 | tf_op jit(solution)/shard_map/all_to_all | solution.py:490
  14.2 2.4 %collective-permute-start = (bf16[64,128]{1,0:T(8,128)(2,1)}, bf16[64,128]{1,0:T(8,128)(2,1)S(1)}, u32[]{:S(2)}, u32[]{:S(2)}) collective-permute-start(bf16[64,128]{1,0:T(8,128)(2,1)} %bitcast.16), channel_id=1, source_target_pairs={{0,4},{1,5},{2,6},{3,7},{4,0},{5,1},{6,2},{7,3},{8,12},{9,13},{10,... | collective-permute-start | bytes 49160 | tf_op jit(solution)/shard_map/ppermute | solution.py:505
  16.6 3.2 %collective-permute-done = bf16[64,128]{1,0:T(8,128)(2,1)S(1)} collective-permute-done((bf16[64,128]{1,0:T(8,128)(2,1)}, bf16[64,128]{1,0:T(8,128)(2,1)S(1)}, u32[]{:S(2)}, u32[]{:S(2)}) %collective-permute-start) | collective-permute-done | bytes 16416 | tf_op jit(solution)/shard_map/ppermute | solution.py:505
  19.7 0.0 copy-start.5
  19.7 0.0 copy-done.3
  19.7 0.6 copy-done.5
  20.3 0.7 pair.1.first
  21.1 0.0 copy-start.2
  21.1 0.0 copy-start
  21.1 0.5 collective-permute-start.1
  21.6 0.1 copy-done.2
  21.7 3.5 %collective-permute-done.1.after_w.second = bf16[2,64,128]{2,1,0:T(8,128)(2,1)} collective-permute-done((bf16[2,64,128]{2,1,0:T(8,128)(2,1)S(1)}, bf16[2,64,128]{2,1,0:T(8,128)(2,1)}, u32[]{:S(2)}, u32[]{:S(2)}) %collective-permute-start.1) | collective-permute-done | bytes 32800 | tf_op jit(solution)/shard_map/ppermute | solution.py:505
  25.2 4.3 %all-to-all-done.parts = bf16[32,16,384]{2,1,0:T(8,128)(2,1)S(1)} async-done(((bf16[32,16,384]{2,1,0:T(8,128)(2,1)}), bf16[32,16,384]{2,1,0:T(8,128)(2,1)S(1)}, u32[]{:S(2)}, u32[]{:S(2)}) %all-to-all-start) | async-done | bytes 393248 | tf_op jit(solution)/shard_map/all_to_all | solution.py:490
  29.5 0.0 copy-start.1
  29.5 0.0 copy-start.4
  29.5 0.9 %share.1 = bf16[32,16,384]{2,1,0:T(8,128)(2,1)S(1)} custom-call(f32[16]{0:T(128)} %bias.1, bf16[32,16,384]{2,1,0:T(8,128)(2,1)S(1)} %all-to-all-done.parts, bf16[2,64,128]{2,1,0:T(8,128)(2,1)} %collective-permute-done.1.after_w.second), custom_call_target="tpu_custom_call" | custom-call | flops 10000000000 | bytes 800000 | tf_op jit(solution)/shard_map/share/pallas_call | solution.py:512
  30.4 19.3 %all_to_all.20.joined = bf16[32,16,384]{2,1,0:T(8,128)(2,1)S(1)} all-to-all(bf16[32,16,384]{2,1,0:T(8,128)(2,1)S(1)} %share.1), channel_id=1, replica_groups=mesh['kv_0'=8,'kv_1'=4,'tp'=8] {'kv_0','kv_1'}, dimensions={0} | all-to-all | bytes 786432 | tf_op jit(solution)/shard_map/all_to_all | solution.py:523
  49.7 0.0 copy-done
  49.7 0.0 copy-done.1
  49.7 0.0 copy-done.4
  49.7 4.0 %attention.1 = (bf16[512,128]{1,0:T(8,128)(2,1)S(1)}, bf16[24,512,128]{2,1,0:T(8,128)(2,1)}) custom-call(s32[16,24]{1,0:T(8,128)} %bitcast.19, bf16[32,16,384]{2,1,0:T(8,128)(2,1)S(1)} %all_to_all.20.joined, f32[24,2,512]{2,1,0:T(2,128)S(1)} %copy-done.4, bf16[24,512,128]{2,1,0:T(8,128)(2,1)S(1)} %copy-done, bf16[24,512,128]{2,1,0:T(8,128)(2,1)S(1)} %copy-done.1), custom_call_target="tpu_custom_call" | custom-call | tf_op jit(solution)/shard_map/attention/pallas_call | solution.py:525
  53.7 19.0 %all_to_all.21 = bf16[256,2,128]{2,1,0:T(2,128)(2,1)S(1)} all-to-all(bf16[256,2,128]{2,1,0:T(2,128)(2,1)S(1)} %bitcast.13), channel_id=1, replica_groups=mesh['kv_0'=8,'kv_1'=4,'tp'=8] {'kv_0','kv_1','tp'}, dimensions={0} | all-to-all | bytes 262144 | tf_op jit(solution)/shard_map/all_to_all | solution.py:542
  72.7 1.1 %combine.1.after = bf16[32,16,128]{2,1,0:T(8,128)(2,1)} custom-call(bf16[512,128]{1,0:T(8,128)(2,1)S(1)} %bitcast.12), custom_call_target="tpu_custom_call" | custom-call | tf_op jit(solution)/shard_map/combine/pallas_call | solution.py:544
  73.8 3.8 %all-to-all-start.3 = ((bf16[32,16,128]{2,1,0:T(8,128)(2,1)}), bf16[32,16,128]{2,1,0:T(8,128)(2,1)S(1)}, u32[]{:S(2)}, u32[]{:S(2)}) async-start(bf16[32,16,128]{2,1,0:T(8,128)(2,1)} %combine.1.after), calls=%async_computation.3 | async-start | bytes 262144 | tf_op jit(solution)/shard_map/all_to_all | solution.py:553
  77.6 0.8 four.1.w_even
  78.4 0.0 collective-permute-start.2
  78.5 4.2 %write.1 = (bf16[24,512,128]{2,1,0:T(8,128)(2,1)}, bf16[24,512,128]{2,1,0:T(8,128)(2,1)}) custom-call(s32[24]{0:T(128)} %prior.3, s32[24]{0:T(128)} %accepted.3, bf16[32,16,384]{2,1,0:T(8,128)(2,1)S(1)} %all_to_all.20.joined, bf16[32,16,128]{2,1,0:T(8,128)(2,1)} %combine.1.after, ...), custom_call_target="tpu_custom_call", output_to_operand_aliasing={{0}: (4, {})} | custom-call | flops 2000000000 | bytes 100000 | tf_op jit(solution)/shard_map/write/pallas_call | solution.py:557
  82.7 0.0 collective-permute-done.2.w_odd
  82.7 6.0 %all-to-all-done.3 = bf16[32,16,128]{2,1,0:T(8,128)(2,1)S(1)} async-done(((bf16[32,16,128]{2,1,0:T(8,128)(2,1)}), bf16[32,16,128]{2,1,0:T(8,128)(2,1)S(1)}, u32[]{:S(2)}, u32[]{:S(2)}) %all-to-all-start.3) | async-done | bytes 131104 | tf_op jit(solution)/shard_map/all_to_all | solution.py:553
  88.7 0.9 %output.1 = bf16[48,64]{1,0:T(8,128)(2,1)} custom-call(bf16[512,128]{1,0:T(8,128)(2,1)S(1)} %bitcast.11, bf16[4,64,128]{2,1,0:T(8,128)(2,1)S(1)} %four.1.w_even, bf16[4,64,128]{2,1,0:T(8,128)(2,1)S(1)} %collective-permute-done.2.w_odd), custom_call_target="tpu_custom_call" | custom-call | tf_op jit(solution)/shard_map/output/pallas_call | solution.py:582
Async XLA Ops:
  2.9 16.9 %copy-start.3 = (f32[24,2,512]{2,1,0:T(2,128)}, f32[24,2,512]{2,1,0:T(2,128)S(1)}, u32[]{:S(2)}) copy-start(f32[24,2,512]{2,1,0:T(2,128)S(1)} %get-tuple-element.10.biases) | copy-start | bytes 294916
  2.9 26.6 %all-to-all-start = ((bf16[32,16,384]{2,1,0:T(8,128)(2,1)}), bf16[32,16,384]{2,1,0:T(8,128)(2,1)S(1)}, u32[]{:S(2)}, u32[]{:S(2)}) async-start(bf16[32,16,384]{2,1,0:T(8,128)(2,1)} %get-tuple-element.9.after), calls=%async_computation | async-start | bytes 786432 | tf_op jit(solution)/shard_map/all_to_all | solution.py:490
  14.2 5.5 %collective-permute-start = (bf16[64,128]{1,0:T(8,128)(2,1)}, bf16[64,128]{1,0:T(8,128)(2,1)S(1)}, u32[]{:S(2)}, u32[]{:S(2)}) collective-permute-start(bf16[64,128]{1,0:T(8,128)(2,1)} %bitcast.16), channel_id=1, source_target_pairs={{0,4},{1,5},{2,6},{3,7},{4,0},{5,1},{6,2},{7,3},{8,12},{9,13},{10,... | collective-permute-start | bytes 49160 | tf_op jit(solution)/shard_map/ppermute | solution.py:505
  19.7 0.6 copy-start.5
  21.1 0.6 copy-start.2
  21.1 28.6 %copy-start = (bf16[24,512,128]{2,1,0:T(8,128)(2,1)S(1)}, bf16[24,512,128]{2,1,0:T(8,128)(2,1)}, u32[]{:S(2)}) copy-start(bf16[24,512,128]{2,1,0:T(8,128)(2,1)} %keys.1) | copy-start | bytes 9437188
  21.1 4.1 %collective-permute-start.1 = (bf16[2,64,128]{2,1,0:T(8,128)(2,1)S(1)}, bf16[2,64,128]{2,1,0:T(8,128)(2,1)}, u32[]{:S(2)}, u32[]{:S(2)}) collective-permute-start(bf16[2,64,128]{2,1,0:T(8,128)(2,1)S(1)} %pair.1.first), channel_id=1, source_target_pairs={{0,2},{1,3},{2,0},{3,1},{4,6},{5,7},{6,4},{7,5},{8,10},{9,11},{10,... | collective-permute-start | bytes 98312 | tf_op jit(solution)/shard_map/ppermute | solution.py:505
  29.5 20.2 %copy-start.1 = (bf16[24,512,128]{2,1,0:T(8,128)(2,1)S(1)}, bf16[24,512,128]{2,1,0:T(8,128)(2,1)}, u32[]{:S(2)}) copy-start(bf16[24,512,128]{2,1,0:T(8,128)(2,1)} %values_in.1) | copy-start | bytes 9437188
  29.5 20.2 %copy-start.4 = (f32[24,2,512]{2,1,0:T(2,128)S(1)}, f32[24,2,512]{2,1,0:T(2,128)}, u32[]{:S(2)}) copy-start(f32[24,2,512]{2,1,0:T(2,128)} %copy-done.3) | copy-start | bytes 294916
  73.8 14.9 %all-to-all-start.3 = ((bf16[32,16,128]{2,1,0:T(8,128)(2,1)}), bf16[32,16,128]{2,1,0:T(8,128)(2,1)S(1)}, u32[]{:S(2)}, u32[]{:S(2)}) async-start(bf16[32,16,128]{2,1,0:T(8,128)(2,1)} %combine.1.after), calls=%async_computation.3 | async-start | bytes 262144 | tf_op jit(solution)/shard_map/all_to_all | solution.py:553
  78.4 4.3 %collective-permute-start.2 = (bf16[4,64,128]{2,1,0:T(8,128)(2,1)S(1)}, bf16[4,64,128]{2,1,0:T(8,128)(2,1)S(1)}, u32[]{:S(2)}, u32[]{:S(2)}) collective-permute-start(bf16[4,64,128]{2,1,0:T(8,128)(2,1)S(1)} %four.1.w_even), channel_id=1, source_target_pairs={{0,1},{1,0},{2,3},{3,2},{4,5},{5,4},{6,7},{7,6},{8,9},{9,8},{10,11... | collective-permute-start | bytes 196616 | tf_op jit(solution)/shard_map/ppermute | solution.py:505

commit v9 on v8

--- a/solution.py
+++ b/solution.py
@@ -93,7 +93,7 @@
     out[STATS + 1 :] = jnp.zeros((N_KV - STATS - 1, PROPS, ROWS), bf16)
 
 
-def share_kernel(bias, parts, after_w, out):
+def share_kernel(bias, parts, after_2, after_6, out):
     kv, tp = lax.axis_index(KV), lax.axis_index("tp")
     total = jnp.zeros((PROPS, ROWS), f32)
     for k in range(N_KV):
@@ -337,10 +337,9 @@
     out[...] = total.astype(bf16)
 
 
-def join_kernel(first, second, after, out):
-    count = first.shape[0]
-    out[0:count] = first[...]
-    out[count:] = second[...]
+def join_kernel(first, second, third, fourth, after, out):
+    for n, w in enumerate((first, second, third, fourth)):
+        out[n] = w[...]
 
 
 def write_kernel(
@@ -491,35 +490,25 @@
 
     tp_count = lax.axis_size("tp")
 
-    def gathered(name, first, second, after, out_shape):
-        return pl.pallas_call(
-            join_kernel,
-            out_shape=out_shape((2 * len(first), *first.shape[1:]), bf16),
-            in_specs=[VM, VM, ANY],
-            out_specs=VM,
-            compiler_params=limit(2),
-            name=name,
-        )(*far(first, second, after))
-
     def across(x, bit):
         return lax.ppermute(x, "tp", [(i, i ^ bit) for i in range(tp_count)])
 
     w_0 = w_out.T
     w_4 = across(w_0, 4)
-    w_pair = gathered("pair", w_0[None], w_4[None], parts, jax.ShapeDtypeStruct)
-    w_2 = across(w_pair, 2)
+    w_2 = across(w_0, 2)
+    w_6 = across(w_4, 2)
 
     block = pl.pallas_call(
         share_kernel,
         out_shape=pltpu.VMEM((N_KV, PROPS, ROWS), bf16),
-        in_specs=[SM, VM, ANY],
+        in_specs=[SM, VM, ANY, ANY],
         out_specs=VM,
         compiler_params=limit(8),
         cost_estimate=pl.CostEstimate(
             flops=10_000_000_000, bytes_accessed=800_000, transcendentals=0
         ),
         name="share",
-    )(*far(gate_bias), *near(arrived), *far(w_2))
+    )(*far(gate_bias), *near(arrived), *far(w_2, w_6))
     joined = lax.all_to_all(block, KV, 0, 0, tiled=True)
 
     sent, keys_copy = pl.pallas_call(
@@ -551,7 +540,14 @@
         name="combine",
     )(*near(pieces.reshape(512, WIDTH)))
     shared = lax.all_to_all(combined, KV, 0, 0, tiled=True)
-    w_even = gathered("four", w_pair, w_2, combined, pltpu.VMEM)
+    w_even = pl.pallas_call(
+        join_kernel,
+        out_shape=pltpu.VMEM((4, *w_0.shape), bf16),
+        in_specs=[VM] * 4 + [ANY],
+        out_specs=VM,
+        compiler_params=limit(2),
+        name="four",
+    )(*far(w_0, w_4, w_2, w_6, combined))
     w_odd = across(w_even, 1)
 
     keys_out, values_out = pl.pallas_call(

time: 90.6 us -> 90.9 us (level)
  starting transfers between devices: 18.1 us -> 19.4 us
    ppermute x3 -> x4, waiting for transfers between devices: 6.66 us -> 4.61 us  [across(): return lax.ppermute(x, 'tp', [(i, i ^ bit) for i in range(tp_count)])]
    all_to_all x1, waiting for transfers between devices: 4.31 us -> 5.88 us  [shards(): arrived = lax.all_to_all(parts, KV, 0, 0, tiled=True)]
    ppermute x3 -> x4, starting transfers between devices: 2.94 us -> 4.22 us  [across(): return lax.ppermute(x, 'tp', [(i, i ^ bit) for i in range(tp_count)])]
  transfers between devices with their start and end apart: 5 -> 6, of which waited for: 4 -> 5; matrix products, arithmetic and copies ran while one was open for 0% -> 0% of each run, Pallas kernels for 6% -> 6%
where the time goes in v9:
time: 90.9 us; the launch traced here: 89.6 us
  blocking collectives  38.3 us (42%)
  starting transfers between devices  19.4 us (21%)
  waiting for transfers between devices  16.5 us (18%)
  Pallas kernels  14.1 us (16%)
    all_to_all x1, blocking collectives, shards(): lax.all_to_all(sent.reshape(256, 2, WIDTH), (*KV, 'tp'), 0, 0, tiled=True)  19.3 us
    all_to_all x1, blocking collectives, shards(): joined = lax.all_to_all(block, KV, 0, 0, tiled=True)  18.9 us
    all_to_all x1, starting transfers between devices, shards(): arrived = lax.all_to_all(parts, KV, 0, 0, tiled=True)  11.3 us
    all_to_all x1, waiting for transfers between devices, shards(): shared = lax.all_to_all(combined, KV, 0, 0, tiled=True)  5.98 us
    all_to_all x1, waiting for transfers between devices, shards(): arrived = lax.all_to_all(parts, KV, 0, 0, tiled=True)  5.88 us
    ppermute x4, waiting for transfers between devices, across(): return lax.ppermute(x, 'tp', [(i, i ^ bit) for i in range(tp_count)])  4.61 us
    ppermute x4, starting transfers between devices, across(): return lax.ppermute(x, 'tp', [(i, i ^ bit) for i in range(tp_count)])  4.22 us
    pallas_call x1, Pallas kernels, shards(): pl.pallas_call(write_kernel, out_shape=(cache, cache), in_specs=[SM, SM,...  4.21 us
  transfers between devices with their start and end apart: 6, of which 5 were waited for; matrix products, arithmetic and copies ran while one was open for 0% of the time, Pallas kernels for 6%

profile of v9, /device:TPU:8, one launch (start us, length us, event | category | flops | bytes accessed | tf_op | source)
XLA Modules:
  0.0 89.6 jit_solution(1128796882040889529)
XLA Ops:
  0.6 2.2 %project.1 = (bf16[32,16,384]{2,1,0:T(8,128)(2,1)}, f32[24,2,512]{2,1,0:T(2,128)S(1)}) custom-call(s32[24]{0:T(128)} %prior.3, s32[24]{0:T(128)} %accepted.3, bf16[64,384]{1,0:T(8,128)(2,1)} %bitcast.12, f32[1,64]{1,0:T(1,128)} %bitcast.17, bf16[64,128]{1,0:T(8,128)(2,1)} %w_q.1, bf16[64,128]{1,0:T(8,128)(2,1)} %w_k.1, bf16[64,128]{1,0:T(8,128)(2,1)} %w_v.1, ...), custom_call_target="tpu_custom_call" | custom-call | tf_op jit(solution)/shard_map/project/pallas_call | solution.py:468
  2.9 0.0 copy-start.2
  2.9 11.3 %all-to-all-start = ((bf16[32,16,384]{2,1,0:T(8,128)(2,1)}), bf16[32,16,384]{2,1,0:T(8,128)(2,1)S(1)}, u32[]{:S(2)}, u32[]{:S(2)}) async-start(bf16[32,16,384]{2,1,0:T(8,128)(2,1)} %get-tuple-element.9), calls=%async_computation | async-start | bytes 786432 | tf_op jit(solution)/shard_map/all_to_all | solution.py:489
  14.2 0.0 copy-done.2
  14.2 0.0 copy-start
  14.2 2.4 %collective-permute-start.1 = (bf16[64,128]{1,0:T(8,128)(2,1)}, bf16[64,128]{1,0:T(8,128)(2,1)S(1)}, u32[]{:S(2)}, u32[]{:S(2)}) collective-permute-start(bf16[64,128]{1,0:T(8,128)(2,1)} %bitcast.13), channel_id=1, source_target_pairs={{0,4},{1,5},{2,6},{3,7},{4,0},{5,1},{6,2},{7,3},{8,12},{9,13},{10,... | collective-permute-start | bytes 49160 | tf_op jit(solution)/shard_map/ppermute | solution.py:494
  16.6 1.3 %collective-permute-start = (bf16[64,128]{1,0:T(8,128)(2,1)}, bf16[64,128]{1,0:T(8,128)(2,1)S(1)}, u32[]{:S(2)}, u32[]{:S(2)}) collective-permute-start(bf16[64,128]{1,0:T(8,128)(2,1)} %bitcast.14), channel_id=1, source_target_pairs={{0,2},{1,3},{2,0},{3,1},{4,6},{5,7},{6,4},{7,5},{8,10},{9,11},{10,... | collective-permute-start | bytes 49160 | tf_op jit(solution)/shard_map/ppermute | solution.py:494
  17.9 1.8 %collective-permute-done.1.second = bf16[64,128]{1,0:T(8,128)(2,1)S(1)} collective-permute-done((bf16[64,128]{1,0:T(8,128)(2,1)}, bf16[64,128]{1,0:T(8,128)(2,1)S(1)}, u32[]{:S(2)}, u32[]{:S(2)}) %collective-permute-start.1) | collective-permute-done | bytes 16416 | tf_op jit(solution)/shard_map/ppermute | solution.py:494
  19.7 0.0 copy-start.4
  19.7 0.4 collective-permute-start.2
  20.2 0.3 collective-permute-done.after_2.third
  20.5 0.0 copy-start.5
  20.5 0.6 copy-done.5
  21.1 2.5 %collective-permute-done.2.after_6.fourth = bf16[64,128]{1,0:T(8,128)(2,1)} collective-permute-done((bf16[64,128]{1,0:T(8,128)(2,1)S(1)}, bf16[64,128]{1,0:T(8,128)(2,1)}, u32[]{:S(2)}, u32[]{:S(2)}) %collective-permute-start.2) | collective-permute-done | bytes 16416 | tf_op jit(solution)/shard_map/ppermute | solution.py:494
  23.6 5.9 %all-to-all-done.parts = bf16[32,16,384]{2,1,0:T(8,128)(2,1)S(1)} async-done(((bf16[32,16,384]{2,1,0:T(8,128)(2,1)}), bf16[32,16,384]{2,1,0:T(8,128)(2,1)S(1)}, u32[]{:S(2)}, u32[]{:S(2)}) %all-to-all-start) | async-done | bytes 393248 | tf_op jit(solution)/shard_map/all_to_all | solution.py:489
  29.5 0.0 copy-start.1
  29.5 0.0 copy-start.3
  29.5 0.9 %share.1 = bf16[32,16,384]{2,1,0:T(8,128)(2,1)S(1)} custom-call(f32[16]{0:T(128)} %bias.1, bf16[32,16,384]{2,1,0:T(8,128)(2,1)S(1)} %all-to-all-done.parts, bf16[64,128]{1,0:T(8,128)(2,1)} %copy-done.5, bf16[64,128]{1,0:T(8,128)(2,1)} %collective-permute-done.2.after_6.fourth), custom_call_target="tpu_custom_call" | custom-call | flops 10000000000 | bytes 800000 | tf_op jit(solution)/shard_map/share/pallas_call | solution.py:501
  30.4 0.0 copy-done.4
  30.4 18.9 %all_to_all.20.joined = bf16[32,16,384]{2,1,0:T(8,128)(2,1)S(1)} all-to-all(bf16[32,16,384]{2,1,0:T(8,128)(2,1)S(1)} %share.1), channel_id=1, replica_groups=mesh['kv_0'=8,'kv_1'=4,'tp'=8] {'kv_0','kv_1'}, dimensions={0} | all-to-all | bytes 786432 | tf_op jit(solution)/shard_map/all_to_all | solution.py:512
  49.3 0.0 copy-done
  49.3 0.0 copy-done.1
  49.3 0.0 copy-done.3
  49.3 4.0 %attention.1 = (bf16[512,128]{1,0:T(8,128)(2,1)S(1)}, bf16[24,512,128]{2,1,0:T(8,128)(2,1)}) custom-call(s32[16,24]{1,0:T(8,128)} %bitcast.16, bf16[32,16,384]{2,1,0:T(8,128)(2,1)S(1)} %all_to_all.20.joined, f32[24,2,512]{2,1,0:T(2,128)S(1)} %copy-done.3, bf16[24,512,128]{2,1,0:T(8,128)(2,1)S(1)} %copy-done, bf16[24,512,128]{2,1,0:T(8,128)(2,1)S(1)} %copy-done.1), custom_call_target="tpu_custom_call" | custom-call | tf_op jit(solution)/shard_map/attention/pallas_call | solution.py:514
  53.4 19.3 %all_to_all.21 = bf16[256,2,128]{2,1,0:T(2,128)(2,1)S(1)} all-to-all(bf16[256,2,128]{2,1,0:T(2,128)(2,1)S(1)} %bitcast.10), channel_id=1, replica_groups=mesh['kv_0'=8,'kv_1'=4,'tp'=8] {'kv_0','kv_1','tp'}, dimensions={0} | all-to-all | bytes 262144 | tf_op jit(solution)/shard_map/all_to_all | solution.py:531
  72.7 1.1 %combine.1.after = bf16[32,16,128]{2,1,0:T(8,128)(2,1)} custom-call(bf16[512,128]{1,0:T(8,128)(2,1)S(1)} %bitcast.9), custom_call_target="tpu_custom_call" | custom-call | tf_op jit(solution)/shard_map/combine/pallas_call | solution.py:533
  73.8 3.9 %all-to-all-start.3 = ((bf16[32,16,128]{2,1,0:T(8,128)(2,1)}), bf16[32,16,128]{2,1,0:T(8,128)(2,1)S(1)}, u32[]{:S(2)}, u32[]{:S(2)}) async-start(bf16[32,16,128]{2,1,0:T(8,128)(2,1)} %combine.1.after), calls=%async_computation.3 | async-start | bytes 262144 | tf_op jit(solution)/shard_map/all_to_all | solution.py:542
  77.6 0.8 four.1.w_even
  78.4 0.0 collective-permute-start.3
  78.5 4.2 %write.1 = (bf16[24,512,128]{2,1,0:T(8,128)(2,1)}, bf16[24,512,128]{2,1,0:T(8,128)(2,1)}) custom-call(s32[24]{0:T(128)} %prior.3, s32[24]{0:T(128)} %accepted.3, bf16[32,16,384]{2,1,0:T(8,128)(2,1)S(1)} %all_to_all.20.joined, bf16[32,16,128]{2,1,0:T(8,128)(2,1)} %combine.1.after, ...), custom_call_target="tpu_custom_call", output_to_operand_aliasing={{0}: (4, {})} | custom-call | flops 2000000000 | bytes 100000 | tf_op jit(solution)/shard_map/write/pallas_call | solution.py:553
  82.7 0.0 collective-permute-done.3.w_odd
  82.7 6.0 %all-to-all-done.3 = bf16[32,16,128]{2,1,0:T(8,128)(2,1)S(1)} async-done(((bf16[32,16,128]{2,1,0:T(8,128)(2,1)}), bf16[32,16,128]{2,1,0:T(8,128)(2,1)S(1)}, u32[]{:S(2)}, u32[]{:S(2)}) %all-to-all-start.3) | async-done | bytes 131104 | tf_op jit(solution)/shard_map/all_to_all | solution.py:542
  88.7 0.9 %output.1 = bf16[48,64]{1,0:T(8,128)(2,1)} custom-call(bf16[512,128]{1,0:T(8,128)(2,1)S(1)} %bitcast.8, bf16[4,64,128]{2,1,0:T(8,128)(2,1)S(1)} %four.1.w_even, bf16[4,64,128]{2,1,0:T(8,128)(2,1)S(1)} %collective-permute-done.3.w_odd), custom_call_target="tpu_custom_call" | custom-call | tf_op jit(solution)/shard_map/output/pallas_call | solution.py:578
Async XLA Ops:
  2.9 11.3 %copy-start.2 = (f32[24,2,512]{2,1,0:T(2,128)}, f32[24,2,512]{2,1,0:T(2,128)S(1)}, u32[]{:S(2)}) copy-start(f32[24,2,512]{2,1,0:T(2,128)S(1)} %get-tuple-element.10.biases) | copy-start | bytes 294916
  2.9 26.6 %all-to-all-start = ((bf16[32,16,384]{2,1,0:T(8,128)(2,1)}), bf16[32,16,384]{2,1,0:T(8,128)(2,1)S(1)}, u32[]{:S(2)}, u32[]{:S(2)}) async-start(bf16[32,16,384]{2,1,0:T(8,128)(2,1)} %get-tuple-element.9), calls=%async_computation | async-start | bytes 786432 | tf_op jit(solution)/shard_map/all_to_all | solution.py:489
  14.2 35.1 %copy-start = (bf16[24,512,128]{2,1,0:T(8,128)(2,1)S(1)}, bf16[24,512,128]{2,1,0:T(8,128)(2,1)}, u32[]{:S(2)}) copy-start(bf16[24,512,128]{2,1,0:T(8,128)(2,1)} %keys.1) | copy-start | bytes 9437188
  14.2 5.5 %collective-permute-start.1 = (bf16[64,128]{1,0:T(8,128)(2,1)}, bf16[64,128]{1,0:T(8,128)(2,1)S(1)}, u32[]{:S(2)}, u32[]{:S(2)}) collective-permute-start(bf16[64,128]{1,0:T(8,128)(2,1)} %bitcast.13), channel_id=1, source_target_pairs={{0,4},{1,5},{2,6},{3,7},{4,0},{5,1},{6,2},{7,3},{8,12},{9,13},{10,... | collective-permute-start | bytes 49160 | tf_op jit(solution)/shard_map/ppermute | solution.py:494
  16.6 3.9 %collective-permute-start = (bf16[64,128]{1,0:T(8,128)(2,1)}, bf16[64,128]{1,0:T(8,128)(2,1)S(1)}, u32[]{:S(2)}, u32[]{:S(2)}) collective-permute-start(bf16[64,128]{1,0:T(8,128)(2,1)} %bitcast.14), channel_id=1, source_target_pairs={{0,2},{1,3},{2,0},{3,1},{4,6},{5,7},{6,4},{7,5},{8,10},{9,11},{10,... | collective-permute-start | bytes 49160 | tf_op jit(solution)/shard_map/ppermute | solution.py:494
  19.7 10.6 %copy-start.4 = (bf16[64,128]{1,0:T(8,128)(2,1)}, bf16[64,128]{1,0:T(8,128)(2,1)S(1)}, u32[]{:S(2)}) copy-start(bf16[64,128]{1,0:T(8,128)(2,1)S(1)} %collective-permute-done.1.second) | copy-start | bytes 49156
  19.7 3.8 %collective-permute-start.2 = (bf16[64,128]{1,0:T(8,128)(2,1)S(1)}, bf16[64,128]{1,0:T(8,128)(2,1)}, u32[]{:S(2)}, u32[]{:S(2)}) collective-permute-start(bf16[64,128]{1,0:T(8,128)(2,1)S(1)} %collective-permute-done.1.second), channel_id=1, source_target_pairs={{0,2},{1,3},{2,0},{3,1},{4,6},{5,7},{6,4},{7,5},{8,10},{9,11},{10,... | collective-permute-start | bytes 49160 | tf_op jit(solution)/shard_map/ppermute | solution.py:494
  20.5 0.6 copy-start.5
  29.5 19.9 %copy-start.1 = (bf16[24,512,128]{2,1,0:T(8,128)(2,1)S(1)}, bf16[24,512,128]{2,1,0:T(8,128)(2,1)}, u32[]{:S(2)}) copy-start(bf16[24,512,128]{2,1,0:T(8,128)(2,1)} %values_in.1) | copy-start | bytes 9437188
  29.5 19.9 %copy-start.3 = (f32[24,2,512]{2,1,0:T(2,128)S(1)}, f32[24,2,512]{2,1,0:T(2,128)}, u32[]{:S(2)}) copy-start(f32[24,2,512]{2,1,0:T(2,128)} %copy-done.2) | copy-start | bytes 294916
  73.8 14.9 %all-to-all-start.3 = ((bf16[32,16,128]{2,1,0:T(8,128)(2,1)}), bf16[32,16,128]{2,1,0:T(8,128)(2,1)S(1)}, u32[]{:S(2)}, u32[]{:S(2)}) async-start(bf16[32,16,128]{2,1,0:T(8,128)(2,1)} %combine.1.after), calls=%async_computation.3 | async-start | bytes 262144 | tf_op jit(solution)/shard_map/all_to_all | solution.py:542
  78.4 4.3 %collective-permute-start.3 = (bf16[4,64,128]{2,1,0:T(8,128)(2,1)S(1)}, bf16[4,64,128]{2,1,0:T(8,128)(2,1)S(1)}, u32[]{:S(2)}, u32[]{:S(2)}) collective-permute-start(bf16[4,64,128]{2,1,0:T(8,128)(2,1)S(1)} %four.1.w_even), channel_id=1, source_target_pairs={{0,1},{1,0},{2,3},{3,2},{4,5},{5,4},{6,7},{7,6},{8,9},{9,8},{10,11... | collective-permute-start | bytes 196616 | tf_op jit(solution)/shard_map/ppermute | solution.py:494

commit v10 on v9

--- a/solution.py
+++ b/solution.py
@@ -93,7 +93,7 @@
     out[STATS + 1 :] = jnp.zeros((N_KV - STATS - 1, PROPS, ROWS), bf16)
 
 
-def share_kernel(bias, parts, after_2, after_6, out):
+def share_kernel(bias, parts, after, out):
     kv, tp = lax.axis_index(KV), lax.axis_index("tp")
     total = jnp.zeros((PROPS, ROWS), f32)
     for k in range(N_KV):
@@ -469,7 +469,7 @@
         project_kernel,
         out_shape=(
             jax.ShapeDtypeStruct((N_KV, PROPS, ROWS), bf16),
-            pltpu.VMEM(cum_gates.shape, f32),
+            jax.ShapeDtypeStruct(cum_gates.shape, f32),
         ),
         in_specs=[SM, SM, VM, VM, VM, VM, VM, VM, VM],
         out_specs=(VM, VM),
@@ -497,18 +497,26 @@
     w_4 = across(w_0, 4)
     w_2 = across(w_0, 2)
     w_6 = across(w_4, 2)
+    w_even = pl.pallas_call(
+        join_kernel,
+        out_shape=jax.ShapeDtypeStruct((4, *w_0.shape), bf16),
+        in_specs=[VM] * 4 + [ANY],
+        out_specs=VM,
+        compiler_params=limit(2),
+        name="four",
+    )(*far(w_0, w_4, w_2, w_6, parts))
 
     block = pl.pallas_call(
         share_kernel,
         out_shape=pltpu.VMEM((N_KV, PROPS, ROWS), bf16),
-        in_specs=[SM, VM, ANY, ANY],
+        in_specs=[SM, VM, ANY],
         out_specs=VM,
         compiler_params=limit(8),
         cost_estimate=pl.CostEstimate(
             flops=10_000_000_000, bytes_accessed=800_000, transcendentals=0
         ),
         name="share",
-    )(*far(gate_bias), *near(arrived), *far(w_2, w_6))
+    )(*far(gate_bias), *near(arrived), *far(w_even))
     joined = lax.all_to_all(block, KV, 0, 0, tiled=True)
 
     sent, keys_copy = pl.pallas_call(
@@ -540,14 +548,6 @@
         name="combine",
     )(*near(pieces.reshape(512, WIDTH)))
     shared = lax.all_to_all(combined, KV, 0, 0, tiled=True)
-    w_even = pl.pallas_call(
-        join_kernel,
-        out_shape=pltpu.VMEM((4, *w_0.shape), bf16),
-        in_specs=[VM] * 4 + [ANY],
-        out_specs=VM,
-        compiler_params=limit(2),
-        name="four",
-    )(*far(w_0, w_4, w_2, w_6, combined))
     w_odd = across(w_even, 1)
 
     keys_out, values_out = pl.pallas_call(

time: 90.9 us -> 91 us (level)
    all_to_all x1, waiting for transfers between devices: 5.88 us -> 4 us  [shards(): arrived = lax.all_to_all(parts, KV, 0, 0, tiled=True)]
where the time goes in v10:
time: 91 us; the launch traced here: 89.7 us
  blocking collectives  38.3 us (42%)
  starting transfers between devices  19.5 us (21%)
  waiting for transfers between devices  15.6 us (17%)
  Pallas kernels  14.3 us (16%)
  local copies, waits for them, and re-layouts  1.25 us (1%)
    all_to_all x1, blocking collectives, shards(): joined = lax.all_to_all(block, KV, 0, 0, tiled=True)  19.4 us
    all_to_all x1, blocking collectives, shards(): lax.all_to_all(sent.reshape(256, 2, WIDTH), (*KV, 'tp'), 0, 0, tiled=True)  19 us
    all_to_all x1, starting transfers between devices, shards(): arrived = lax.all_to_all(parts, KV, 0, 0, tiled=True)  11.3 us
    all_to_all x1, waiting for transfers between devices, shards(): shared = lax.all_to_all(combined, KV, 0, 0, tiled=True)  6.54 us
    ppermute x4, waiting for transfers between devices, across(): return lax.ppermute(x, 'tp', [(i, i ^ bit) for i in range(tp_count)])  5.1 us
    pallas_call x1, Pallas kernels, shards(): pl.pallas_call(write_kernel, out_shape=(cache, cache), in_specs=[SM, SM,...  4.34 us
    ppermute x4, starting transfers between devices, across(): return lax.ppermute(x, 'tp', [(i, i ^ bit) for i in range(tp_count)])  4.31 us
    pallas_call x1, Pallas kernels, shards(): pl.pallas_call(attention_kernel, out_shape=(pltpu.VMEM((512, WIDTH), bf16...  4.02 us
  transfers between devices with their start and end apart: 6, of which 5 were waited for; matrix products, arithmetic and copies ran while one was open for 0% of the time, Pallas kernels for 6%

profile of v10, /device:TPU:8, one launch (start us, length us, event | category | flops | bytes accessed | tf_op | source)
XLA Modules:
  0.0 89.7 jit_solution(4234882211638076955)
XLA Ops:
  0.6 2.2 %project.1 = (bf16[32,16,384]{2,1,0:T(8,128)(2,1)}, f32[24,2,512]{2,1,0:T(2,128)}) custom-call(s32[24]{0:T(128)} %prior.3, s32[24]{0:T(128)} %accepted.3, bf16[64,384]{1,0:T(8,128)(2,1)} %bitcast.12, f32[1,64]{1,0:T(1,128)} %bitcast.17, bf16[64,128]{1,0:T(8,128)(2,1)} %w_q.1, bf16[64,128]{1,0:T(8,128)(2,1)} %w_k.1, bf16[64,128]{1,0:T(8,128)(2,1)} %w_v.1, ...), custom_call_target="tpu_custom_call" | custom-call | tf_op jit(solution)/shard_map/project/pallas_call | solution.py:468
  2.9 11.3 %all-to-all-start = ((bf16[32,16,384]{2,1,0:T(8,128)(2,1)}), bf16[32,16,384]{2,1,0:T(8,128)(2,1)S(1)}, u32[]{:S(2)}, u32[]{:S(2)}) async-start(bf16[32,16,384]{2,1,0:T(8,128)(2,1)} %get-tuple-element.9.after), calls=%async_computation | async-start | bytes 786432 | tf_op jit(solution)/shard_map/all_to_all | solution.py:489
  14.2 2.4 %collective-permute-start = (bf16[64,128]{1,0:T(8,128)(2,1)}, bf16[64,128]{1,0:T(8,128)(2,1)S(1)}, u32[]{:S(2)}, u32[]{:S(2)}) collective-permute-start(bf16[64,128]{1,0:T(8,128)(2,1)} %bitcast.13), channel_id=1, source_target_pairs={{0,4},{1,5},{2,6},{3,7},{4,0},{5,1},{6,2},{7,3},{8,12},{9,13},{10,... | collective-permute-start | bytes 49160 | tf_op jit(solution)/shard_map/ppermute | solution.py:494
  16.6 1.3 %collective-permute-start.1 = (bf16[64,128]{1,0:T(8,128)(2,1)}, bf16[64,128]{1,0:T(8,128)(2,1)S(1)}, u32[]{:S(2)}, u32[]{:S(2)}) collective-permute-start(bf16[64,128]{1,0:T(8,128)(2,1)} %bitcast.14), channel_id=1, source_target_pairs={{0,2},{1,3},{2,0},{3,1},{4,6},{5,7},{6,4},{7,5},{8,10},{9,11},{10,... | collective-permute-start | bytes 49160 | tf_op jit(solution)/shard_map/ppermute | solution.py:494
  17.9 1.8 %collective-permute-done.second = bf16[64,128]{1,0:T(8,128)(2,1)S(1)} collective-permute-done((bf16[64,128]{1,0:T(8,128)(2,1)}, bf16[64,128]{1,0:T(8,128)(2,1)S(1)}, u32[]{:S(2)}, u32[]{:S(2)}) %collective-permute-start) | collective-permute-done | bytes 16416 | tf_op jit(solution)/shard_map/ppermute | solution.py:494
  19.7 0.0 copy-start.5
  19.7 0.5 collective-permute-start.2
  20.2 0.3 collective-permute-done.1.third
  20.5 0.0 copy-start.6
  20.5 2.9 %collective-permute-done.2.fourth = bf16[64,128]{1,0:T(8,128)(2,1)S(1)} collective-permute-done((bf16[64,128]{1,0:T(8,128)(2,1)S(1)}, bf16[64,128]{1,0:T(8,128)(2,1)S(1)}, u32[]{:S(2)}, u32[]{:S(2)}) %collective-permute-start.2) | collective-permute-done | bytes 16416 | tf_op jit(solution)/shard_map/ppermute | solution.py:494
  23.5 0.0 copy-done.5
  23.5 0.0 copy-done.6
  23.5 0.0 copy-start.7
  23.5 0.6 copy-done.7
  24.1 0.8 four.1.after.w_even
  24.8 0.0 copy-start.2
  24.8 0.6 copy-done.2
  25.5 0.0 copy-start
  25.5 4.0 %all-to-all-done.parts = bf16[32,16,384]{2,1,0:T(8,128)(2,1)S(1)} async-done(((bf16[32,16,384]{2,1,0:T(8,128)(2,1)}), bf16[32,16,384]{2,1,0:T(8,128)(2,1)S(1)}, u32[]{:S(2)}, u32[]{:S(2)}) %all-to-all-start) | async-done | bytes 393248 | tf_op jit(solution)/shard_map/all_to_all | solution.py:489
  29.5 0.0 copy-start.1
  29.5 0.0 copy-start.4
  29.5 0.9 %share.1 = bf16[32,16,384]{2,1,0:T(8,128)(2,1)S(1)} custom-call(f32[16]{0:T(128)} %bias.1, bf16[32,16,384]{2,1,0:T(8,128)(2,1)S(1)} %all-to-all-done.parts, bf16[4,64,128]{2,1,0:T(8,128)(2,1)} %copy-done.2), custom_call_target="tpu_custom_call" | custom-call | flops 10000000000 | bytes 800000 | tf_op jit(solution)/shard_map/share/pallas_call | solution.py:509
  30.4 19.4 %all_to_all.20.joined = bf16[32,16,384]{2,1,0:T(8,128)(2,1)S(1)} all-to-all(bf16[32,16,384]{2,1,0:T(8,128)(2,1)S(1)} %share.1), channel_id=1, replica_groups=mesh['kv_0'=8,'kv_1'=4,'tp'=8] {'kv_0','kv_1'}, dimensions={0} | all-to-all | bytes 786432 | tf_op jit(solution)/shard_map/all_to_all | solution.py:520
  49.8 0.0 copy-done
  49.8 0.0 copy-done.1
  49.8 0.0 copy-done.4
  49.8 4.0 %attention.1 = (bf16[512,128]{1,0:T(8,128)(2,1)S(1)}, bf16[24,512,128]{2,1,0:T(8,128)(2,1)}) custom-call(s32[16,24]{1,0:T(8,128)} %bitcast.16, bf16[32,16,384]{2,1,0:T(8,128)(2,1)S(1)} %all_to_all.20.joined, f32[24,2,512]{2,1,0:T(2,128)S(1)} %copy-done.4, bf16[24,512,128]{2,1,0:T(8,128)(2,1)S(1)} %copy-done, bf16[24,512,128]{2,1,0:T(8,128)(2,1)S(1)} %copy-done.1), custom_call_target="tpu_custom_call" | custom-call | tf_op jit(solution)/shard_map/attention/pallas_call | solution.py:522
  53.8 19.0 %all_to_all.21 = bf16[256,2,128]{2,1,0:T(2,128)(2,1)S(1)} all-to-all(bf16[256,2,128]{2,1,0:T(2,128)(2,1)S(1)} %bitcast.10), channel_id=1, replica_groups=mesh['kv_0'=8,'kv_1'=4,'tp'=8] {'kv_0','kv_1','tp'}, dimensions={0} | all-to-all | bytes 262144 | tf_op jit(solution)/shard_map/all_to_all | solution.py:539
  72.8 1.1 %combine.1.after = bf16[32,16,128]{2,1,0:T(8,128)(2,1)} custom-call(bf16[512,128]{1,0:T(8,128)(2,1)S(1)} %bitcast.9), custom_call_target="tpu_custom_call" | custom-call | tf_op jit(solution)/shard_map/combine/pallas_call | solution.py:541
  73.9 3.9 %all-to-all-start.3 = ((bf16[32,16,128]{2,1,0:T(8,128)(2,1)}), bf16[32,16,128]{2,1,0:T(8,128)(2,1)S(1)}, u32[]{:S(2)}, u32[]{:S(2)}) async-start(bf16[32,16,128]{2,1,0:T(8,128)(2,1)} %combine.1.after), calls=%async_computation.3 | async-start | bytes 262144 | tf_op jit(solution)/shard_map/all_to_all | solution.py:550
  77.7 0.1 collective-permute-start.3
  77.9 0.0 copy-start.3
  77.9 4.3 %write.1 = (bf16[24,512,128]{2,1,0:T(8,128)(2,1)}, bf16[24,512,128]{2,1,0:T(8,128)(2,1)}) custom-call(s32[24]{0:T(128)} %prior.3, s32[24]{0:T(128)} %accepted.3, bf16[32,16,384]{2,1,0:T(8,128)(2,1)S(1)} %all_to_all.20.joined, bf16[32,16,128]{2,1,0:T(8,128)(2,1)} %combine.1.after, ...), custom_call_target="tpu_custom_call", output_to_operand_aliasing={{0}: (4, {})} | custom-call | flops 2000000000 | bytes 100000 | tf_op jit(solution)/shard_map/write/pallas_call | solution.py:553
  82.2 0.0 collective-permute-done.3.w_odd
  82.2 6.5 %all-to-all-done.3 = bf16[32,16,128]{2,1,0:T(8,128)(2,1)S(1)} async-done(((bf16[32,16,128]{2,1,0:T(8,128)(2,1)}), bf16[32,16,128]{2,1,0:T(8,128)(2,1)S(1)}, u32[]{:S(2)}, u32[]{:S(2)}) %all-to-all-start.3) | async-done | bytes 131104 | tf_op jit(solution)/shard_map/all_to_all | solution.py:550
  88.8 0.0 copy-done.3
  88.8 0.9 %output.1 = bf16[48,64]{1,0:T(8,128)(2,1)} custom-call(bf16[512,128]{1,0:T(8,128)(2,1)S(1)} %bitcast.8, bf16[4,64,128]{2,1,0:T(8,128)(2,1)S(1)} %copy-done.3, bf16[4,64,128]{2,1,0:T(8,128)(2,1)S(1)} %collective-permute-done.3.w_odd), custom_call_target="tpu_custom_call" | custom-call | tf_op jit(solution)/shard_map/output/pallas_call | solution.py:578
Async XLA Ops:
  2.9 26.6 %all-to-all-start = ((bf16[32,16,384]{2,1,0:T(8,128)(2,1)}), bf16[32,16,384]{2,1,0:T(8,128)(2,1)S(1)}, u32[]{:S(2)}, u32[]{:S(2)}) async-start(bf16[32,16,384]{2,1,0:T(8,128)(2,1)} %get-tuple-element.9.after), calls=%async_computation | async-start | bytes 786432 | tf_op jit(solution)/shard_map/all_to_all | solution.py:489
  14.2 5.5 %collective-permute-start = (bf16[64,128]{1,0:T(8,128)(2,1)}, bf16[64,128]{1,0:T(8,128)(2,1)S(1)}, u32[]{:S(2)}, u32[]{:S(2)}) collective-permute-start(bf16[64,128]{1,0:T(8,128)(2,1)} %bitcast.13), channel_id=1, source_target_pairs={{0,4},{1,5},{2,6},{3,7},{4,0},{5,1},{6,2},{7,3},{8,12},{9,13},{10,... | collective-permute-start | bytes 49160 | tf_op jit(solution)/shard_map/ppermute | solution.py:494
  16.6 3.9 %collective-permute-start.1 = (bf16[64,128]{1,0:T(8,128)(2,1)}, bf16[64,128]{1,0:T(8,128)(2,1)S(1)}, u32[]{:S(2)}, u32[]{:S(2)}) collective-permute-start(bf16[64,128]{1,0:T(8,128)(2,1)} %bitcast.14), channel_id=1, source_target_pairs={{0,2},{1,3},{2,0},{3,1},{4,6},{5,7},{6,4},{7,5},{8,10},{9,11},{10,... | collective-permute-start | bytes 49160 | tf_op jit(solution)/shard_map/ppermute | solution.py:494
  19.7 3.7 %copy-start.5 = (bf16[64,128]{1,0:T(8,128)(2,1)}, bf16[64,128]{1,0:T(8,128)(2,1)S(1)}, u32[]{:S(2)}) copy-start(bf16[64,128]{1,0:T(8,128)(2,1)S(1)} %collective-permute-done.second) | copy-start | bytes 49156
  19.7 3.7 %collective-permute-start.2 = (bf16[64,128]{1,0:T(8,128)(2,1)S(1)}, bf16[64,128]{1,0:T(8,128)(2,1)S(1)}, u32[]{:S(2)}, u32[]{:S(2)}) collective-permute-start(bf16[64,128]{1,0:T(8,128)(2,1)S(1)} %collective-permute-done.second), channel_id=1, source_target_pairs={{0,2},{1,3},{2,0},{3,1},{4,6},{5,7},{6,4},{7,5},{8,10},{9,11},{10,... | collective-permute-start | bytes 49160 | tf_op jit(solution)/shard_map/ppermute | solution.py:494
  20.5 3.0 %copy-start.6 = (bf16[64,128]{1,0:T(8,128)(2,1)}, bf16[64,128]{1,0:T(8,128)(2,1)S(1)}, u32[]{:S(2)}) copy-start(bf16[64,128]{1,0:T(8,128)(2,1)S(1)} %collective-permute-done.1.third) | copy-start | bytes 49156
  23.5 0.6 copy-start.7
  24.8 0.6 copy-start.2
  25.5 24.3 %copy-start = (bf16[24,512,128]{2,1,0:T(8,128)(2,1)S(1)}, bf16[24,512,128]{2,1,0:T(8,128)(2,1)}, u32[]{:S(2)}) copy-start(bf16[24,512,128]{2,1,0:T(8,128)(2,1)} %keys.1) | copy-start | bytes 9437188
  29.5 20.3 %copy-start.1 = (bf16[24,512,128]{2,1,0:T(8,128)(2,1)S(1)}, bf16[24,512,128]{2,1,0:T(8,128)(2,1)}, u32[]{:S(2)}) copy-start(bf16[24,512,128]{2,1,0:T(8,128)(2,1)} %values_in.1) | copy-start | bytes 9437188
  29.5 20.3 %copy-start.4 = (f32[24,2,512]{2,1,0:T(2,128)S(1)}, f32[24,2,512]{2,1,0:T(2,128)}, u32[]{:S(2)}) copy-start(f32[24,2,512]{2,1,0:T(2,128)} %get-tuple-element.10.biases) | copy-start | bytes 294916
  73.9 14.9 %all-to-all-start.3 = ((bf16[32,16,128]{2,1,0:T(8,128)(2,1)}), bf16[32,16,128]{2,1,0:T(8,128)(2,1)S(1)}, u32[]{:S(2)}, u32[]{:S(2)}) async-start(bf16[32,16,128]{2,1,0:T(8,128)(2,1)} %combine.1.after), calls=%async_computation.3 | async-start | bytes 262144 | tf_op jit(solution)/shard_map/all_to_all | solution.py:550
  77.7 4.5 %collective-permute-start.3 = (bf16[4,64,128]{2,1,0:T(8,128)(2,1)}, bf16[4,64,128]{2,1,0:T(8,128)(2,1)S(1)}, u32[]{:S(2)}, u32[]{:S(2)}) collective-permute-start(bf16[4,64,128]{2,1,0:T(8,128)(2,1)} %copy-done.2), channel_id=1, source_target_pairs={{0,1},{1,0},{2,3},{3,2},{4,5},{5,4},{6,7},{7,6},{8,9},{9,8},{10,11... | collective-permute-start | bytes 196616 | tf_op jit(solution)/shard_map/ppermute | solution.py:494
  77.9 10.9 %copy-start.3 = (bf16[4,64,128]{2,1,0:T(8,128)(2,1)S(1)}, bf16[4,64,128]{2,1,0:T(8,128)(2,1)}, u32[]{:S(2)}) copy-start(bf16[4,64,128]{2,1,0:T(8,128)(2,1)} %copy-done.2) | copy-start | bytes 196612
